TPU v7x, 256 devices: a whole 4x4x8 slice. The times are simulated.
256 devices in a mesh: ep: 16 (over y, x), tp: 16 (over z, core).
Axes of the slice: x: 4, y: 4, z: 8, core: 2. Of those that a mesh axis runs over, the one named last changes fastest.
Arguments:
- tokens: bfloat16 [3072, 2048], P('ep'), may hold values from -6 to 6
- cotangent: bfloat16 [3072, 2048], P('ep'), may hold values from -6 to 6
- routing: int32 [3072, 2], P('ep'), may hold values from 0 to 15, all different within a row; in each aligned block of 192 rows (0 to 191, 192 to 383, ...) at most 48 rows name the same one
- gate_weights: bfloat16 [3072, 2], P('ep'), may hold values from 0.19921875 to 1
- gate_proj: bfloat16 [16, 2048, 7168], P('ep', None, 'tp'), may hold values from -0.125 to 0.125
- up_proj: bfloat16 [16, 2048, 7168], P('ep', None, 'tp'), may hold values from -0.125 to 0.125
- down_proj: bfloat16 [16, 7168, 2048], P('ep', 'tp'), may hold values from -0.0625 to 0.0625
Outputs:
- grad_tokens: bfloat16 [3072, 2048], P('ep', 'tp')
- grad_gates: float32 [3072, 2], P('ep')
- grad_gate_proj: bfloat16 [16, 2048, 7168], P('ep', None, 'tp')
- grad_up_proj: bfloat16 [16, 2048, 7168], P('ep', None, 'tp')
- grad_down_proj: bfloat16 [16, 7168, 2048], P('ep', 'tp')
Inputs may be any that keep to these rules, and one draw needn't show every extreme that they name: `routing`: each row names 2 different experts. Within each aligned block of 192 rows no expert is named by more than 48 rows, and in every draw some expert is named by exactly 48 rows of some block.
All inputs are finite; a program needn't handle non-finite values.
Results may differ from a plain program's by a relative error of at most 0.019.
Values may be sent and summed in bfloat16 or wider, within the bound.
No kernel may reach another device: no remote copies, remote signals or barrier semaphores. Data moves between devices by JAX's collectives and lax.ppermute only.
A program may use at most 128 MiB of HBM per device.

v0:
```python
import jax
import jax.numpy as jnp
from jax import lax
from jax.sharding import PartitionSpec as P


def side_by_side(arrays, axis, dim, along):
    widths = [a.shape[along] for a in arrays]
    both = jnp.concatenate(arrays, axis=along)
    out = lax.all_gather(both, axis, axis=dim, tiled=True)
    return tuple(jnp.split(out, [sum(widths[:k]) for k in range(1, len(widths))], axis=along))


def copy_for_each(shard, axis):
    count = lax.axis_size(axis)
    return lax.all_to_all(
        jnp.broadcast_to(shard[None], (count, *shard.shape)), axis, 0, 0, tiled=True
    )


def of_everyone(shard, axis):
    everything = copy_for_each(shard, axis)
    return jnp.sum(everything, axis=0)


def expert_backward(in_rows, cot_rows, gate_col, w_gate, w_up, w_down):
    gate_pre = jnp.dot(in_rows, w_gate, preferred_element_type=jnp.float32)
    up_value = jnp.dot(in_rows, w_up, preferred_element_type=jnp.float32)
    sigmoid_val = jax.nn.sigmoid(gate_pre)
    active = gate_pre * sigmoid_val
    hidden = (active * up_value).astype(jnp.bfloat16)
    contract_cols = (((1,), (1,)), ((), ()))
    contract_rows = (((0,), (0,)), ((), ()))
    back_hidden = lax.dot_general(
        cot_rows, w_down, contract_cols, preferred_element_type=jnp.float32
    )
    gate_part = jnp.sum(hidden.astype(jnp.float32) * back_hidden, axis=1)
    scaled_back = gate_col * back_hidden
    grad_pre = (
        scaled_back * up_value * sigmoid_val * (1.0 + gate_pre * (1.0 - sigmoid_val))
    ).astype(jnp.bfloat16)
    grad_upval = (scaled_back * active).astype(jnp.bfloat16)
    scaled_cot = (gate_col * cot_rows.astype(jnp.float32)).astype(jnp.bfloat16)
    grad_down = lax.dot_general(
        hidden, scaled_cot, contract_rows, preferred_element_type=jnp.float32
    ).astype(jnp.bfloat16)
    grad_gate = lax.dot_general(
        in_rows, grad_pre, contract_rows, preferred_element_type=jnp.float32
    ).astype(jnp.bfloat16)
    grad_upw = lax.dot_general(
        in_rows, grad_upval, contract_rows, preferred_element_type=jnp.float32
    ).astype(jnp.bfloat16)
    grad_in = lax.dot_general(grad_pre, w_gate, contract_cols, preferred_element_type=jnp.float32)
    grad_in = grad_in + lax.dot_general(
        grad_upval, w_up, contract_cols, preferred_element_type=jnp.float32
    )
    return (grad_in, gate_part, grad_gate, grad_upw, grad_down)


def local(tokens, cotangent, routing, gate_weights, gate_proj, up_proj, down_proj):
    expert_count = lax.axis_size("ep")
    tok_rows, model_width = tokens.shape
    top_k = routing.shape[1]
    capacity = 2 * tok_rows * top_k // expert_count
    flat_routes = routing.reshape(-1)
    onehot = (flat_routes[:, None] == jnp.arange(expert_count, dtype=jnp.int32)[None, :]).astype(
        jnp.int32
    )
    position = jnp.sum(jnp.cumsum(onehot, axis=0) * onehot, axis=1) - 1
    slot_index = flat_routes * capacity + position
    slot_owner = (
        jnp.full((expert_count * capacity,), -1, jnp.int32)
        .at[slot_index]
        .set(jnp.arange(flat_routes.shape[0], dtype=jnp.int32))
    )
    is_used = slot_owner >= 0
    safe_owner = jnp.where(is_used, slot_owner, 0)
    token_index = safe_owner // top_k
    slot_gates = jnp.where(
        is_used, gate_weights.reshape(-1)[safe_owner], jnp.zeros((), jnp.bfloat16)
    )
    slot_gates = slot_gates.reshape(expert_count, capacity)

    def gather_slots(source):
        picked_rows = jnp.where(is_used[:, None], source[token_index], jnp.zeros((), jnp.bfloat16))
        return picked_rows.reshape(expert_count, capacity, source.shape[1])

    col_width = model_width // lax.axis_size("tp")
    col_start = lax.axis_index("tp") * col_width
    token_cols = lax.dynamic_slice_in_dim(tokens, col_start, col_width, 1)
    cot_cols = lax.dynamic_slice_in_dim(cotangent, col_start, col_width, 1)
    rows_part, cots_part, gates_in = (
        lax.all_to_all(gather_slots(token_cols), "ep", split_axis=0, concat_axis=0, tiled=True),
        lax.all_to_all(gather_slots(cot_cols), "ep", split_axis=0, concat_axis=0, tiled=True),
        lax.all_to_all(slot_gates, "ep", split_axis=0, concat_axis=0, tiled=True),
    )
    in_rows, cot_in = side_by_side((rows_part, cots_part), "tp", 2, 0)
    slot_count = in_rows.shape[0] * in_rows.shape[1]
    grad_in, gate_part, grad_gate, grad_upw, grad_down = expert_backward(
        in_rows.reshape(slot_count, model_width),
        cot_in.reshape(slot_count, model_width),
        gates_in.reshape(slot_count, 1).astype(jnp.float32),
        gate_proj[0],
        up_proj[0],
        down_proj[0],
    )
    gate_total = of_everyone(gate_part, "tp")
    grad_cols = lax.psum_scatter(
        grad_in.astype(jnp.bfloat16), "tp", scatter_dimension=1, tiled=True
    ).astype(jnp.float32)
    back_rows, back_gates = (
        lax.all_to_all(
            grad_cols.reshape(expert_count, capacity, grad_cols.shape[1]).astype(jnp.bfloat16),
            "ep",
            split_axis=0,
            concat_axis=0,
            tiled=True,
        ).astype(jnp.float32),
        lax.all_to_all(
            gate_total.reshape(expert_count, capacity).astype(jnp.bfloat16),
            "ep",
            split_axis=0,
            concat_axis=0,
            tiled=True,
        ).astype(jnp.float32),
    )
    picked = back_rows.reshape(expert_count * capacity, back_rows.shape[2])[slot_index]
    grad_tokens = jnp.sum(picked.reshape(tok_rows, top_k, picked.shape[1]), axis=1).astype(
        jnp.bfloat16
    )
    grad_gates = back_gates.reshape(-1)[slot_index].reshape(tok_rows, top_k)
    return (grad_tokens, grad_gates, grad_gate[None], grad_upw[None], grad_down[None])


def solution(mesh):
    return jax.shard_map(
        local,
        mesh=mesh,
        in_specs=(
            P("ep", None),
            P("ep", None),
            P("ep", None),
            P("ep", None),
            P("ep", None, "tp"),
            P("ep", None, "tp"),
            P("ep", "tp", None),
        ),
        out_specs=(
            P("ep", "tp"),
            P("ep", None),
            P("ep", None, "tp"),
            P("ep", None, "tp"),
            P("ep", "tp", None),
        ),
        check_vma=False,
    )
```

profile of v0, /device:TPU:1, one launch (start us, length us, event | category | flops | bytes accessed | tf_op | source)
XLA Modules:
  0.0 206.7 jit_solution(3970222531800738396)
XLA Ops:
  7.2 0.8 broadcast_multiply_fusion
  8.0 0.8 copy.35
  8.8 0.1 eq.29
  9.0 0.1 eq.25
  9.1 0.1 copy.34
  9.3 0.1 mul.64
  9.4 0.9 reduce-window.6
  10.3 0.2 slice_reduce_fusion
  10.5 0.1 fusion.17
  10.7 2.9 %scatter_custom_fusion = s32[768]{0:T(1024)S(1)} fusion(s32[384]{0:T(512)S(1)} %fusion.23, s32[384]{0:T(512)S(1)} %iota.11, s32[]{:T(128)} %constant.13.clone.1), kind=kCustom, calls=%fused_computation.59 | custom fusion | bytes 3076 | tf_op jit(solution)/shard_map/scatter | solution.py:74
  13.6 0.1 broadcast_in_dim.58
  13.7 0.8 constant_dynamic-slice_fusion
  14.6 1.9 gather_fusion.2
  16.5 1.9 gather_fusion.1
  18.4 0.2 broadcast_select_fusion.1
  18.5 14.6 %all_to_all.37 = bf16[16,48,128]{2,1,0:T(8,128)(2,1)S(1)} all-to-all(bf16[16,48,128]{2,1,0:T(8,128)(2,1)S(1)} %get-tuple-element.33), channel_id=1, replica_groups=mesh['ep'=16,'tp'=16] {'ep'}, dimensions={0} | all-to-all | bytes 393216 | tf_op jit(solution)/shard_map/all_to_all | solution.py:93
  33.1 10.2 %all_to_all.38 = bf16[16,48,128]{2,1,0:T(8,128)(2,1)S(1)} all-to-all(bf16[16,48,128]{2,1,0:T(8,128)(2,1)S(1)} %get-tuple-element.34), channel_id=1, replica_groups=mesh['ep'=16,'tp'=16] {'ep'}, dimensions={0} | all-to-all | bytes 393216 | tf_op jit(solution)/shard_map/all_to_all | solution.py:94
  43.3 0.8 pad_maximum_fusion
  44.1 0.1 copy.38
  44.3 0.2 reshape.138
  44.5 5.0 %gather_fusion = bf16[768]{0:T(1024)(128)(2,1)S(1)} fusion(bf16[384]{0:T(512)(128)(2,1)S(1)} %reshape.138, s32[1024]{0:T(1024)S(1)} %pad_clamp_fusion.2), kind=kCustom, calls=%fused_computation | custom fusion | bytes 6144 | tf_op jit(solution)/shard_map/gather | solution.py:80
  49.5 0.1 all_to_all.30
  49.6 9.4 %all_to_all.39 = bf16[16,1,48]{2,1,0:T(2,128)(2,1)S(1)} all-to-all(bf16[16,1,48]{2,1,0:T(2,128)(2,1)S(1)} %all_to_all.30), channel_id=1, replica_groups=mesh['ep'=16,'tp'=16] {'ep'}, dimensions={0} | all-to-all | bytes 3072 | tf_op jit(solution)/shard_map/all_to_all | solution.py:95
  59.1 44.2 %all-gather.2.cloned.1.call-done = bf16[32,48,2048]{2,1,0:T(8,128)(2,1)} async-done(((bf16[32,48,128]{2,1,0:T(8,128)(2,1)}), bf16[32,48,2048]{2,1,0:T(8,128)(2,1)}) %all-gather.2.cloned.1.call-update) | async-done | bytes 6291472 | tf_op jit(solution)/shard_map/all_gather | solution.py:10
  103.3 3.4 %fusion.24 = (bf16[16,48,2048]{2,1,0:T(8,128)(2,1)S(1)}, bf16[16,48,2048]{2,1,0:T(8,128)(2,1)S(1)}) fusion(bf16[32,48,2048]{2,1,0:T(8,128)(2,1)} %all-gather.2.cloned.1.call-done), kind=kLoop, calls=%fused_computation.67 | loop fusion | bytes 12582912 | tf_op jit(solution)/shard_map/split | solution.py:11
  106.7 1.6 fusion.8
  108.4 1.2 copy-done.5
  109.6 1.6 fusion.11
  111.3 3.0 %multiply_reduce_fusion = (f32[768]{0:T(1024)S(1)}, bf16[768,448]{0,1:T(8,128)(2,1)}, bf16[768,448]{0,1:T(8,128)(2,1)S(1)}, bf16[768,448]{0,1:T(8,128)(2,1)S(1)}) fusion(f32[768,448]{0,1:T(8,128)S(1)} %fusion.11, f32[768,448]{0,1:T(8,128)S(1)} %fusion.8, f32[768]{0:T(1024)S(1)} %reshape.145, bf16[768,2048]{1,0:T(8,128)(2,1)S(1)} %bitcast.64, ...), kind=kOutput, calls=%fused_computation.25 | convolution fusion | flops 1415822592 | bytes 9803776 | tf_op jit(solution)/shard_map/dot_general | solution.py:34
  114.3 1.8 fusion.6
  116.2 3.5 %add_convert_fusion = bf16[768,2048]{1,0:T(8,128)(2,1)} fusion(f32[768,2048]{1,0:T(8,128)S(1)} %fusion.6, bf16[768,448]{0,1:T(8,128)(2,1)S(1)} %get-tuple-element.32, bf16[1,2048,448]{1,2,0:T(8,128)(2,1)S(1)} %copy-done.5), kind=kOutput, calls=%fused_computation.7 | convolution fusion | flops 1412431872 | bytes 11960320 | tf_op jit(solution)/shard_map/dot_general | solution.py:54
  119.6 4.7 %copy.43 = bf16[768,2048]{0,1:T(8,128)(2,1)} copy(bf16[768,2048]{1,0:T(8,128)(2,1)} %add_convert_fusion) | data formatting | bytes 6291456
  124.4 0.6 broadcast_in_dim.62
  125.0 5.2 %all-to-all-start.4 = ((f32[16,1,768]{2,1,0:T(1,128)}), f32[16,1,768]{2,1,0:T(1,128)S(1)}, u32[]{:S(2)}, u32[]{:S(2)}) async-start(f32[16,1,768]{2,1,0:T(1,128)} %broadcast_in_dim.62), calls=%async_computation.4 | async-start | bytes 98304 | tf_op jit(solution)/shard_map/all_to_all | solution.py:16
  130.2 5.0 %fusion.5 = bf16[1,448,2048]{2,1,0:T(8,128)(2,1)} fusion(bf16[768,448]{0,1:T(8,128)(2,1)} %get-tuple-element.26, bf16[768,2048]{1,0:T(8,128)(2,1)} %bitcast.65, f32[768]{0:T(1024)S(1)} %reshape.145), kind=kOutput, calls=%fused_computation.15 | convolution fusion | flops 1414922240 | bytes 5671936 | tf_op jit(solution)/shard_map/dot_general | solution.py:44
  135.2 2.5 %all-to-all-done.4 = f32[16,1,768]{2,1,0:T(1,128)S(1)} async-done(((f32[16,1,768]{2,1,0:T(1,128)}), f32[16,1,768]{2,1,0:T(1,128)S(1)}, u32[]{:S(2)}, u32[]{:S(2)}) %all-to-all-start.4) | async-done | bytes 49184 | tf_op jit(solution)/shard_map/all_to_all | solution.py:16
  137.8 0.7 convert_element_type.96
  138.4 6.5 %all-to-all-start.5 = ((bf16[16,1,48]{2,1,0:T(2,128)(2,1)}), bf16[16,1,48]{2,1,0:T(2,128)(2,1)S(1)}, u32[]{:S(2)}, u32[]{:S(2)}) async-start(bf16[16,1,48]{2,1,0:T(2,128)(2,1)} %convert_element_type.96), calls=%async_computation.5 | async-start | bytes 16384 | tf_op jit(solution)/shard_map/all_to_all | solution.py:119
  145.0 4.7 %fusion.3 = bf16[1,2048,448]{1,2,0:T(8,128)(2,1)} fusion(bf16[768,448]{0,1:T(8,128)(2,1)S(1)} %get-tuple-element.31, bf16[768,2048]{1,0:T(8,128)(2,1)} %bitcast.62), kind=kOutput, calls=%fused_computation.13 | convolution fusion | flops 1410203648 | bytes 5668864 | tf_op jit(solution)/shard_map/dot_general | solution.py:47
  149.7 32.5 %reduce-scatter.4.cloned.1.call-done = bf16[128,768]{1,0:T(8,128)(2,1)} async-done(((bf16[2048,768]{1,0:T(8,128)(2,1)}), bf16[128,768]{1,0:T(8,128)(2,1)}) %reduce-scatter.4.cloned.1.call-update) | async-done | bytes 196624
  182.2 1.7 copy.44
  183.9 6.2 %all-to-all-start.3 = ((bf16[16,48,128]{2,1,0:T(8,128)(2,1)}), bf16[16,48,128]{2,1,0:T(8,128)(2,1)S(1)}, u32[]{:S(2)}, u32[]{:S(2)}) async-start(bf16[16,48,128]{2,1,0:T(8,128)(2,1)} %bitcast.8), calls=%async_computation.3 | async-start | bytes 393216 | tf_op jit(solution)/shard_map/all_to_all | solution.py:112
  190.1 4.9 %fusion.4 = bf16[1,2048,448]{1,2,0:T(8,128)(2,1)} fusion(bf16[768,448]{0,1:T(8,128)(2,1)} %copy-done.6, bf16[768,2048]{1,0:T(8,128)(2,1)} %bitcast.63), kind=kOutput, calls=%fused_computation.14 | convolution fusion | flops 1410203648 | bytes 5668864 | tf_op jit(solution)/shard_map/dot_general | solution.py:50
  195.2 1.9 gather_fusion.4
  197.0 0.1 reshape.144
  197.2 0.7 copy.42
  197.9 1.1 gather_fusion.3
  199.0 0.9 reduce_sum.37
  (36 shorter events, 0.6 us)
Async XLA Ops:
  7.2 99.6 %copy-start = (bf16[1,2048,448]{1,2,0:T(8,128)(2,1)S(1)}, bf16[1,2048,448]{1,2,0:T(8,128)(2,1)}, u32[]{:S(2)}) copy-start(bf16[1,2048,448]{1,2,0:T(8,128)(2,1)} %param.11) | copy-start | bytes 5505028
  7.2 96.1 %all-gather.2.cloned.1.call-start = ((), (), s32[]{:S(2)}) async-start(), calls=%async_computation.7 | async-start | bytes 6684672 | tf_op jit(solution)/shard_map/all_gather | solution.py:10
  16.5 27.7 %copy-start.3 = (bf16[192,2]{0,1:T(2,128)(2,1)S(1)}, bf16[192,2]{0,1:T(2,128)(2,1)}, u32[]{:S(2)}) copy-start(bf16[192,2]{0,1:T(2,128)(2,1)} %param.10) | copy-start | bytes 2308
  44.1 138.1 %reduce-scatter.4.cloned.1.call-start = ((), (), s32[]{:S(2)}) async-start(), calls=%async_computation.8 | async-start | bytes 3342336
  106.7 1.7 copy-start.1
  106.7 4.5 %copy-start.2 = (bf16[16,48,2048]{2,1,0:T(8,128)(2,1)}, bf16[16,48,2048]{2,1,0:T(8,128)(2,1)S(1)}, u32[]{:S(2)}) copy-start(bf16[16,48,2048]{2,1,0:T(8,128)(2,1)S(1)} %get-tuple-element.29) | copy-start | bytes 9437188
  106.7 2.9 %copy-start.5 = (bf16[1,2048,448]{1,2,0:T(8,128)(2,1)S(1)}, bf16[1,2048,448]{1,2,0:T(8,128)(2,1)}, u32[]{:S(2)}) copy-start(bf16[1,2048,448]{1,2,0:T(8,128)(2,1)} %param.12) | copy-start | bytes 5505028
  109.6 1.6 copy-start.4
  114.3 1.8 copy-start.6
  125.0 12.7 %all-to-all-start.4 = ((f32[16,1,768]{2,1,0:T(1,128)}), f32[16,1,768]{2,1,0:T(1,128)S(1)}, u32[]{:S(2)}, u32[]{:S(2)}) async-start(f32[16,1,768]{2,1,0:T(1,128)} %broadcast_in_dim.62), calls=%async_computation.4 | async-start | bytes 98304 | tf_op jit(solution)/shard_map/all_to_all | solution.py:16
  138.4 45.4 %all-to-all-start.5 = ((bf16[16,1,48]{2,1,0:T(2,128)(2,1)}), bf16[16,1,48]{2,1,0:T(2,128)(2,1)S(1)}, u32[]{:S(2)}, u32[]{:S(2)}) async-start(bf16[16,1,48]{2,1,0:T(2,128)(2,1)} %convert_element_type.96), calls=%async_computation.5 | async-start | bytes 16384 | tf_op jit(solution)/shard_map/all_to_all | solution.py:119
  183.9 14.0 %all-to-all-start.3 = ((bf16[16,48,128]{2,1,0:T(8,128)(2,1)}), bf16[16,48,128]{2,1,0:T(8,128)(2,1)S(1)}, u32[]{:S(2)}, u32[]{:S(2)}) async-start(bf16[16,48,128]{2,1,0:T(8,128)(2,1)} %bitcast.8), calls=%async_computation.3 | async-start | bytes 393216 | tf_op jit(solution)/shard_map/all_to_all | solution.py:112
Sparse Core Ops, SparseCore 0:
  44.2 59.0 all-gather.1
  124.5 57.6 reduce-scatter.3
where the time goes:
time: 210 us; the launch traced here: 207 us
  waiting for transfers between devices  79.1 us (38%)
  blocking collectives  34.2 us (16%)
  local copies, waits for them, and re-layouts  31 us (15%)
  matrix products  26.3 us (13%)
  starting transfers between devices  18 us (9%)
  between operations  14.3 us (7%)
  other arithmetic  3.85 us (2%)
    all_gather x1, waiting for transfers between devices, side_by_side(): out = lax.all_gather(both, axis, axis=dim, tiled=True)  44.2 us
    unnamed x3, waiting for transfers between devices  32.5 us
    all_to_all x1, blocking collectives, local(): lax.all_to_all(gather_slots(token_cols), 'ep', split_axis=0, concat_axis=...  14.6 us
    all_to_all x1, blocking collectives, local(): lax.all_to_all(gather_slots(cot_cols), 'ep', split_axis=0, concat_axis=0,...  10.2 us
    all_to_all x1, blocking collectives, local(): lax.all_to_all(slot_gates, 'ep', split_axis=0, concat_axis=0, tiled=True)  9.43 us
    unnamed x19, local copies, waits for them, and re-layouts  9.32 us
    all_to_all x1, starting transfers between devices, local(): lax.all_to_all(gate_total.reshape(expert_count, capacity).astype(jnp.bflo...  6.52 us
    all_to_all x1, starting transfers between devices, local(): lax.all_to_all(grad_cols.reshape(expert_count, capacity, grad_cols.shape[...  6.22 us
  transfers between devices with their start and end apart: 5, of which 3 were waited for; matrix products, arithmetic and copies ran while one was open for 13% of the time, Pallas kernels for 0%

commit v1 on v0

v1 whole, which is shorter than its diff:
```python
import functools

import jax
import jax.numpy as jnp
from jax import lax
from jax.experimental import pallas as pl
from jax.experimental.pallas import tpu as pltpu
from jax.sharding import PartitionSpec as P

EP = ("y", "x")
LANES = 128
BF16 = jnp.bfloat16
F32 = jnp.float32
NN = (((1,), (0,)), ((), ()))
NT = (((1,), (1,)), ((), ()))
TN = (((0,), (0,)), ((), ()))
VMEM = pl.BlockSpec(memory_space=pltpu.VMEM)
SMEM = pl.BlockSpec(memory_space=pltpu.SMEM)


def dot(a, b, dims):
    return lax.dot_general(a, b, dims, preferred_element_type=F32)


def call(kernel, out_shape, *args, in_specs=None, flops=0):
    moved = sum(a.size * a.dtype.itemsize for a in (*args, *jax.tree.leaves(out_shape)))
    return pl.pallas_call(
        kernel,
        out_shape=out_shape,
        in_specs=in_specs or [VMEM] * len(args),
        out_specs=jax.tree.map(lambda _: VMEM, out_shape),
        cost_estimate=pl.CostEstimate(flops=flops, bytes_accessed=moved, transcendentals=0),
        compiler_params=pltpu.CompilerParams(vmem_limit_bytes=56 * 1024 * 1024),
    )(*args)


def slots_of(core, routes, experts, half):
    top_k, rows = routes.shape
    expert = lax.broadcasted_iota(jnp.int32, (experts, rows), 0)
    hits = [routes[k : k + 1, :] == expert for k in range(top_k)]
    named = functools.reduce(jnp.logical_or, hits)
    before = lax.broadcasted_iota(jnp.int32, (rows, rows), 0) < lax.broadcasted_iota(
        jnp.int32, (rows, rows), 1
    )
    ones = lambda mask: jnp.where(mask, 1.0, 0.0).astype(BF16)
    count = dot(ones(named), ones(before), NN)
    slots = []
    for k in range(top_k):
        place = jnp.sum(jnp.where(hits[k], count, 0.0), axis=0, keepdims=True).astype(jnp.int32)
        place = place - core * half
        inside = (place >= 0) & (place < half)
        slots.append(jnp.where(inside, routes[k : k + 1, :] * half + place, -1))
    return slots


def masks_of(slots, count):
    row = lax.broadcasted_iota(jnp.int32, (count, slots[0].shape[1]), 0)
    return [row == s for s in slots]


def prepare(experts, half, core_ref, routes_ref, gates_ref, tok_ref, cot_ref, out_ref):
    width = tok_ref.shape[1]
    slots = slots_of(core_ref[0], routes_ref[...], experts, half)
    masks = masks_of(slots, experts * half)
    gates = gates_ref[...].astype(F32)
    pick = jnp.zeros(masks[0].shape, F32)
    weigh = jnp.zeros(masks[0].shape, F32)
    for k, mask in enumerate(masks):
        pick = jnp.where(mask, 1.0, pick)
        weigh = jnp.where(mask, gates[k : k + 1, :], weigh)
    out_ref[:, :width] = dot(pick.astype(BF16), tok_ref[...], NN).astype(BF16)
    out_ref[:, width:] = dot(weigh.astype(BF16), cot_ref[...], NN).astype(BF16)


def expert(x_ref, *refs):
    weights, outs = refs[:6], refs[6:]
    back_ref, hid_ref, pre_ref, up_ref = outs
    width = weights[0].shape[1]
    tok = x_ref[:, :width]
    cot = x_ref[:, width:]
    gate = jnp.zeros((x_ref.shape[0], 1), F32)
    for part in range(2):
        wg, wu, wd = weights[3 * part : 3 * part + 3]
        pre = dot(tok, wg[...], NT)
        up = dot(tok, wu[...], NT)
        back = dot(cot, wd[...], NT)
        sig = jax.nn.sigmoid(pre)
        act = pre * sig
        hidden = (act * up).astype(BF16)
        gate = gate + jnp.sum(hidden.astype(F32) * back, axis=1, keepdims=True)
        hid_ref[part] = hidden
        pre_ref[part] = (back * up * sig * (1.0 + pre * (1.0 - sig))).astype(BF16)
        up_ref[part] = (back * act).astype(BF16)
    total = dot(pre_ref[0], weights[0][...], NN)
    total += dot(up_ref[0], weights[1][...], NN)
    total += dot(pre_ref[1], weights[3][...], NN)
    total += dot(up_ref[1], weights[4][...], NN)
    back_ref[:, :width] = total.astype(BF16)
    back_ref[:, width:] = jnp.broadcast_to(gate, (gate.shape[0], LANES)).astype(BF16)


def weight_grads(part, width, x_ref, hid_ref, pre_ref, up_ref, *refs):
    lefts = (pre_ref, up_ref, hid_ref)
    if len(refs) > 3:
        received, outs = refs[:3], refs[3:]
    else:
        received, outs = (None,) * 3, refs
    for n in range(3):
        right = x_ref[:, width:] if n == 2 else x_ref[:, :width]
        grad = dot(lefts[n][part], right, TN)
        if received[n] is not None:
            grad += received[n][...].astype(F32)
        outs[n][...] = grad.astype(BF16)


def combine(experts, half, tp, core_ref, routes_ref, x_ref, out_ref):
    rows = routes_ref.shape[1]
    width = tp * LANES
    slots = slots_of(core_ref[0], routes_ref[...], experts, half)
    masks = masks_of(slots, experts * half)
    pick = functools.reduce(lambda a, m: jnp.where(m, 1.0, a), masks, jnp.zeros(masks[0].shape, F32))
    grads = dot(pick.astype(BF16), x_ref[:, :width], TN).astype(BF16)
    gate = x_ref[:, width : width + 1].astype(F32)
    lines = []
    for mask in masks:
        line = jnp.sum(jnp.where(mask, gate, 0.0), axis=0, keepdims=True)
        line = jnp.concatenate([line, jnp.zeros((1, 2 * LANES - rows), F32)], axis=1)
        lines += [line[:, :LANES], line[:, LANES:]]
    lines.append(jnp.zeros((16 - len(lines), LANES), F32))
    tail = jnp.concatenate(lines, axis=0).astype(BF16)
    for t in range(tp):
        out_ref[t, :rows, :] = grads[:, t * LANES : (t + 1) * LANES]
        out_ref[t, rows:, :] = tail


def finish(gates_ref, x_ref, tok_ref, gate_ref):
    top_k, rows = gates_ref.shape
    total = jnp.sum(x_ref[...].astype(F32), axis=0)
    tok_ref[...] = total[:rows].astype(BF16)
    gates = gates_ref[...].astype(F32)
    for k in range(top_k):
        line = jnp.concatenate(
            [total[rows + 2 * k : rows + 2 * k + 1], total[rows + 2 * k + 1 : rows + 2 * k + 2]],
            axis=1,
        )
        gate_ref[k : k + 1, :] = line[:, :rows] / gates[k : k + 1, :]


def local(experts, tp, tokens, cotangent, routing, gate_weights, gate_proj, up_proj, down_proj):
    rows, width = tokens.shape
    top_k = routing.shape[1]
    half = rows * top_k // experts
    count = experts * half
    core = lax.axis_index("c").astype(jnp.int32).reshape(1)
    routes, gates = routing.T, gate_weights.T
    swap = lambda v: lax.ppermute(v, "c", [(0, 1), (1, 0)])

    own = (gate_proj[0].T, up_proj[0].T, down_proj[0])
    other = tuple(swap(w) for w in own)
    ff = own[0].shape[0]

    sent = call(
        functools.partial(prepare, experts, half),
        jax.ShapeDtypeStruct((count, 2 * width), BF16),
        core, routes, gates, tokens, cotangent,
        in_specs=[SMEM, VMEM, VMEM, VMEM, VMEM],
        flops=4 * count * rows * width,
    )
    got = lax.all_to_all(
        sent.reshape(experts, half, 2 * width), EP, split_axis=0, concat_axis=0, tiled=True
    ).reshape(count, 2 * width)

    mid = jax.ShapeDtypeStruct((2, count, ff), BF16)
    back, hid, pre, up = call(
        expert,
        (jax.ShapeDtypeStruct((count, width + LANES), BF16), mid, mid, mid),
        got, *own, *other,
        flops=20 * count * width * ff,
    )
    returned = lax.all_to_all(
        back.reshape(experts, half, width + LANES), EP, split_axis=0, concat_axis=0, tiled=True
    ).reshape(count, width + LANES)

    shard = (jax.ShapeDtypeStruct((ff, width), BF16),) * 3
    theirs = call(
        functools.partial(weight_grads, 1, width), shard, got, hid, pre, up,
        flops=6 * count * width * ff,
    )
    received = tuple(swap(g) for g in theirs)
    grad_gate, grad_up, grad_down = call(
        functools.partial(weight_grads, 0, width), shard, got, hid, pre, up, *received,
        flops=6 * count * width * ff,
    )

    pieces = call(
        functools.partial(combine, experts, half, tp),
        jax.ShapeDtypeStruct((tp, rows + 16, LANES), BF16),
        core, routes, returned,
        in_specs=[SMEM, VMEM, VMEM],
        flops=2 * count * rows * width,
    )
    summed = lax.all_to_all(pieces, ("z", "c"), split_axis=0, concat_axis=0, tiled=True)
    grad_tokens, grad_gates = call(
        finish,
        (jax.ShapeDtypeStruct((rows, LANES), BF16), jax.ShapeDtypeStruct((top_k, rows), F32)),
        gates, summed,
    )
    return (grad_tokens, grad_gates.T, grad_gate.T[None], grad_up.T[None], grad_down[None])


def solution(mesh):
    devices = mesh.devices.reshape(4, 4, 8, 2)
    inner = jax.sharding.Mesh(devices, ("y", "x", "z", "c"))
    ep, tp = EP, ("z", "c")
    return jax.shard_map(
        functools.partial(local, 16, 16),
        mesh=inner,
        in_specs=(
            P(ep, None),
            P(ep, None),
            P(ep, None),
            P(ep, None),
            P(ep, None, tp),
            P(ep, None, tp),
            P(ep, tp, None),
        ),
        out_specs=(
            P(ep, tp),
            P(ep, None),
            P(ep, None, tp),
            P(ep, None, tp),
            P(ep, tp, None),
        ),
        check_vma=False,
    )
```

time: 210 us -> 146 us (0.70); the launches traced: 207 us -> 146 us
  Pallas kernels: 0 us -> 40 us
  blocking collectives: 34.2 us -> 0 us
  matrix products: 26.3 us -> 0 us
  local copies, waits for them, and re-layouts: 31 us -> 6.33 us
  between operations: 14.3 us -> 0.69 us
  starting transfers between devices: 18 us -> 28.5 us
  waiting for transfers between devices: 79.1 us -> 70.5 us
  other arithmetic: 3.85 us -> 0 us
    all_to_all x3, waiting for transfers between devices: 2.46 us -> 63.2 us  [the longest x1 36.8 us: local(): lax.all_to_all(sent.reshape(experts, half, 2 * width), EP, split_axis=0,...]
    all_gather x1 -> x0, waiting for transfers between devices: 44.2 us -> none  [side_by_side(): out = lax.all_gather(both, axis, axis=dim, tiled=True)]
    pallas_call x0 -> x6, Pallas kernels: none -> 40 us  [call(): pl.pallas_call(kernel, out_shape=out_shape, in_specs=in_specs or [VMEM] *...]
    all_to_all x3 -> x0, blocking collectives: 34.2 us -> none  [the longest x1 14.6 us: local(): lax.all_to_all(gather_slots(token_cols), 'ep', split_axis=0, concat_axis=...]
    unnamed x3 -> x0, waiting for transfers between devices: 32.5 us -> none
    dot_general x8 -> x0, matrix products: 26.3 us -> none  [the longest x1 5.03 us: expert_backward(): lax.dot_general(hidden, scaled_cot, contract_rows, preferred_element_type...]
    gather x5 -> x0, local copies, waits for them, and re-layouts: 11.8 us -> none  [the longest x1 5 us: local(): gate_weights.reshape(-1)[safe_owner]]
    ppermute x0 -> x6, waiting for transfers between devices: none -> 7.26 us  [local(): swap = lambda v: lax.ppermute(v, 'c', [(0, 1), (1, 0)])]
  transfers between devices with their start and end apart: 5 -> 9, of which waited for: 3 -> 6; matrix products, arithmetic and copies ran while one was open for 13% -> 0% of each run, Pallas kernels for 0% -> 13%
where the time goes in v1:
time: 146 us
  waiting for transfers between devices  70.5 us (48%)
  Pallas kernels  40 us (27%)
  starting transfers between devices  28.5 us (20%)
  local copies, waits for them, and re-layouts  6.33 us (4%)
    pallas_call x6, Pallas kernels, call(): pl.pallas_call(kernel, out_shape=out_shape, in_specs=in_specs or [VMEM] *...  40 us
    all_to_all x1, waiting for transfers between devices, local(): lax.all_to_all(sent.reshape(experts, half, 2 * width), EP, split_axis=0,...  36.8 us
    all_to_all x1, waiting for transfers between devices, local(): lax.all_to_all(pieces, ('z', 'c'), split_axis=0, concat_axis=0, tiled=True)  14.2 us
    all_to_all x1, starting transfers between devices, local(): lax.all_to_all(pieces, ('z', 'c'), split_axis=0, concat_axis=0, tiled=True)  12.7 us
    all_to_all x1, waiting for transfers between devices, local(): lax.all_to_all(back.reshape(experts, half, width + LANES), EP, split_axis...  12.2 us
    all_to_all x1, starting transfers between devices, local(): lax.all_to_all(sent.reshape(experts, half, 2 * width), EP, split_axis=0,...  7.57 us
    ppermute x6, waiting for transfers between devices, local(): swap = lambda v: lax.ppermute(v, 'c', [(0, 1), (1, 0)])  7.26 us
    unnamed x12, local copies, waits for them, and re-layouts  6.33 us
  transfers between devices with their start and end apart: 9, of which 6 were waited for; matrix products, arithmetic and copies ran while one was open for 0% of the time, Pallas kernels for 13%

profile of v1, /device:TPU:1, one launch (start us, length us, event | category | flops | bytes accessed | tf_op | source)
XLA Modules:
  0.0 145.9 jit_solution(17978956923454325519)
XLA Ops:
  0.6 4.3 %shard_map.110 = bf16[384,4096]{1,0:T(8,128)(2,1)} custom-call(s32[1]{0:T(128)} %bitcast.1.core_ref, s32[2,192]{1,0:T(2,128)} %bitcast.28, bf16[2,192]{1,0:T(2,128)(2,1)} %bitcast.30, bf16[192,2048]{1,0:T(8,128)(2,1)} %tok_ref.1, bf16[192,2048]{1,0:T(8,128)(2,1)} %cot_ref.1), custom_call_target="tpu_custom_call" | custom-call | flops 603979776 | bytes 4720900 | tf_op jit(solution)/shard_map/pallas_call | solution.py:27
  4.9 7.6 %all-to-all-start = ((bf16[16,24,4096]{2,1,0:T(8,128)(2,1)}), bf16[16,24,4096]{2,1,0:T(8,128)(2,1)S(1)}, u32[]{:S(2)}, u32[]{:S(2)}) async-start(bf16[16,24,4096]{2,1,0:T(8,128)(2,1)} %bitcast.22), calls=%async_computation | async-start | bytes 6291456 | tf_op jit(solution)/shard_map/all_to_all | solution.py:169
  12.5 1.0 collective-permute-start
  13.5 0.1 collective-permute-start.1
  13.6 0.4 collective-permute-start.2
  14.1 3.1 %collective-permute-done.refs_3_ = bf16[448,2048]{1,0:T(8,128)(2,1)S(1)} collective-permute-done((bf16[448,2048]{1,0:T(8,128)(2,1)}, bf16[448,2048]{1,0:T(8,128)(2,1)S(1)}, u32[]{:S(2)}, u32[]{:S(2)}) %collective-permute-start) | collective-permute-done | bytes 1835040 | tf_op jit(solution)/shard_map/ppermute | solution.py:156
  17.2 0.0 copy-start.4
  17.2 2.6 %collective-permute-done.1.refs_4_ = bf16[448,2048]{1,0:T(8,128)(2,1)S(1)} collective-permute-done((bf16[448,2048]{1,0:T(8,128)(2,1)}, bf16[448,2048]{1,0:T(8,128)(2,1)S(1)}, u32[]{:S(2)}, u32[]{:S(2)}) %collective-permute-start.1) | collective-permute-done | bytes 1835040 | tf_op jit(solution)/shard_map/ppermute | solution.py:156
  19.8 0.0 copy-done.4
  19.8 0.0 copy-start.5
  19.8 1.2 copy-done.5
  21.0 1.5 %collective-permute-done.2.refs_5_ = bf16[448,2048]{1,0:T(8,128)(2,1)} collective-permute-done((bf16[448,2048]{1,0:T(8,128)(2,1)}, bf16[448,2048]{1,0:T(8,128)(2,1)}, u32[]{:S(2)}, u32[]{:S(2)}) %collective-permute-start.2) | collective-permute-done | bytes 1835040 | tf_op jit(solution)/shard_map/ppermute | solution.py:156
  22.6 36.8 %all-to-all-done = bf16[16,24,4096]{2,1,0:T(8,128)(2,1)S(1)} async-done(((bf16[16,24,4096]{2,1,0:T(8,128)(2,1)}), bf16[16,24,4096]{2,1,0:T(8,128)(2,1)S(1)}, u32[]{:S(2)}, u32[]{:S(2)}) %all-to-all-start) | async-done | bytes 3145760 | tf_op jit(solution)/shard_map/all_to_all | solution.py:169
  59.3 0.0 copy-start
  59.3 1.6 %copy-done = bf16[16,24,4096]{2,1,0:T(8,128)(2,1)} copy-done((bf16[16,24,4096]{2,1,0:T(8,128)(2,1)}, bf16[16,24,4096]{2,1,0:T(8,128)(2,1)S(1)}, u32[]{:S(2)}) %copy-start) | copy-done | bytes 3145752
  61.0 15.1 %shard_map.111 = (bf16[384,2176]{1,0:T(8,128)(2,1)}, bf16[2,384,448]{2,1,0:T(8,128)(2,1)}, bf16[2,384,448]{2,1,0:T(8,128)(2,1)}, bf16[2,384,448]{2,1,0:T(8,128)(2,1)}) custom-call(bf16[384,4096]{1,0:T(8,128)(2,1)} %bitcast.23, bf16[448,2048]{1,0:T(8,128)(2,1)} %bitcast.33, bf16[448,2048]{1,0:T(8,128)(2,1)} %bitcast.35, bf16[448,2048]{1,0:T(8,128)(2,1)} %bitcast.37, ...), custom_call_target="tpu_custom_call" | custom-call | flops 7046430720 | bytes 17891328 | tf_op jit(solution)/shard_map/pallas_call | solution.py:27
  76.1 4.1 %all-to-all-start.1 = ((bf16[16,24,2176]{2,1,0:T(8,128)(2,1)}), bf16[16,24,2176]{2,1,0:T(8,128)(2,1)S(1)}, u32[]{:S(2)}, u32[]{:S(2)}) async-start(bf16[16,24,2176]{2,1,0:T(8,128)(2,1)} %bitcast.27), calls=%async_computation.1 | async-start | bytes 3342336 | tf_op jit(solution)/shard_map/all_to_all | solution.py:180
  80.2 6.8 %shard_map.114 = (bf16[448,2048]{1,0:T(8,128)(2,1)}, bf16[448,2048]{1,0:T(8,128)(2,1)}, bf16[448,2048]{1,0:T(8,128)(2,1)}) custom-call(bf16[384,4096]{1,0:T(8,128)(2,1)} %bitcast.24, bf16[2,384,448]{2,1,0:T(8,128)(2,1)} %get-tuple-element.20.hid_ref, bf16[2,384,448]{2,1,0:T(8,128)(2,1)} %get-tuple-element.21.pre_ref, ...), custom_call_target="tpu_custom_call" | custom-call | flops 2113929216 | bytes 10715136 | tf_op jit(solution)/shard_map/pallas_call | solution.py:27
  87.0 2.1 %collective-permute-start.3 = (bf16[448,2048]{1,0:T(8,128)(2,1)}, bf16[448,2048]{1,0:T(8,128)(2,1)S(1)}, u32[]{:S(2)}, u32[]{:S(2)}) collective-permute-start(bf16[448,2048]{1,0:T(8,128)(2,1)} %get-tuple-element.23), channel_id=1, source_target_pairs={{0,1},{1,0},{2,3},{3,2},{4,5},{5,4},{6,7},{7,6},{8,9},{9,8},{10,11... | collective-permute-start | bytes 5505032 | tf_op jit(solution)/shard_map/ppermute | solution.py:156
  89.1 0.0 collective-permute-start.4
  89.1 0.5 collective-permute-start.5
  89.6 12.2 %all-to-all-done.1 = bf16[16,24,2176]{2,1,0:T(8,128)(2,1)S(1)} async-done(((bf16[16,24,2176]{2,1,0:T(8,128)(2,1)}), bf16[16,24,2176]{2,1,0:T(8,128)(2,1)S(1)}, u32[]{:S(2)}, u32[]{:S(2)}) %all-to-all-start.1) | async-done | bytes 1671200 | tf_op jit(solution)/shard_map/all_to_all | solution.py:180
  101.8 0.0 copy-start.1
  101.8 1.3 copy-done.1
  103.1 3.3 %shard_map.112 = bf16[16,208,128]{2,1,0:T(8,128)(2,1)} custom-call(s32[1]{0:T(128)} %bitcast.1.core_ref, s32[2,192]{1,0:T(2,128)} %bitcast.29, bf16[384,2176]{1,0:T(8,128)(2,1)} %bitcast.26), custom_call_target="tpu_custom_call" | custom-call | flops 301989888 | bytes 2524676 | tf_op jit(solution)/shard_map/pallas_call | solution.py:27
  106.4 12.7 %all-to-all-start.2 = ((bf16[16,208,128]{2,1,0:T(8,128)(2,1)}), bf16[16,208,128]{2,1,0:T(8,128)(2,1)S(1)}, u32[]{:S(2)}, u32[]{:S(2)}) async-start(bf16[16,208,128]{2,1,0:T(8,128)(2,1)} %shard_map.112), calls=%async_computation.2 | async-start | bytes 1703936 | tf_op jit(solution)/shard_map/all_to_all | solution.py:202
  119.1 0.0 collective-permute-done.3.refs_0_
  119.1 0.0 copy-start.3
  119.1 0.0 collective-permute-done.4.refs_1_
  119.1 0.0 collective-permute-done.5.refs_2_
  119.1 1.3 copy-done.3
  120.4 8.5 %shard_map.115 = (bf16[448,2048]{1,0:T(8,128)(2,1)}, bf16[448,2048]{1,0:T(8,128)(2,1)}, bf16[448,2048]{1,0:T(8,128)(2,1)}) custom-call(bf16[384,4096]{1,0:T(8,128)(2,1)} %bitcast.25, bf16[2,384,448]{2,1,0:T(8,128)(2,1)} %get-tuple-element.20.hid_ref, bf16[2,384,448]{2,1,0:T(8,128)(2,1)} %get-tuple-element.21.pre_ref, ...), custom_call_target="tpu_custom_call" | custom-call | flops 2113929216 | bytes 16220160 | tf_op jit(solution)/shard_map/pallas_call | solution.py:27
  128.9 14.2 %all-to-all-done.2.x_ref = bf16[16,208,128]{2,1,0:T(8,128)(2,1)S(1)} async-done(((bf16[16,208,128]{2,1,0:T(8,128)(2,1)}), bf16[16,208,128]{2,1,0:T(8,128)(2,1)S(1)}, u32[]{:S(2)}, u32[]{:S(2)}) %all-to-all-start.2) | async-done | bytes 852000 | tf_op jit(solution)/shard_map/all_to_all | solution.py:202
  143.1 0.0 copy-start.2
  143.1 0.9 copy-done.2
  144.0 1.9 %shard_map.113 = (bf16[192,128]{1,0:T(8,128)(2,1)}, f32[2,192]{1,0:T(2,128)}) custom-call(bf16[2,192]{1,0:T(2,128)(2,1)} %bitcast.31, bf16[16,208,128]{2,1,0:T(8,128)(2,1)} %copy-done.2), custom_call_target="tpu_custom_call" | custom-call | bytes 903424 | tf_op jit(solution)/shard_map/pallas_call | solution.py:27
Async XLA Ops:
  4.9 54.4 %all-to-all-start = ((bf16[16,24,4096]{2,1,0:T(8,128)(2,1)}), bf16[16,24,4096]{2,1,0:T(8,128)(2,1)S(1)}, u32[]{:S(2)}, u32[]{:S(2)}) async-start(bf16[16,24,4096]{2,1,0:T(8,128)(2,1)} %bitcast.22), calls=%async_computation | async-start | bytes 6291456 | tf_op jit(solution)/shard_map/all_to_all | solution.py:169
  12.5 4.7 %collective-permute-start = (bf16[448,2048]{1,0:T(8,128)(2,1)}, bf16[448,2048]{1,0:T(8,128)(2,1)S(1)}, u32[]{:S(2)}, u32[]{:S(2)}) collective-permute-start(bf16[448,2048]{1,0:T(8,128)(2,1)} %bitcast.32), channel_id=1, source_target_pairs={{0,1},{1,0},{2,3},{3,2},{4,5},{5,4},{6,7},{7,6},{8,9},{9,8},{10,11... | collective-permute-start | bytes 5505032 | tf_op jit(solution)/shard_map/ppermute | solution.py:156
  13.5 6.2 %collective-permute-start.1 = (bf16[448,2048]{1,0:T(8,128)(2,1)}, bf16[448,2048]{1,0:T(8,128)(2,1)S(1)}, u32[]{:S(2)}, u32[]{:S(2)}) collective-permute-start(bf16[448,2048]{1,0:T(8,128)(2,1)} %bitcast.34), channel_id=1, source_target_pairs={{0,1},{1,0},{2,3},{3,2},{4,5},{5,4},{6,7},{7,6},{8,9},{9,8},{10,11... | collective-permute-start | bytes 5505032 | tf_op jit(solution)/shard_map/ppermute | solution.py:156
  13.6 8.9 %collective-permute-start.2 = (bf16[448,2048]{1,0:T(8,128)(2,1)}, bf16[448,2048]{1,0:T(8,128)(2,1)}, u32[]{:S(2)}, u32[]{:S(2)}) collective-permute-start(bf16[448,2048]{1,0:T(8,128)(2,1)} %bitcast.36), channel_id=1, source_target_pairs={{0,1},{1,0},{2,3},{3,2},{4,5},{5,4},{6,7},{7,6},{8,9},{9,8},{10,11... | collective-permute-start | bytes 5505032 | tf_op jit(solution)/shard_map/ppermute | solution.py:156
  17.2 2.6 %copy-start.4 = (bf16[448,2048]{1,0:T(8,128)(2,1)}, bf16[448,2048]{1,0:T(8,128)(2,1)S(1)}, u32[]{:S(2)}) copy-start(bf16[448,2048]{1,0:T(8,128)(2,1)S(1)} %collective-permute-done.refs_3_) | copy-start | bytes 5505028
  19.8 1.2 copy-start.5
  59.3 1.6 %copy-start = (bf16[16,24,4096]{2,1,0:T(8,128)(2,1)}, bf16[16,24,4096]{2,1,0:T(8,128)(2,1)S(1)}, u32[]{:S(2)}) copy-start(bf16[16,24,4096]{2,1,0:T(8,128)(2,1)S(1)} %all-to-all-done) | copy-start | bytes 9437188
  76.1 25.7 %all-to-all-start.1 = ((bf16[16,24,2176]{2,1,0:T(8,128)(2,1)}), bf16[16,24,2176]{2,1,0:T(8,128)(2,1)S(1)}, u32[]{:S(2)}, u32[]{:S(2)}) async-start(bf16[16,24,2176]{2,1,0:T(8,128)(2,1)} %bitcast.27), calls=%async_computation.1 | async-start | bytes 3342336 | tf_op jit(solution)/shard_map/all_to_all | solution.py:180
  87.0 32.0 %collective-permute-start.3 = (bf16[448,2048]{1,0:T(8,128)(2,1)}, bf16[448,2048]{1,0:T(8,128)(2,1)S(1)}, u32[]{:S(2)}, u32[]{:S(2)}) collective-permute-start(bf16[448,2048]{1,0:T(8,128)(2,1)} %get-tuple-element.23), channel_id=1, source_target_pairs={{0,1},{1,0},{2,3},{3,2},{4,5},{5,4},{6,7},{7,6},{8,9},{9,8},{10,11... | collective-permute-start | bytes 5505032 | tf_op jit(solution)/shard_map/ppermute | solution.py:156
  89.1 30.0 %collective-permute-start.4 = (bf16[448,2048]{1,0:T(8,128)(2,1)}, bf16[448,2048]{1,0:T(8,128)(2,1)}, u32[]{:S(2)}, u32[]{:S(2)}) collective-permute-start(bf16[448,2048]{1,0:T(8,128)(2,1)} %get-tuple-element.24), channel_id=1, source_target_pairs={{0,1},{1,0},{2,3},{3,2},{4,5},{5,4},{6,7},{7,6},{8,9},{9,8},{10,11... | collective-permute-start | bytes 5505032 | tf_op jit(solution)/shard_map/ppermute | solution.py:156
  89.1 30.0 %collective-permute-start.5 = (bf16[448,2048]{1,0:T(8,128)(2,1)}, bf16[448,2048]{1,0:T(8,128)(2,1)}, u32[]{:S(2)}, u32[]{:S(2)}) collective-permute-start(bf16[448,2048]{1,0:T(8,128)(2,1)} %get-tuple-element.25), channel_id=1, source_target_pairs={{0,1},{1,0},{2,3},{3,2},{4,5},{5,4},{6,7},{7,6},{8,9},{9,8},{10,11... | collective-permute-start | bytes 5505032 | tf_op jit(solution)/shard_map/ppermute | solution.py:156
  101.8 1.3 copy-start.1
  106.4 36.7 %all-to-all-start.2 = ((bf16[16,208,128]{2,1,0:T(8,128)(2,1)}), bf16[16,208,128]{2,1,0:T(8,128)(2,1)S(1)}, u32[]{:S(2)}, u32[]{:S(2)}) async-start(bf16[16,208,128]{2,1,0:T(8,128)(2,1)} %shard_map.112), calls=%async_computation.2 | async-start | bytes 1703936 | tf_op jit(solution)/shard_map/all_to_all | solution.py:202
  119.1 1.3 copy-start.3
  143.1 0.9 copy-start.2

commit v2 on v1

v2 whole, which is shorter than its diff:
```python
import functools

import jax
import jax.numpy as jnp
from jax import lax
from jax.experimental import pallas as pl
from jax.experimental.pallas import tpu as pltpu
from jax.sharding import PartitionSpec as P

EP = ("y", "x")
LANES = 128
BF16 = jnp.bfloat16
F32 = jnp.float32
NN = (((1,), (0,)), ((), ()))
NT = (((1,), (1,)), ((), ()))
TN = (((0,), (0,)), ((), ()))
IN_VMEM = pl.BlockSpec(memory_space=pltpu.VMEM)
IN_HBM = pl.BlockSpec(memory_space=pltpu.HBM)
IN_SMEM = pl.BlockSpec(memory_space=pltpu.SMEM)


def dot(a, b, dims):
    return lax.dot_general(a, b, dims, preferred_element_type=F32)


def call(kernel, outs, *args, scratch=(), flops=0, mib=24):
    place = {"v": pltpu.VMEM, "h": pltpu.HBM, "w": pltpu.HBM}
    spec = {"v": IN_VMEM, "w": IN_VMEM, "h": IN_HBM, "s": IN_SMEM}
    moved = sum(a.size * a.dtype.itemsize for a, _ in args)
    return pl.pallas_call(
        kernel,
        out_shape=[place[m](shape, dtype) for shape, dtype, m in outs],
        in_specs=[spec[m] for _, m in args],
        out_specs=[spec[m] for _, _, m in outs],
        scratch_shapes=list(scratch),
        cost_estimate=pl.CostEstimate(flops=flops, bytes_accessed=moved, transcendentals=0),
        compiler_params=pltpu.CompilerParams(vmem_limit_bytes=mib * 1024 * 1024),
    )(*(a if m == "s" else pltpu.with_memory_space_constraint(a, place[m]) for a, m in args))


def slots_of(core, routes, experts, half):
    top_k, rows = routes.shape
    expert = lax.broadcasted_iota(jnp.int32, (experts, rows), 0)
    hits = [routes[k : k + 1, :] == expert for k in range(top_k)]
    named = functools.reduce(jnp.logical_or, hits)
    before = lax.broadcasted_iota(jnp.int32, (rows, rows), 0) < lax.broadcasted_iota(
        jnp.int32, (rows, rows), 1
    )
    ones = lambda mask: jnp.where(mask, 1.0, 0.0).astype(BF16)
    count = dot(ones(named), ones(before), NN)
    slots = []
    for k in range(top_k):
        place = jnp.sum(jnp.where(hits[k], count, 0.0), axis=0, keepdims=True).astype(jnp.int32)
        place = place - core * half
        inside = (place >= 0) & (place < half)
        slots.append(jnp.where(inside, routes[k : k + 1, :] * half + place, -1))
    return slots


def masks_of(slots, count):
    row = lax.broadcasted_iota(jnp.int32, (count, slots[0].shape[1]), 0)
    return [row == s for s in slots]


def send_tokens(experts, half, core_ref, par_ref, routes_ref, tok_ref, out_ref, tok, sem):
    part = out_ref.shape[1]
    copy = pltpu.make_async_copy(
        tok_ref.at[:, pl.ds(pl.multiple_of(par_ref[0] * part, part), part)], tok, sem
    )
    copy.start()
    masks = masks_of(slots_of(core_ref[0], routes_ref[...], experts, half), experts * half)
    pick = functools.reduce(lambda a, m: jnp.where(m, 1.0, a), masks, jnp.zeros(masks[0].shape, F32))
    copy.wait()
    out_ref[...] = dot(pick.astype(BF16), tok[...], NN).astype(BF16)


def send_cotangents(experts, half, core_ref, routes_ref, gates_ref, cot_ref, out_ref):
    masks = masks_of(slots_of(core_ref[0], routes_ref[...], experts, half), experts * half)
    gates = gates_ref[...].astype(F32)
    weigh = jnp.zeros(masks[0].shape, F32)
    for k, mask in enumerate(masks):
        weigh = jnp.where(mask, gates[k : k + 1, :], weigh)
    out_ref[...] = dot(weigh.astype(BF16), cot_ref[...], NN).astype(BF16)


def fetch(refs, buf, sem):
    copies = [pltpu.make_async_copy(r, buf.at[n], sem.at[n]) for n, r in enumerate(refs)]
    for copy in copies:
        copy.start()
    return copies


def forward(par_ref, mine_ref, low_ref, high_ref, *refs):
    weights, (hid_ref, slope_ref, act_ref, buf, sem) = refs[:4], refs[4:]
    copies = fetch(weights, buf, sem)
    rows, part = low_ref.shape
    here = pl.ds(pl.multiple_of(par_ref[0] * part, part), part)
    there = pl.ds(pl.multiple_of((1 - par_ref[0]) * part, part), part)

    def product(n):
        copies[n].wait()
        own = dot(mine_ref[...], buf[n, :, here], NT)
        other = buf[n, :, there]
        return own + jnp.concatenate(
            [dot(low_ref[...], other, NT), dot(high_ref[...], other, NT)], axis=0
        )

    for p in range(2):
        pre = product(2 * p)
        up = product(2 * p + 1)
        sig = jax.nn.sigmoid(pre)
        act = pre * sig
        hid_ref[p] = (act * up).astype(BF16)
        slope_ref[p] = up * sig * (1.0 + pre * (1.0 - sig))
        act_ref[p] = act


def backward(cot_ref, hid_ref, slope_ref, act_ref, *refs):
    weights, (back_ref, pre_ref, up_ref, *scratch) = refs[:6], refs[6:]
    buf, sem, hid, slope, act, mid_sem, pre, up, stage, out_sem = scratch
    copies = fetch(weights[:2], buf.at[:2], sem)
    mids = [
        pltpu.make_async_copy(ref, to, mid_sem.at[n])
        for n, (ref, to) in enumerate(((hid_ref, hid), (slope_ref, slope), (act_ref, act)))
    ]
    for mid in mids:
        mid.start()
    copies += fetch(weights[2:], buf.at[2:], sem.at[2:])
    rows, width = cot_ref.shape
    gate = jnp.zeros((rows, 1), F32)
    outs = []
    for p in range(2):
        copies[p].wait()
        back = dot(cot_ref[...], buf[p], NT)
        if p == 0:
            for mid in mids:
                mid.wait()
        gate = gate + jnp.sum(hid[p].astype(F32) * back, axis=1, keepdims=True)
        pre[p] = (back * slope[p]).astype(BF16)
        up[p] = (back * act[p]).astype(BF16)
        for n, (frm, to) in enumerate(((pre, pre_ref), (up, up_ref))):
            outs.append(pltpu.make_async_copy(frm.at[p], to.at[p], out_sem.at[2 * p + n]))
            outs[-1].start()
    for copy in copies[2:]:
        copy.wait()
    stage[:, width:] = jnp.broadcast_to(gate, (rows, LANES)).astype(BF16)
    step = width // 4
    for n in range(4):
        cols = slice(n * step, (n + 1) * step)
        total = dot(pre[0], buf[2, :, cols], NN)
        total += dot(up[0], buf[3, :, cols], NN)
        total += dot(pre[1], buf[4, :, cols], NN)
        total += dot(up[1], buf[5, :, cols], NN)
        stage[:, cols] = total.astype(BF16)
        span = slice(n * step, (n + 1) * step if n < 3 else width + LANES)
        outs.append(pltpu.make_async_copy(stage.at[:, span], back_ref.at[:, span], out_sem.at[4 + n]))
        outs[-1].start()
    for out in outs:
        out.wait()


def weight_grads(p, par_ref, mine_ref, low_ref, high_ref, cot_ref, hid_ref, pre_ref, up_ref, *refs):
    received, outs = (refs[:3], refs[3:]) if len(refs) > 3 else ((None,) * 3, refs)
    rows, part = low_ref.shape
    here = pl.ds(pl.multiple_of(par_ref[0] * part, part), part)
    there = pl.ds(pl.multiple_of((1 - par_ref[0]) * part, part), part)

    def put(n, cols, grad):
        if received[n] is not None:
            grad += received[n][:, cols].astype(F32)
        outs[n][:, cols] = grad.astype(BF16)

    for n, left in enumerate((pre_ref, up_ref)):
        put(n, here, dot(left[p], mine_ref[...], TN))
        grad = dot(left[p, :rows], low_ref[...], TN) + dot(left[p, rows:], high_ref[...], TN)
        put(n, there, grad)
    put(2, slice(None), dot(hid_ref[p], cot_ref[...], TN))


def combine(experts, half, core_ref, routes_ref, x_ref, keep_ref, send_ref):
    blocks, padded, _ = keep_ref.shape
    rows = routes_ref.shape[1]
    width = 2 * blocks * LANES
    core = core_ref[0]
    masks = masks_of(slots_of(core, routes_ref[...], experts, half), experts * half)
    pick = functools.reduce(lambda a, m: jnp.where(m, 1.0, a), masks, jnp.zeros(masks[0].shape, F32))
    grads = dot(pick.astype(BF16), x_ref[:, :width], TN)
    gate = x_ref[:, width : width + 1].astype(F32)
    lines = []
    for mask in masks:
        line = jnp.sum(jnp.where(mask, gate, 0.0), axis=0, keepdims=True)
        line = jnp.concatenate([line, jnp.zeros((1, 2 * LANES - rows), F32)], axis=1)
        lines += [line[:, :LANES], line[:, LANES:]]
    lines.append(jnp.zeros((padded - rows - len(lines), LANES), F32))
    tail = jnp.concatenate(lines, axis=0)
    for b in range(blocks):
        first = grads[:, 2 * b * LANES : (2 * b + 1) * LANES]
        second = grads[:, (2 * b + 1) * LANES : (2 * b + 2) * LANES]
        keep_ref[b, :rows, :] = jnp.where(core == 0, first, second)
        send_ref[b, :rows, :] = jnp.where(core == 0, second, first).astype(BF16)
        keep_ref[b, rows:, :] = tail
        send_ref[b, rows:, :] = tail.astype(BF16)


def join(keep_ref, got_ref, out_ref):
    out_ref[...] = (keep_ref[...] + got_ref[...].astype(F32)).astype(BF16)


def finish(gates_ref, x_ref, tok_ref, gate_ref):
    top_k, rows = gates_ref.shape
    total = jnp.sum(x_ref[...].astype(F32), axis=0)
    tok_ref[...] = total[:rows].astype(BF16)
    gates = gates_ref[...].astype(F32)
    for k in range(top_k):
        line = jnp.concatenate(
            [total[rows + 2 * k : rows + 2 * k + 1], total[rows + 2 * k + 1 : rows + 2 * k + 2]],
            axis=1,
        )
        gate_ref[k : k + 1, :] = line[:, :rows] / gates[k : k + 1, :]


def local(experts, tokens, cotangent, routing, gate_weights, gate_proj, up_proj, down_proj):
    rows, width = tokens.shape
    top_k = routing.shape[1]
    half = rows * top_k // experts
    count = experts * half
    part = width // 2
    depth = lax.axis_size("z")
    core = lax.axis_index("c").astype(jnp.int32).reshape(1)
    parity = (lax.axis_index("z") % 2).astype(jnp.int32).reshape(1)
    routes, gates = routing.T, gate_weights.T
    swap = lambda v: lax.ppermute(v, "c", [(0, 1), (1, 0)])
    shift = lambda v, k: lax.ppermute(v, "z", [(i, (i + k) % depth) for i in range(depth)])
    exchange = lambda v, axis: lax.all_to_all(v, axis, split_axis=0, concat_axis=0, tiled=True)
    dma = lambda n: pltpu.SemaphoreType.DMA((n,))

    own = (gate_proj[0].T, up_proj[0].T, down_proj[0])
    other = tuple(swap(w) for w in own)
    ff = own[0].shape[0]

    (tok_out,) = call(
        functools.partial(send_tokens, experts, half),
        [((count, part), BF16, "w")],
        (core, "s"), (parity, "s"), (routes, "w"), (tokens, "h"),
        scratch=[pltpu.VMEM((rows, part), BF16), pltpu.SemaphoreType.DMA],
        flops=2 * count * rows * part, mib=8,
    )
    mine = exchange(tok_out.reshape(experts, half, part), EP).reshape(count, part)
    (cot_out,) = call(
        functools.partial(send_cotangents, experts, half),
        [((count, width), BF16, "w")],
        (core, "s"), (routes, "w"), (gates, "w"), (cotangent, "w"),
        flops=2 * count * rows * width, mib=8,
    )
    cot = exchange(cot_out.reshape(experts, half, width), EP).reshape(count, width)
    low = shift(mine[: count // 2], 1)
    high = shift(mine[count // 2 :], -1)

    mid = lambda dtype, mode: ((2, count, ff), dtype, mode)
    hid, slope, act = call(
        forward,
        [mid(BF16, "w"), mid(F32, "w"), mid(F32, "w")],
        (parity, "s"), (mine, "v"), (low, "v"), (high, "v"),
        (own[0], "h"), (own[1], "h"), (other[0], "h"), (other[1], "h"),
        scratch=[pltpu.VMEM((4, ff, width), BF16), dma(4)],
        flops=8 * count * width * ff, mib=20,
    )
    mids = [pltpu.VMEM((2, count, ff), dtype) for dtype in (BF16, F32, F32)]
    back, pre, up = call(
        backward,
        [((count, width + LANES), BF16, "h"), mid(BF16, "h"), mid(BF16, "h")],
        (cot, "v"), (hid, "h"), (slope, "h"), (act, "h"),
        *((w, "h") for w in (own[2], other[2], own[0], own[1], other[0], other[1])),
        scratch=[
            pltpu.VMEM((6, ff, width), BF16), dma(6), *mids, dma(3),
            mids[0], mids[0], pltpu.VMEM((count, width + LANES), BF16), dma(8),
        ],
        flops=12 * count * width * ff, mib=28,
    )
    returned = exchange(back.reshape(experts, half, width + LANES), EP).reshape(count, width + LANES)

    pieces = [(v, "v") for v in (mine, low, high, cot)] + [(v, "w") for v in (hid, pre, up)]
    shard = [((ff, width), BF16, "w")] * 3
    theirs = call(
        functools.partial(weight_grads, 1), shard, (parity, "s"), *pieces,
        flops=6 * count * width * ff, mib=16,
    )
    received = [(swap(g), "w") for g in theirs]
    grad_gate, grad_up, grad_down = call(
        functools.partial(weight_grads, 0), shard, (parity, "s"), *pieces, *received,
        flops=6 * count * width * ff, mib=24,
    )

    block = (depth, rows + 16, LANES)
    keep, send = call(
        functools.partial(combine, experts, half),
        [(block, F32, "v"), (block, BF16, "v")],
        (core, "s"), (routes, "w"), (returned, "v"),
        flops=2 * count * rows * width, mib=12,
    )
    (joined,) = call(join, [(block, BF16, "w")], (keep, "v"), (swap(send), "v"), mib=4)
    summed = exchange(joined, "z")
    grad_tokens, grad_gates = call(
        finish,
        [((rows, LANES), BF16, "w"), ((top_k, rows), F32, "w")],
        (gates, "w"), (summed, "v"), mib=4,
    )
    return (grad_tokens, grad_gates.T, grad_gate.T[None], grad_up.T[None], grad_down[None])


def solution(mesh):
    devices = mesh.devices.reshape(4, 4, 8, 2)
    inner = jax.sharding.Mesh(devices, ("y", "x", "z", "c"))
    ep, tp = EP, ("z", "c")
    return jax.shard_map(
        functools.partial(local, 16),
        mesh=inner,
        in_specs=(
            P(ep, None),
            P(ep, None),
            P(ep, None),
            P(ep, None),
            P(ep, None, tp),
            P(ep, None, tp),
            P(ep, tp, None),
        ),
        out_specs=(
            P(ep, tp),
            P(ep, None),
            P(ep, None, tp),
            P(ep, None, tp),
            P(ep, tp, None),
        ),
        check_vma=False,
    )
```

time: 146 us -> 121 us (0.83)
  waiting for transfers between devices: 70.5 us -> 34.5 us
  starting transfers between devices: 28.5 us -> 40.7 us
  local copies, waits for them, and re-layouts: 6.33 us -> 1.05 us
  Pallas kernels: 40 us -> 43.5 us
    all_to_all x3 -> x4, waiting for transfers between devices: 63.2 us -> 26.1 us  [local(): lax.all_to_all(v, axis, split_axis=0, concat_axis=0, tiled=True)]
    ppermute x0 -> x2, waiting for transfers between devices: none -> 6.99 us  [local(): lax.ppermute(v, 'z', [(i, (i + k) % depth) for i in range(depth)])]
    ppermute x6 -> x7, starting transfers between devices: 4.13 us -> 11 us  [local(): swap = lambda v: lax.ppermute(v, 'c', [(0, 1), (1, 0)])]
    ppermute x0 -> x2, starting transfers between devices: none -> 5.92 us  [local(): lax.ppermute(v, 'z', [(i, (i + k) % depth) for i in range(depth)])]
    ppermute x6 -> x7, waiting for transfers between devices: 7.26 us -> 1.41 us  [local(): swap = lambda v: lax.ppermute(v, 'c', [(0, 1), (1, 0)])]
    unnamed x12 -> x4, local copies, waits for them, and re-layouts: 6.33 us -> 0.99 us
    pallas_call x6 -> x9, Pallas kernels: 40 us -> 43.5 us  [call(): pl.pallas_call(kernel, out_shape=[place[m](shape, dtype) for shape, dtype...]
    all_to_all x3 -> x4, starting transfers between devices: 24.3 us -> 23.7 us  [local(): lax.all_to_all(v, axis, split_axis=0, concat_axis=0, tiled=True)]
  transfers between devices with their start and end apart: 9 -> 13, of which waited for: 6 -> 5; matrix products, arithmetic and copies ran while one was open for 0% -> 0% of each run, Pallas kernels for 13% -> 24%
where the time goes in v2:
time: 121 us; the launch traced here: 120 us
  Pallas kernels  43.5 us (36%)
  starting transfers between devices  40.7 us (34%)
  waiting for transfers between devices  34.5 us (29%)
    pallas_call x9, Pallas kernels, call(): pl.pallas_call(kernel, out_shape=[place[m](shape, dtype) for shape, dtype...  43.5 us
    all_to_all x4, waiting for transfers between devices, local(): lax.all_to_all(v, axis, split_axis=0, concat_axis=0, tiled=True)  26.1 us
    all_to_all x4, starting transfers between devices, local(): lax.all_to_all(v, axis, split_axis=0, concat_axis=0, tiled=True)  23.7 us
    ppermute x7, starting transfers between devices, local(): swap = lambda v: lax.ppermute(v, 'c', [(0, 1), (1, 0)])  11 us
    ppermute x2, waiting for transfers between devices, local(): lax.ppermute(v, 'z', [(i, (i + k) % depth) for i in range(depth)])  6.99 us
    ppermute x2, starting transfers between devices, local(): lax.ppermute(v, 'z', [(i, (i + k) % depth) for i in range(depth)])  5.92 us
  transfers between devices with their start and end apart: 13, of which 5 were waited for; matrix products, arithmetic and copies ran while one was open for 0% of the time, Pallas kernels for 24%

profile of v2, /device:TPU:1, one launch (start us, length us, event | category | flops | bytes accessed | tf_op | source)
XLA Modules:
  0.0 120.5 jit_solution(3603823531934718369)
XLA Ops:
  0.6 3.0 %shard_map.111 = bf16[384,1024]{1,0:T(8,128)(2,1)} custom-call(s32[1]{0:T(128)} %bitcast.1.core_ref, s32[1]{0:T(128)} %bitcast.5.par_ref, s32[2,192]{1,0:T(2,128)} %bitcast.38, bf16[192,2048]{1,0:T(8,128)(2,1)} %tok_ref.1), custom_call_target="tpu_custom_call" | custom-call | flops 150994944 | bytes 787976 | tf_op jit(solution)/shard_map/pallas_call | solution.py:30
  3.6 7.6 %all-to-all-start.1 = ((bf16[16,24,1024]{2,1,0:T(8,128)(2,1)}), bf16[16,24,1024]{2,1,0:T(8,128)(2,1)S(1)}, u32[]{:S(2)}, u32[]{:S(2)}) async-start(bf16[16,24,1024]{2,1,0:T(8,128)(2,1)} %bitcast.34), calls=%async_computation.1 | async-start | bytes 1572864 | tf_op jit(solution)/shard_map/all_to_all | solution.py:234
  11.2 1.0 collective-permute-start.2
  12.2 0.1 collective-permute-start.3
  12.3 0.4 collective-permute-start.4
  12.7 3.0 %shard_map.110 = bf16[384,2048]{1,0:T(8,128)(2,1)} custom-call(s32[1]{0:T(128)} %bitcast.1.core_ref, s32[2,192]{1,0:T(2,128)} %bitcast.39, bf16[2,192]{1,0:T(2,128)(2,1)} %bitcast.41, bf16[192,2048]{1,0:T(8,128)(2,1)} %cot_ref.1), custom_call_target="tpu_custom_call" | custom-call | flops 301989888 | bytes 788740 | tf_op jit(solution)/shard_map/pallas_call | solution.py:30
  15.8 8.6 %all-to-all-done.1 = bf16[16,24,1024]{2,1,0:T(8,128)(2,1)S(1)} async-done(((bf16[16,24,1024]{2,1,0:T(8,128)(2,1)}), bf16[16,24,1024]{2,1,0:T(8,128)(2,1)S(1)}, u32[]{:S(2)}, u32[]{:S(2)}) %all-to-all-start.1) | async-done | bytes 786464 | tf_op jit(solution)/shard_map/all_to_all | solution.py:234
  24.4 3.7 %all-to-all-start = ((bf16[16,24,2048]{2,1,0:T(8,128)(2,1)}), bf16[16,24,2048]{2,1,0:T(8,128)(2,1)S(1)}, u32[]{:S(2)}, u32[]{:S(2)}) async-start(bf16[16,24,2048]{2,1,0:T(8,128)(2,1)} %bitcast.33), calls=%async_computation | async-start | bytes 3145728 | tf_op jit(solution)/shard_map/all_to_all | solution.py:234
  28.1 0.1 fusion
  28.2 1.7 %collective-permute-start = (bf16[192,1024]{1,0:T(8,128)(2,1)S(1)}, bf16[192,1024]{1,0:T(8,128)(2,1)S(1)}, u32[]{:S(2)}, u32[]{:S(2)}) collective-permute-start(bf16[192,1024]{1,0:T(8,128)(2,1)S(1)} %bitcast.37), channel_id=1, source_target_pairs={{0,2},{2,4},{4,6},{6,8},{8,10},{10,12},{12,14},{14,0},{1,3},{3,5},... | collective-permute-start | bytes 1179656 | tf_op jit(solution)/shard_map/ppermute | solution.py:233
  29.9 4.2 %collective-permute-start.1 = (bf16[192,1024]{1,0:T(8,128)(2,1)S(1)}, bf16[192,1024]{1,0:T(8,128)(2,1)S(1)}, u32[]{:S(2)}, u32[]{:S(2)}) collective-permute-start(bf16[192,1024]{1,0:T(8,128)(2,1)S(1)} %bitcast.36), channel_id=1, source_target_pairs={{0,14},{2,0},{4,2},{6,4},{8,6},{10,8},{12,10},{14,12},{1,15},{3,1}... | collective-permute-start | bytes 1179656 | tf_op jit(solution)/shard_map/ppermute | solution.py:233
  34.1 7.0 %collective-permute-done.low_ref = bf16[192,1024]{1,0:T(8,128)(2,1)S(1)} collective-permute-done((bf16[192,1024]{1,0:T(8,128)(2,1)S(1)}, bf16[192,1024]{1,0:T(8,128)(2,1)S(1)}, u32[]{:S(2)}, u32[]{:S(2)}) %collective-permute-start) | collective-permute-done | bytes 393248 | tf_op jit(solution)/shard_map/ppermute | solution.py:233
  41.1 0.0 collective-permute-done.1.high_ref
  41.1 0.0 copy-start
  41.1 0.0 collective-permute-done.2.refs_2_.refs_4_
  41.1 0.0 collective-permute-done.3.refs_3_.refs_5_
  41.1 8.3 %shard_map.112 = (bf16[2,384,448]{2,1,0:T(8,128)(2,1)}, f32[2,384,448]{2,1,0:T(8,128)}, f32[2,384,448]{2,1,0:T(8,128)}) custom-call(s32[1]{0:T(128)} %bitcast.5.par_ref, bf16[384,1024]{1,0:T(8,128)(2,1)S(1)} %bitcast.30, bf16[192,1024]{1,0:T(8,128)(2,1)S(1)} %collective-permute-done.low_ref, bf16[192,1024]{1,0:T(8,128)(2,1)S(1)} %collective-permute-done.1.high_ref, ...), custom_call_target="tpu_custom_call" | custom-call | flops 2818572288 | bytes 8912900 | tf_op jit(solution)/shard_map/pallas_call | solution.py:30
  49.5 0.0 all-to-all-done
  49.5 0.0 collective-permute-done.4.refs_1_
  49.5 10.6 %shard_map.113 = (bf16[384,2176]{1,0:T(8,128)(2,1)}, bf16[2,384,448]{2,1,0:T(8,128)(2,1)}, bf16[2,384,448]{2,1,0:T(8,128)(2,1)}) custom-call(bf16[384,2048]{1,0:T(8,128)(2,1)S(1)} %bitcast.27, bf16[2,384,448]{2,1,0:T(8,128)(2,1)} %get-tuple-element.21.hid_ref, f32[2,384,448]{2,1,0:T(8,128)} %get-tuple-element.22.slope_ref, ...), custom_call_target="tpu_custom_call" | custom-call | flops 4227858432 | bytes 16023552 | tf_op jit(solution)/shard_map/pallas_call | solution.py:30
  60.1 6.5 %all-to-all-start.2 = ((bf16[16,24,2176]{2,1,0:T(8,128)(2,1)}), bf16[16,24,2176]{2,1,0:T(8,128)(2,1)}, u32[]{:S(2)}, u32[]{:S(2)}) async-start(bf16[16,24,2176]{2,1,0:T(8,128)(2,1)} %bitcast.35), calls=%async_computation.2 | async-start | bytes 3342336 | tf_op jit(solution)/shard_map/all_to_all | solution.py:234
  66.5 0.0 copy-done
  66.5 6.2 %shard_map.117 = (bf16[448,2048]{1,0:T(8,128)(2,1)}, bf16[448,2048]{1,0:T(8,128)(2,1)}, bf16[448,2048]{1,0:T(8,128)(2,1)}) custom-call(s32[1]{0:T(128)} %bitcast.5.par_ref, bf16[384,1024]{1,0:T(8,128)(2,1)S(1)} %bitcast.31, bf16[192,1024]{1,0:T(8,128)(2,1)S(1)} %collective-permute-done.low_ref, bf16[192,1024]{1,0:T(8,128)(2,1)S(1)} %collective-permute-done.1.high_ref, ...), custom_call_target="tpu_custom_call" | custom-call | flops 2113929216 | bytes 5210116 | tf_op jit(solution)/shard_map/pallas_call | solution.py:30
  72.7 3.3 %collective-permute-start.6 = (bf16[448,2048]{1,0:T(8,128)(2,1)}, bf16[448,2048]{1,0:T(8,128)(2,1)}, u32[]{:S(2)}, u32[]{:S(2)}) collective-permute-start(bf16[448,2048]{1,0:T(8,128)(2,1)} %get-tuple-element.31), channel_id=1, source_target_pairs={{0,1},{1,0},{2,3},{3,2},{4,5},{5,4},{6,7},{7,6},{8,9},{9,8},{10,11... | collective-permute-start | bytes 5505032 | tf_op jit(solution)/shard_map/ppermute | solution.py:232
  76.1 0.0 collective-permute-start.7
  76.1 0.5 collective-permute-start.8
  76.6 10.5 %all-to-all-done.2 = bf16[16,24,2176]{2,1,0:T(8,128)(2,1)} async-done(((bf16[16,24,2176]{2,1,0:T(8,128)(2,1)}), bf16[16,24,2176]{2,1,0:T(8,128)(2,1)}, u32[]{:S(2)}, u32[]{:S(2)}) %all-to-all-start.2) | async-done | bytes 1671200 | tf_op jit(solution)/shard_map/all_to_all | solution.py:234
  87.1 2.3 %shard_map.114 = (f32[8,208,128]{2,1,0:T(8,128)S(1)}, bf16[8,208,128]{2,1,0:T(8,128)(2,1)S(1)}) custom-call(s32[1]{0:T(128)} %bitcast.1.core_ref, s32[2,192]{1,0:T(2,128)} %bitcast.40, bf16[384,2176]{1,0:T(8,128)(2,1)} %bitcast.18.x_ref), custom_call_target="tpu_custom_call" | custom-call | flops 301989888 | bytes 1672708 | tf_op jit(solution)/shard_map/pallas_call | solution.py:30
  89.4 5.6 %collective-permute-start.5 = (bf16[8,208,128]{2,1,0:T(8,128)(2,1)S(1)}, bf16[8,208,128]{2,1,0:T(8,128)(2,1)S(1)}, u32[]{:S(2)}, u32[]{:S(2)}) collective-permute-start(bf16[8,208,128]{2,1,0:T(8,128)(2,1)S(1)} %get-tuple-element.26), channel_id=1, source_target_pairs={{0,1},{1,0},{2,3},{3,2},{4,5},{5,4},{6,7},{7,6},{8,9},{9,8},{10,11... | collective-permute-start | bytes 1277960 | tf_op jit(solution)/shard_map/ppermute | solution.py:232
  95.1 1.4 %collective-permute-done.5.got_ref = bf16[8,208,128]{2,1,0:T(8,128)(2,1)S(1)} collective-permute-done((bf16[8,208,128]{2,1,0:T(8,128)(2,1)S(1)}, bf16[8,208,128]{2,1,0:T(8,128)(2,1)S(1)}, u32[]{:S(2)}, u32[]{:S(2)}) %collective-permute-start.5) | collective-permute-done | bytes 426016 | tf_op jit(solution)/shard_map/ppermute | solution.py:232
  96.4 0.8 shard_map.115
  97.3 6.0 %all-to-all-start.3 = ((bf16[8,208,128]{2,1,0:T(8,128)(2,1)}), bf16[8,208,128]{2,1,0:T(8,128)(2,1)S(1)}, u32[]{:S(2)}, u32[]{:S(2)}) async-start(bf16[8,208,128]{2,1,0:T(8,128)(2,1)} %shard_map.115), calls=%async_computation.3 | async-start | bytes 851968 | tf_op jit(solution)/shard_map/all_to_all | solution.py:234
  103.3 0.0 collective-permute-done.6.refs_0_
  103.3 0.0 collective-permute-done.7.refs_1_
  103.3 0.0 collective-permute-done.8.refs_2_
  103.3 0.0 copy-start.1
  103.3 1.0 copy-done.1
  104.3 7.9 %shard_map.118 = (bf16[448,2048]{1,0:T(8,128)(2,1)}, bf16[448,2048]{1,0:T(8,128)(2,1)}, bf16[448,2048]{1,0:T(8,128)(2,1)}) custom-call(s32[1]{0:T(128)} %bitcast.5.par_ref, bf16[384,1024]{1,0:T(8,128)(2,1)S(1)} %bitcast.32, bf16[192,1024]{1,0:T(8,128)(2,1)S(1)} %collective-permute-done.low_ref, bf16[192,1024]{1,0:T(8,128)(2,1)S(1)} %copy-done.1, ...), custom_call_target="tpu_custom_call" | custom-call | flops 2113929216 | bytes 10715140 | tf_op jit(solution)/shard_map/pallas_call | solution.py:30
  112.2 6.9 %all-to-all-done.3.x_ref = bf16[8,208,128]{2,1,0:T(8,128)(2,1)S(1)} async-done(((bf16[8,208,128]{2,1,0:T(8,128)(2,1)}), bf16[8,208,128]{2,1,0:T(8,128)(2,1)S(1)}, u32[]{:S(2)}, u32[]{:S(2)}) %all-to-all-start.3) | async-done | bytes 426016 | tf_op jit(solution)/shard_map/all_to_all | solution.py:234
  119.1 1.4 %shard_map.116 = (bf16[192,128]{1,0:T(8,128)(2,1)}, f32[2,192]{1,0:T(2,128)}) custom-call(bf16[2,192]{1,0:T(2,128)(2,1)} %bitcast.42, bf16[8,208,128]{2,1,0:T(8,128)(2,1)S(1)} %all-to-all-done.3.x_ref), custom_call_target="tpu_custom_call" | custom-call | bytes 426752 | tf_op jit(solution)/shard_map/pallas_call | solution.py:30
Async XLA Ops:
  3.6 20.8 %all-to-all-start.1 = ((bf16[16,24,1024]{2,1,0:T(8,128)(2,1)}), bf16[16,24,1024]{2,1,0:T(8,128)(2,1)S(1)}, u32[]{:S(2)}, u32[]{:S(2)}) async-start(bf16[16,24,1024]{2,1,0:T(8,128)(2,1)} %bitcast.34), calls=%async_computation.1 | async-start | bytes 1572864 | tf_op jit(solution)/shard_map/all_to_all | solution.py:234
  11.2 29.9 %collective-permute-start.2 = (bf16[448,2048]{1,0:T(8,128)(2,1)}, bf16[448,2048]{1,0:T(8,128)(2,1)}, u32[]{:S(2)}, u32[]{:S(2)}) collective-permute-start(bf16[448,2048]{1,0:T(8,128)(2,1)} %bitcast.11.refs_0_.refs_2_), channel_id=1, source_target_pairs={{0,1},{1,0},{2,3},{3,2},{4,5},{5,4},{6,7},{7,6},{8,9},{9,8},{10,11... | collective-permute-start | bytes 5505032 | tf_op jit(solution)/shard_map/ppermute | solution.py:232
  12.2 28.9 %collective-permute-start.3 = (bf16[448,2048]{1,0:T(8,128)(2,1)}, bf16[448,2048]{1,0:T(8,128)(2,1)}, u32[]{:S(2)}, u32[]{:S(2)}) collective-permute-start(bf16[448,2048]{1,0:T(8,128)(2,1)} %bitcast.13.refs_1_.refs_3_), channel_id=1, source_target_pairs={{0,1},{1,0},{2,3},{3,2},{4,5},{5,4},{6,7},{7,6},{8,9},{9,8},{10,11... | collective-permute-start | bytes 5505032 | tf_op jit(solution)/shard_map/ppermute | solution.py:232
  12.3 37.1 %collective-permute-start.4 = (bf16[448,2048]{1,0:T(8,128)(2,1)}, bf16[448,2048]{1,0:T(8,128)(2,1)}, u32[]{:S(2)}, u32[]{:S(2)}) collective-permute-start(bf16[448,2048]{1,0:T(8,128)(2,1)} %bitcast.16.refs_0_), channel_id=1, source_target_pairs={{0,1},{1,0},{2,3},{3,2},{4,5},{5,4},{6,7},{7,6},{8,9},{9,8},{10,11... | collective-permute-start | bytes 5505032 | tf_op jit(solution)/shard_map/ppermute | solution.py:232
  24.4 25.0 %all-to-all-start = ((bf16[16,24,2048]{2,1,0:T(8,128)(2,1)}), bf16[16,24,2048]{2,1,0:T(8,128)(2,1)S(1)}, u32[]{:S(2)}, u32[]{:S(2)}) async-start(bf16[16,24,2048]{2,1,0:T(8,128)(2,1)} %bitcast.33), calls=%async_computation | async-start | bytes 3145728 | tf_op jit(solution)/shard_map/all_to_all | solution.py:234
  28.2 12.9 %collective-permute-start = (bf16[192,1024]{1,0:T(8,128)(2,1)S(1)}, bf16[192,1024]{1,0:T(8,128)(2,1)S(1)}, u32[]{:S(2)}, u32[]{:S(2)}) collective-permute-start(bf16[192,1024]{1,0:T(8,128)(2,1)S(1)} %bitcast.37), channel_id=1, source_target_pairs={{0,2},{2,4},{4,6},{6,8},{8,10},{10,12},{12,14},{14,0},{1,3},{3,5},... | collective-permute-start | bytes 1179656 | tf_op jit(solution)/shard_map/ppermute | solution.py:233
  29.9 11.2 %collective-permute-start.1 = (bf16[192,1024]{1,0:T(8,128)(2,1)S(1)}, bf16[192,1024]{1,0:T(8,128)(2,1)S(1)}, u32[]{:S(2)}, u32[]{:S(2)}) collective-permute-start(bf16[192,1024]{1,0:T(8,128)(2,1)S(1)} %bitcast.36), channel_id=1, source_target_pairs={{0,14},{2,0},{4,2},{6,4},{8,6},{10,8},{12,10},{14,12},{1,15},{3,1}... | collective-permute-start | bytes 1179656 | tf_op jit(solution)/shard_map/ppermute | solution.py:233
  41.1 25.4 %copy-start = (bf16[192,1024]{1,0:T(8,128)(2,1)}, bf16[192,1024]{1,0:T(8,128)(2,1)S(1)}, u32[]{:S(2)}) copy-start(bf16[192,1024]{1,0:T(8,128)(2,1)S(1)} %collective-permute-done.1.high_ref) | copy-start | bytes 1179652
  60.1 27.0 %all-to-all-start.2 = ((bf16[16,24,2176]{2,1,0:T(8,128)(2,1)}), bf16[16,24,2176]{2,1,0:T(8,128)(2,1)}, u32[]{:S(2)}, u32[]{:S(2)}) async-start(bf16[16,24,2176]{2,1,0:T(8,128)(2,1)} %bitcast.35), calls=%async_computation.2 | async-start | bytes 3342336 | tf_op jit(solution)/shard_map/all_to_all | solution.py:234
  72.7 30.5 %collective-permute-start.6 = (bf16[448,2048]{1,0:T(8,128)(2,1)}, bf16[448,2048]{1,0:T(8,128)(2,1)}, u32[]{:S(2)}, u32[]{:S(2)}) collective-permute-start(bf16[448,2048]{1,0:T(8,128)(2,1)} %get-tuple-element.31), channel_id=1, source_target_pairs={{0,1},{1,0},{2,3},{3,2},{4,5},{5,4},{6,7},{7,6},{8,9},{9,8},{10,11... | collective-permute-start | bytes 5505032 | tf_op jit(solution)/shard_map/ppermute | solution.py:232
  76.1 27.2 %collective-permute-start.7 = (bf16[448,2048]{1,0:T(8,128)(2,1)}, bf16[448,2048]{1,0:T(8,128)(2,1)}, u32[]{:S(2)}, u32[]{:S(2)}) collective-permute-start(bf16[448,2048]{1,0:T(8,128)(2,1)} %get-tuple-element.32), channel_id=1, source_target_pairs={{0,1},{1,0},{2,3},{3,2},{4,5},{5,4},{6,7},{7,6},{8,9},{9,8},{10,11... | collective-permute-start | bytes 5505032 | tf_op jit(solution)/shard_map/ppermute | solution.py:232
  76.1 27.2 %collective-permute-start.8 = (bf16[448,2048]{1,0:T(8,128)(2,1)}, bf16[448,2048]{1,0:T(8,128)(2,1)}, u32[]{:S(2)}, u32[]{:S(2)}) collective-permute-start(bf16[448,2048]{1,0:T(8,128)(2,1)} %get-tuple-element.33), channel_id=1, source_target_pairs={{0,1},{1,0},{2,3},{3,2},{4,5},{5,4},{6,7},{7,6},{8,9},{9,8},{10,11... | collective-permute-start | bytes 5505032 | tf_op jit(solution)/shard_map/ppermute | solution.py:232
  89.4 7.0 %collective-permute-start.5 = (bf16[8,208,128]{2,1,0:T(8,128)(2,1)S(1)}, bf16[8,208,128]{2,1,0:T(8,128)(2,1)S(1)}, u32[]{:S(2)}, u32[]{:S(2)}) collective-permute-start(bf16[8,208,128]{2,1,0:T(8,128)(2,1)S(1)} %get-tuple-element.26), channel_id=1, source_target_pairs={{0,1},{1,0},{2,3},{3,2},{4,5},{5,4},{6,7},{7,6},{8,9},{9,8},{10,11... | collective-permute-start | bytes 1277960 | tf_op jit(solution)/shard_map/ppermute | solution.py:232
  97.3 21.8 %all-to-all-start.3 = ((bf16[8,208,128]{2,1,0:T(8,128)(2,1)}), bf16[8,208,128]{2,1,0:T(8,128)(2,1)S(1)}, u32[]{:S(2)}, u32[]{:S(2)}) async-start(bf16[8,208,128]{2,1,0:T(8,128)(2,1)} %shard_map.115), calls=%async_computation.3 | async-start | bytes 851968 | tf_op jit(solution)/shard_map/all_to_all | solution.py:234
  103.3 1.0 copy-start.1

commit v3 on v2

v3 whole, which is shorter than its diff:
```python
import functools

import jax
import jax.numpy as jnp
from jax import lax
from jax.experimental import pallas as pl
from jax.experimental.pallas import tpu as pltpu
from jax.sharding import PartitionSpec as P


EP = ("y", "x")
LANES = 128
BF16 = jnp.bfloat16
F32 = jnp.float32
NN = (((1,), (0,)), ((), ()))
NT = (((1,), (1,)), ((), ()))
TN = (((0,), (0,)), ((), ()))
IN_VMEM = pl.BlockSpec(memory_space=pltpu.VMEM)
IN_HBM = pl.BlockSpec(memory_space=pltpu.HBM)
IN_SMEM = pl.BlockSpec(memory_space=pltpu.SMEM)


def dot(a, b, dims):
    return lax.dot_general(a, b, dims, preferred_element_type=F32)


def call(kernel, outs, *args, scratch=(), flops=0, mib=24):
    place = {"v": pltpu.VMEM, "h": pltpu.HBM, "w": pltpu.HBM}
    spec = {"v": IN_VMEM, "w": IN_VMEM, "h": IN_HBM, "s": IN_SMEM}
    moved = sum(a.size * a.dtype.itemsize for a, _ in args)
    kernel_call = pl.pallas_call(
        kernel,
        out_shape=[place[m](shape, dtype) for shape, dtype, m in outs],
        in_specs=[spec[m] for _, m in args],
        out_specs=[spec[m] for _, _, m in outs],
        scratch_shapes=list(scratch),
        cost_estimate=pl.CostEstimate(flops=flops, bytes_accessed=moved, transcendentals=0),
        compiler_params=pltpu.CompilerParams(vmem_limit_bytes=mib * 1024 * 1024),
    )
    return kernel_call(
        *(a if m == "s" else pltpu.with_memory_space_constraint(a, place[m]) for a, m in args)
    )


def slots_of(core, routes, experts, half):
    top_k, rows = routes.shape
    expert = lax.broadcasted_iota(jnp.int32, (experts, rows), 0)
    hits = [routes[k : k + 1, :] == expert for k in range(top_k)]
    named = functools.reduce(jnp.logical_or, hits)
    before = lax.broadcasted_iota(jnp.int32, (rows, rows), 0) < lax.broadcasted_iota(
        jnp.int32, (rows, rows), 1
    )
    ones = lambda mask: jnp.where(mask, 1.0, 0.0).astype(BF16)
    count = dot(ones(named), ones(before), NN)
    slots = []
    for k in range(top_k):
        place = jnp.sum(jnp.where(hits[k], count, 0.0), axis=0, keepdims=True).astype(jnp.int32)
        place = place - core * half
        inside = (place >= 0) & (place < half)
        slots.append(jnp.where(inside, routes[k : k + 1, :] * half + place, -1))
    return slots


def masks_of(slots, count):
    row = lax.broadcasted_iota(jnp.int32, (count, slots[0].shape[1]), 0)
    return [row == s for s in slots]


def send_tokens(experts, half, core_ref, par_ref, routes_ref, tok_ref, out_ref, tok, sem):
    part = out_ref.shape[1]
    copy = pltpu.make_async_copy(
        tok_ref.at[:, pl.ds(pl.multiple_of(par_ref[0] * part, part), part)], tok, sem
    )
    copy.start()
    masks = masks_of(slots_of(core_ref[0], routes_ref[...], experts, half), experts * half)
    pick = functools.reduce(lambda a, m: jnp.where(m, 1.0, a), masks, jnp.zeros(masks[0].shape, F32))
    copy.wait()
    out_ref[...] = dot(pick.astype(BF16), tok[...], NN).astype(BF16)


def send_cotangents(experts, half, core_ref, routes_ref, gates_ref, cot_ref, out_ref):
    masks = masks_of(slots_of(core_ref[0], routes_ref[...], experts, half), experts * half)
    gates = gates_ref[...].astype(F32)
    weigh = jnp.zeros(masks[0].shape, F32)
    for k, mask in enumerate(masks):
        weigh = jnp.where(mask, gates[k : k + 1, :], weigh)
    out_ref[...] = dot(weigh.astype(BF16), cot_ref[...], NN).astype(BF16)


def join_rows(low_ref, high_ref, both):
    rows = low_ref.shape[0]
    both[:rows] = low_ref[...]
    both[rows:] = high_ref[...]


def forward(par_ref, mine_ref, low_ref, high_ref, *refs):
    weights, outs, (buf, sem, both, *stages, out_sem) = refs[:4], refs[4:7], refs[7:]
    copies = [pltpu.make_async_copy(w, buf.at[n], sem.at[n]) for n, w in enumerate(weights)]
    copies[0].start()
    copies[1].start()
    join_rows(low_ref, high_ref, both)
    part = low_ref.shape[1]
    here = pl.ds(pl.multiple_of(par_ref[0] * part, part), part)
    there = pl.ds(pl.multiple_of((1 - par_ref[0]) * part, part), part)

    def product(n):
        copies[n].wait()
        if n + 2 < 4:
            copies[n + 2].start()
        return dot(mine_ref[...], buf[n, :, here], NT) + dot(both[...], buf[n, :, there], NT)

    done = []
    for p in range(2):
        pre = product(2 * p)
        up = product(2 * p + 1)
        sig = jax.nn.sigmoid(pre)
        act = pre * sig
        stages[0][p] = (act * up).astype(BF16)
        stages[1][p] = up * sig * (1.0 + pre * (1.0 - sig))
        stages[2][p] = act
        for n in range(3):
            copy = pltpu.make_async_copy(stages[n].at[p], outs[n].at[p], out_sem.at[3 * p + n])
            copy.start()
            done.append(copy)
    for copy in done:
        copy.wait()


def gather_columns(weights, buf, sem, side, width):
    step = width // 8
    copies = []
    for n, w in enumerate(weights):
        for m in range(4):
            cols = pl.ds(pl.multiple_of((2 * m + side) * step, step), step)
            to = buf.at[n, :, m * step : (m + 1) * step]
            copies.append(pltpu.make_async_copy(w.at[:, cols], to, sem.at[4 * n + m]))
    return copies


def input_grad(pre, up, buf):
    total = dot(pre[0], buf[0], NN)
    total += dot(up[0], buf[1], NN)
    total += dot(pre[1], buf[2], NN)
    return total + dot(up[1], buf[3], NN)


def backward(par_ref, cot_ref, *refs):
    mid_refs, down, weights, outs, scratch = refs[:3], refs[3:5], refs[5:9], refs[9:14], refs[14:]
    low_ref, high_ref, pre_ref, up_ref, gate_ref = outs
    hid, slope, act, mid_sem, wd, wd_sem, buf, sem, pre, up, out_sem = scratch
    rows, width = cot_ref.shape
    mid_copies = [
        [pltpu.make_async_copy(r.at[p], to.at[p], mid_sem.at[3 * p + n])
         for n, (r, to) in enumerate(zip(mid_refs, (hid, slope, act)))]
        for p in range(2)
    ]
    downs = [pltpu.make_async_copy(w, wd.at[p], wd_sem.at[p]) for p, w in enumerate(down)]
    columns = gather_columns(weights, buf, sem, 1 - par_ref[0], width)
    downs[0].start()
    for copy in mid_copies[0]:
        copy.start()
    downs[1].start()
    gate = jnp.zeros((rows, 1), F32)
    done = []
    for p in range(2):
        downs[p].wait()
        for copy in mid_copies[1] if p == 0 else columns:
            copy.start()
        back = dot(cot_ref[...], wd[p], NT)
        for copy in mid_copies[p]:
            copy.wait()
        gate = gate + jnp.sum(hid[p].astype(F32) * back, axis=1, keepdims=True)
        pre[p] = (back * slope[p]).astype(BF16)
        up[p] = (back * act[p]).astype(BF16)
        for n, (frm, to) in enumerate(((pre, pre_ref), (up, up_ref))):
            copy = pltpu.make_async_copy(frm.at[p], to.at[p], out_sem.at[2 * p + n])
            copy.start()
            done.append(copy)
    for copy in columns:
        copy.wait()
    total = input_grad(pre, up, buf).astype(BF16)
    wide = jnp.broadcast_to(gate, (rows, LANES))
    gate_ref[...] = wide
    low_ref[:, : width // 2] = total[: rows // 2]
    low_ref[:, width // 2 :] = wide[: rows // 2].astype(BF16)
    high_ref[:, : width // 2] = total[rows // 2 :]
    high_ref[:, width // 2 :] = wide[rows // 2 :].astype(BF16)
    for copy in done:
        copy.wait()


def own_half(par_ref, pre_ref, up_ref, gate_ref, *refs):
    weights, (out_ref, buf, sem) = refs[:4], refs[4:]
    half = buf.shape[2]
    columns = gather_columns(weights, buf, sem, par_ref[0], 2 * half)
    for copy in columns:
        copy.start()
    for copy in columns:
        copy.wait()
    out_ref[:, :half] = input_grad(pre_ref, up_ref, buf)
    out_ref[:, half:] = gate_ref[...]


def add_pair(own_ref, low_ref, high_ref, out_ref):
    rows = low_ref.shape[0]
    out_ref[:rows] = (own_ref[:rows] + low_ref[...].astype(F32)).astype(BF16)
    out_ref[rows:] = (own_ref[rows:] + high_ref[...].astype(F32)).astype(BF16)


def weight_grads(p, par_ref, mine_ref, low_ref, high_ref, cot_ref, hid_ref, pre_ref, up_ref, *refs):
    both = refs[-1]
    received, outs = (refs[:3], refs[3:6]) if len(refs) > 4 else ((None,) * 3, refs[:3])
    join_rows(low_ref, high_ref, both)
    part = low_ref.shape[1]
    here = pl.ds(pl.multiple_of(par_ref[0] * part, part), part)
    there = pl.ds(pl.multiple_of((1 - par_ref[0]) * part, part), part)

    def put(n, cols, grad):
        if received[n] is not None:
            grad += received[n][:, cols].astype(F32)
        outs[n][:, cols] = grad.astype(BF16)

    for n, left in enumerate((pre_ref, up_ref)):
        put(n, here, dot(left[p], mine_ref[...], TN))
        put(n, there, dot(left[p], both[...], TN))
    put(2, slice(None), dot(hid_ref[p], cot_ref[...], TN))


def combine(experts, half, core_ref, routes_ref, x_ref, keep_ref, send_ref):
    blocks, padded, _ = keep_ref.shape
    rows = routes_ref.shape[1]
    width = 2 * blocks * LANES
    core = core_ref[0]
    masks = masks_of(slots_of(core, routes_ref[...], experts, half), experts * half)
    pick = functools.reduce(lambda a, m: jnp.where(m, 1.0, a), masks, jnp.zeros(masks[0].shape, F32))
    grads = dot(pick.astype(BF16), x_ref[:, :width], TN)
    gate = x_ref[:, width : width + 1].astype(F32)
    lines = []
    for mask in masks:
        line = jnp.sum(jnp.where(mask, gate, 0.0), axis=0, keepdims=True)
        line = jnp.concatenate([line, jnp.zeros((1, 2 * LANES - rows), F32)], axis=1)
        lines += [line[:, :LANES], line[:, LANES:]]
    lines.append(jnp.zeros((padded - rows - len(lines), LANES), F32))
    tail = jnp.concatenate(lines, axis=0)
    for b in range(blocks):
        first = grads[:, 2 * b * LANES : (2 * b + 1) * LANES]
        second = grads[:, (2 * b + 1) * LANES : (2 * b + 2) * LANES]
        keep_ref[b, :rows, :] = jnp.where(core == 0, first, second)
        send_ref[b, :rows, :] = jnp.where(core == 0, second, first).astype(BF16)
        keep_ref[b, rows:, :] = tail
        send_ref[b, rows:, :] = tail.astype(BF16)


def join(turn_ref, keep_ref, got_ref, *out_refs):
    for k, out_ref in enumerate(out_refs):
        block = lax.rem(turn_ref[0] + k, len(out_refs))
        out_ref[...] = (keep_ref[block] + got_ref[block].astype(F32)).astype(BF16)


def finish(gates_ref, *refs):
    parts, (tok_ref, gate_ref) = refs[:-2], refs[-2:]
    top_k, rows = gates_ref.shape
    total = functools.reduce(jnp.add, [x[...].astype(F32) for x in parts])
    tok_ref[...] = total[:rows].astype(BF16)
    gates = gates_ref[...].astype(F32)
    for k in range(top_k):
        line = jnp.concatenate(
            [total[rows + 2 * k : rows + 2 * k + 1], total[rows + 2 * k + 1 : rows + 2 * k + 2]],
            axis=1,
        )
        gate_ref[k : k + 1, :] = line[:, :rows] / gates[k : k + 1, :]


def local(experts, tokens, cotangent, routing, gate_weights, gate_proj, up_proj, down_proj):
    rows, width = tokens.shape
    top_k = routing.shape[1]
    half = rows * top_k // experts
    count = experts * half
    part = width // 2
    depth = lax.axis_size("z")
    core = lax.axis_index("c").astype(jnp.int32).reshape(1)
    parity = (lax.axis_index("z") % 2).astype(jnp.int32).reshape(1)
    routes, gates = routing.T, gate_weights.T

    def swap(v):
        return lax.ppermute(v, "c", [(0, 1), (1, 0)])

    def shift(v, k):
        return lax.ppermute(v, "z", [(i, (i + k) % depth) for i in range(depth)])

    def exchange(v):
        return lax.all_to_all(v, EP, split_axis=0, concat_axis=0, tiled=True)

    dma = lambda n: pltpu.SemaphoreType.DMA((n,))

    own = (gate_proj[0].T, up_proj[0].T, down_proj[0])
    other = tuple(swap(w) for w in own)
    ff = own[0].shape[0]

    (tok_out,) = call(
        functools.partial(send_tokens, experts, half),
        [((count, part), BF16, "w")],
        (core, "s"), (parity, "s"), (routes, "w"), (tokens, "h"),
        scratch=[pltpu.VMEM((rows, part), BF16), pltpu.SemaphoreType.DMA],
        flops=2 * count * rows * part, mib=8,
    )
    mine = exchange(tok_out.reshape(experts, half, part)).reshape(count, part)
    (cot_out,) = call(
        functools.partial(send_cotangents, experts, half),
        [((count, width), BF16, "w")],
        (core, "s"), (routes, "w"), (gates, "w"), (cotangent, "w"),
        flops=2 * count * rows * width, mib=8,
    )
    cot = exchange(cot_out.reshape(experts, half, width)).reshape(count, width)
    low = shift(mine[: count // 2], 1)
    high = shift(mine[count // 2 :], -1)

    mid = lambda dtype, mode: ((2, count, ff), dtype, mode)
    mids = [pltpu.VMEM((2, count, ff), dtype) for dtype in (BF16, F32, F32)]
    proj = [(w, "h") for w in (own[0], own[1], other[0], other[1])]
    hid, slope, act = call(
        forward,
        [mid(BF16, "h"), mid(F32, "h"), mid(F32, "h")],
        (parity, "s"), (mine, "v"), (low, "v"), (high, "v"), *proj,
        scratch=[
            pltpu.VMEM((4, ff, width), BF16), dma(4), pltpu.VMEM((count, part), BF16),
            *mids, dma(6),
        ],
        flops=8 * count * width * ff, mib=24,
    )
    message = (count // 2, part + LANES)
    packed = [pltpu.VMEM((4, ff, part), BF16), dma(16)]
    to_low, to_high, pre, up, gate = call(
        backward,
        [(message, BF16, "v"), (message, BF16, "v"), mid(BF16, "h"), mid(BF16, "h"), ((count, LANES), F32, "w")],
        (parity, "s"), (cot, "v"), (hid, "h"), (slope, "h"), (act, "h"),
        (own[2], "h"), (other[2], "h"), *proj,
        scratch=[
            *mids, dma(6), pltpu.VMEM((2, ff, width), BF16), dma(2), *packed,
            mids[0], mids[0], dma(4),
        ],
        flops=8 * count * width * ff, mib=24,
    )
    from_low, from_high = shift(to_low, -1), shift(to_high, 1)
    (kept,) = call(
        own_half,
        [((count, part + LANES), F32, "v")],
        (parity, "s"), (pre, "w"), (up, "w"), (gate, "w"), *proj,
        scratch=packed,
        flops=4 * count * width * ff, mib=16,
    )
    (pair,) = call(
        add_pair, [((count, part + LANES), BF16, "w")], (kept, "v"), (from_low, "v"), (from_high, "v"), mib=8
    )
    returned = exchange(pair.reshape(experts, half, part + LANES)).reshape(count, part + LANES)

    pieces = [(v, "v") for v in (mine, low, high, cot)] + [(v, "w") for v in (hid, pre, up)]
    shard = [((ff, width), BF16, "w")] * 3
    theirs = call(
        functools.partial(weight_grads, 1), shard, (parity, "s"), *pieces,
        scratch=[pltpu.VMEM((count, part), BF16)],
        flops=6 * count * width * ff, mib=16,
    )
    received = [(swap(g), "w") for g in theirs]
    grad_gate, grad_up, grad_down = call(
        functools.partial(weight_grads, 0), shard, (parity, "s"), *pieces, *received,
        scratch=[pltpu.VMEM((count, part), BF16)],
        flops=6 * count * width * ff, mib=24,
    )

    steps = depth // 2
    block = (rows + 16, LANES)
    keep, send = call(
        functools.partial(combine, experts, half),
        [((steps, *block), F32, "v"), ((steps, *block), BF16, "v")],
        (core, "s"), (routes, "w"), (returned, "v"),
        flops=2 * count * rows * part, mib=12,
    )
    turn = (lax.axis_index("z") // 2).astype(jnp.int32).reshape(1)
    parts = call(join, [(block, BF16, "v")] * steps, (turn, "s"), (keep, "v"), (swap(send), "v"), mib=4)
    sums = [parts[0]] + [shift(parts[k], 2 * k) for k in range(1, steps)]
    grad_tokens, grad_gates = call(
        finish,
        [((rows, LANES), BF16, "w"), ((top_k, rows), F32, "w")],
        (gates, "w"), *((v, "v") for v in sums), mib=4,
    )
    return (grad_tokens, grad_gates.T, grad_gate.T[None], grad_up.T[None], grad_down[None])


def solution(mesh):
    devices = mesh.devices.reshape(4, 4, 8, 2)
    inner = jax.sharding.Mesh(devices, ("y", "x", "z", "c"))
    ep, tp = EP, ("z", "c")

    def body(*args):
        return local(16, *args)

    return jax.shard_map(
        body,
        mesh=inner,
        in_specs=(
            P(ep, None),
            P(ep, None),
            P(ep, None),
            P(ep, None),
            P(ep, None, tp),
            P(ep, None, tp),
            P(ep, tp, None),
        ),
        out_specs=(
            P(ep, tp),
            P(ep, None),
            P(ep, None, tp),
            P(ep, None, tp),
            P(ep, tp, None),
        ),
        check_vma=False,
    )
```

time: 121 us -> 132 us (1.091)
  blocking collectives: 0 us -> 18 us
  starting transfers between devices: 40.7 us -> 35.2 us
  waiting for transfers between devices: 34.5 us -> 30.1 us
  Pallas kernels: 43.5 us -> 46.2 us
    all_to_all x0 -> x1, blocking collectives: none -> 18 us  [exchange(): return lax.all_to_all(v, EP, split_axis=0, concat_axis=0, tiled=True)]
    all_to_all x4 -> x2, waiting for transfers between devices: 26.1 us -> 8.77 us  [exchange(): return lax.all_to_all(v, EP, split_axis=0, concat_axis=0, tiled=True)]
    ppermute x9 -> x14, waiting for transfers between devices: 8.41 us -> 21.3 us  [the longest x7 20 us: shift(): return lax.ppermute(v, 'z', [(i, (i + k) % depth) for i in range(depth)])]
    all_to_all x4 -> x2, starting transfers between devices: 23.7 us -> 11.3 us  [exchange(): return lax.all_to_all(v, EP, split_axis=0, concat_axis=0, tiled=True)]
    ppermute x9 -> x14, starting transfers between devices: 16.9 us -> 23.9 us  [the longest x7 15.9 us: shift(): return lax.ppermute(v, 'z', [(i, (i + k) % depth) for i in range(depth)])]
    pallas_call x9 -> x11, Pallas kernels: 43.5 us -> 46.2 us  [call(): kernel_call(*(a if m == 's' else pltpu.with_memory_space_constraint(a, pl...]
  transfers between devices with their start and end apart: 13 -> 16, of which waited for: 5 -> 9; matrix products, arithmetic and copies ran while one was open for 0% -> 0% of each run, Pallas kernels for 24% -> 15%
where the time goes in v3:
time: 132 us; the launch traced here: 131 us
  Pallas kernels  46.2 us (35%)
  starting transfers between devices  35.2 us (27%)
  waiting for transfers between devices  30.1 us (23%)
  blocking collectives  18 us (14%)
    pallas_call x11, Pallas kernels, call(): kernel_call(*(a if m == 's' else pltpu.with_memory_space_constraint(a, pl...  46.2 us
    ppermute x7, waiting for transfers between devices, shift(): return lax.ppermute(v, 'z', [(i, (i + k) % depth) for i in range(depth)])  20 us
    all_to_all x1, blocking collectives, exchange(): return lax.all_to_all(v, EP, split_axis=0, concat_axis=0, tiled=True)  18 us
    ppermute x7, starting transfers between devices, shift(): return lax.ppermute(v, 'z', [(i, (i + k) % depth) for i in range(depth)])  15.9 us
    all_to_all x2, starting transfers between devices, exchange(): return lax.all_to_all(v, EP, split_axis=0, concat_axis=0, tiled=True)  11.3 us
    all_to_all x2, waiting for transfers between devices, exchange(): return lax.all_to_all(v, EP, split_axis=0, concat_axis=0, tiled=True)  8.77 us
    ppermute x7, starting transfers between devices, swap(): return lax.ppermute(v, 'c', [(0, 1), (1, 0)])  8.05 us
  transfers between devices with their start and end apart: 16, of which 9 were waited for; matrix products, arithmetic and copies ran while one was open for 0% of the time, Pallas kernels for 15%

profile of v3, /device:TPU:1, one launch (start us, length us, event | category | flops | bytes accessed | tf_op | source)
XLA Modules:
  0.0 131.3 jit_solution(8649037448656780662)
XLA Ops:
  0.6 3.0 %shard_map.111 = bf16[384,1024]{1,0:T(8,128)(2,1)} custom-call(s32[1]{0:T(128)} %bitcast.2.core_ref, s32[1]{0:T(128)} %bitcast.4.par_ref, s32[2,192]{1,0:T(2,128)} %bitcast.40, bf16[192,2048]{1,0:T(8,128)(2,1)} %tok_ref.1), custom_call_target="tpu_custom_call" | custom-call | flops 150994944 | bytes 787976 | tf_op jit(solution)/shard_map/pallas_call | solution.py:40
  3.6 7.6 %all-to-all-start.1 = ((bf16[16,24,1024]{2,1,0:T(8,128)(2,1)}), bf16[16,24,1024]{2,1,0:T(8,128)(2,1)S(1)}, u32[]{:S(2)}, u32[]{:S(2)}) async-start(bf16[16,24,1024]{2,1,0:T(8,128)(2,1)} %bitcast.37), calls=%async_computation.1 | async-start | bytes 1572864 | tf_op jit(solution)/shard_map/all_to_all | solution.py:292
  11.2 1.0 collective-permute-start.2
  12.2 0.1 collective-permute-start.3
  12.3 0.4 collective-permute-start.4
  12.7 3.0 %shard_map.110 = bf16[384,2048]{1,0:T(8,128)(2,1)} custom-call(s32[1]{0:T(128)} %bitcast.2.core_ref, s32[2,192]{1,0:T(2,128)} %bitcast.41, bf16[2,192]{1,0:T(2,128)(2,1)} %bitcast.43, bf16[192,2048]{1,0:T(8,128)(2,1)} %cot_ref.1), custom_call_target="tpu_custom_call" | custom-call | flops 301989888 | bytes 788740 | tf_op jit(solution)/shard_map/pallas_call | solution.py:40
  15.8 8.6 %all-to-all-done.1 = bf16[16,24,1024]{2,1,0:T(8,128)(2,1)S(1)} async-done(((bf16[16,24,1024]{2,1,0:T(8,128)(2,1)}), bf16[16,24,1024]{2,1,0:T(8,128)(2,1)S(1)}, u32[]{:S(2)}, u32[]{:S(2)}) %all-to-all-start.1) | async-done | bytes 786464 | tf_op jit(solution)/shard_map/all_to_all | solution.py:292
  24.4 3.7 %all-to-all-start = ((bf16[16,24,2048]{2,1,0:T(8,128)(2,1)}), bf16[16,24,2048]{2,1,0:T(8,128)(2,1)S(1)}, u32[]{:S(2)}, u32[]{:S(2)}) async-start(bf16[16,24,2048]{2,1,0:T(8,128)(2,1)} %bitcast.35), calls=%async_computation | async-start | bytes 3145728 | tf_op jit(solution)/shard_map/all_to_all | solution.py:292
  28.1 0.1 fusion
  28.2 1.7 %collective-permute-start = (bf16[192,1024]{1,0:T(8,128)(2,1)S(1)}, bf16[192,1024]{1,0:T(8,128)(2,1)S(1)}, u32[]{:S(2)}, u32[]{:S(2)}) collective-permute-start(bf16[192,1024]{1,0:T(8,128)(2,1)S(1)} %bitcast.39), channel_id=1, source_target_pairs={{0,2},{2,4},{4,6},{6,8},{8,10},{10,12},{12,14},{14,0},{1,3},{3,5},... | collective-permute-start | bytes 1179656 | tf_op jit(solution)/shard_map/ppermute | solution.py:289
  29.9 4.2 %collective-permute-start.1 = (bf16[192,1024]{1,0:T(8,128)(2,1)S(1)}, bf16[192,1024]{1,0:T(8,128)(2,1)S(1)}, u32[]{:S(2)}, u32[]{:S(2)}) collective-permute-start(bf16[192,1024]{1,0:T(8,128)(2,1)S(1)} %bitcast.38), channel_id=1, source_target_pairs={{0,14},{2,0},{4,2},{6,4},{8,6},{10,8},{12,10},{14,12},{1,15},{3,1}... | collective-permute-start | bytes 1179656 | tf_op jit(solution)/shard_map/ppermute | solution.py:289
  34.1 7.0 %collective-permute-done.low_ref = bf16[192,1024]{1,0:T(8,128)(2,1)S(1)} collective-permute-done((bf16[192,1024]{1,0:T(8,128)(2,1)S(1)}, bf16[192,1024]{1,0:T(8,128)(2,1)S(1)}, u32[]{:S(2)}, u32[]{:S(2)}) %collective-permute-start) | collective-permute-done | bytes 393248 | tf_op jit(solution)/shard_map/ppermute | solution.py:289
  41.1 0.0 collective-permute-done.1.high_ref
  41.1 0.0 copy-start
  41.1 0.0 collective-permute-done.2.refs_2_.refs_7_
  41.1 0.0 collective-permute-done.3.refs_3_.refs_8_
  41.1 7.3 %shard_map.112 = (bf16[2,384,448]{2,1,0:T(8,128)(2,1)}, f32[2,384,448]{2,1,0:T(8,128)}, f32[2,384,448]{2,1,0:T(8,128)}) custom-call(s32[1]{0:T(128)} %bitcast.4.par_ref, bf16[384,1024]{1,0:T(8,128)(2,1)S(1)} %bitcast.31, bf16[192,1024]{1,0:T(8,128)(2,1)S(1)} %collective-permute-done.low_ref, bf16[192,1024]{1,0:T(8,128)(2,1)S(1)} %collective-permute-done.1.high_ref, ...), custom_call_target="tpu_custom_call" | custom-call | flops 2818572288 | bytes 8912900 | tf_op jit(solution)/shard_map/pallas_call | solution.py:40
  48.4 0.1 all-to-all-done
  48.5 0.0 collective-permute-done.4.refs_4_
  48.5 8.9 %shard_map.113 = (bf16[192,1152]{1,0:T(8,128)(2,1)S(1)}, bf16[192,1152]{1,0:T(8,128)(2,1)S(1)}, bf16[2,384,448]{2,1,0:T(8,128)(2,1)}, bf16[2,384,448]{2,1,0:T(8,128)(2,1)}, f32[384,128]{1,0:T(8,128)}) custom-call(s32[1]{0:T(128)} %bitcast.4.par_ref, bf16[384,2048]{1,0:T(8,128)(2,1)S(1)} %bitcast.28, bf16[2,384,448]{2,1,0:T(8,128)(2,1)} %get-tuple-element.27.refs_0_.hid_ref, ...), custom_call_target="tpu_custom_call" | custom-call | flops 2818572288 | bytes 16023556 | tf_op jit(solution)/shard_map/pallas_call | solution.py:40
  57.5 0.0 copy-done
  57.5 6.2 %shard_map.119 = (bf16[448,2048]{1,0:T(8,128)(2,1)}, bf16[448,2048]{1,0:T(8,128)(2,1)}, bf16[448,2048]{1,0:T(8,128)(2,1)}) custom-call(s32[1]{0:T(128)} %bitcast.4.par_ref, bf16[384,1024]{1,0:T(8,128)(2,1)S(1)} %bitcast.32, bf16[192,1024]{1,0:T(8,128)(2,1)S(1)} %collective-permute-done.low_ref, bf16[192,1024]{1,0:T(8,128)(2,1)S(1)} %collective-permute-done.1.high_ref, ...), custom_call_target="tpu_custom_call" | custom-call | flops 2113929216 | bytes 5210116 | tf_op jit(solution)/shard_map/pallas_call | solution.py:40
  63.7 4.0 %collective-permute-start.11 = (bf16[448,2048]{1,0:T(8,128)(2,1)}, bf16[448,2048]{1,0:T(8,128)(2,1)}, u32[]{:S(2)}, u32[]{:S(2)}) collective-permute-start(bf16[448,2048]{1,0:T(8,128)(2,1)} %get-tuple-element.43), channel_id=1, source_target_pairs={{0,1},{1,0},{2,3},{3,2},{4,5},{5,4},{6,7},{7,6},{8,9},{9,8},{10,11... | collective-permute-start | bytes 5505032 | tf_op jit(solution)/shard_map/ppermute | solution.py:286
  67.7 0.0 collective-permute-start.12
  67.7 0.5 collective-permute-start.13
  68.2 5.6 %collective-permute-start.5 = (bf16[192,1152]{1,0:T(8,128)(2,1)S(1)}, bf16[192,1152]{1,0:T(8,128)(2,1)S(1)}, u32[]{:S(2)}, u32[]{:S(2)}) collective-permute-start(bf16[192,1152]{1,0:T(8,128)(2,1)S(1)} %get-tuple-element.33), channel_id=1, source_target_pairs={{0,14},{2,0},{4,2},{6,4},{8,6},{10,8},{12,10},{14,12},{1,15},{3,1}... | collective-permute-start | bytes 1327112 | tf_op jit(solution)/shard_map/ppermute | solution.py:289
  73.8 0.0 collective-permute-start.6
  73.8 5.5 %shard_map.114.own_ref = f32[384,1152]{1,0:T(8,128)S(1)} custom-call(s32[1]{0:T(128)} %bitcast.4.par_ref, bf16[2,384,448]{2,1,0:T(8,128)(2,1)} %get-tuple-element.30.pre_ref, bf16[2,384,448]{2,1,0:T(8,128)(2,1)} %get-tuple-element.31.up_ref, f32[384,128]{1,0:T(8,128)} %get-tuple-element.32.gate_ref, bf16[448,2048]{1,0:T(8,128)(2,1)} %bitcast.12.refs_0_.refs_5_, ...), custom_call_target="tpu_custom_call" | custom-call | flops 1409286144 | bytes 8912900 | tf_op jit(solution)/shard_map/pallas_call | solution.py:40
  79.3 4.0 %collective-permute-done.5.low_ref = bf16[192,1152]{1,0:T(8,128)(2,1)S(1)} collective-permute-done((bf16[192,1152]{1,0:T(8,128)(2,1)S(1)}, bf16[192,1152]{1,0:T(8,128)(2,1)S(1)}, u32[]{:S(2)}, u32[]{:S(2)}) %collective-permute-start.5) | collective-permute-done | bytes 442400 | tf_op jit(solution)/shard_map/ppermute | solution.py:289
  83.3 3.1 %collective-permute-done.6.high_ref = bf16[192,1152]{1,0:T(8,128)(2,1)S(1)} collective-permute-done((bf16[192,1152]{1,0:T(8,128)(2,1)S(1)}, bf16[192,1152]{1,0:T(8,128)(2,1)S(1)}, u32[]{:S(2)}, u32[]{:S(2)}) %collective-permute-start.6) | collective-permute-done | bytes 442400 | tf_op jit(solution)/shard_map/ppermute | solution.py:289
  86.4 1.1 shard_map.115
  87.5 18.0 %all_to_all.15 = bf16[16,24,1152]{2,1,0:T(8,128)(2,1)S(1)} all-to-all(bf16[16,24,1152]{2,1,0:T(8,128)(2,1)} %bitcast.36), channel_id=1, replica_groups=mesh['y'=4,'x'=4,'z'=8,'c'=2] {'y','x'}, dimensions={0} | all-to-all | bytes 1769472 | tf_op jit(solution)/shard_map/all_to_all | solution.py:292
  105.5 2.0 %shard_map.116 = (f32[4,208,128]{2,1,0:T(8,128)S(1)}, bf16[4,208,128]{2,1,0:T(8,128)(2,1)}) custom-call(s32[1]{0:T(128)} %bitcast.2.core_ref, s32[2,192]{1,0:T(2,128)} %bitcast.42, bf16[384,1152]{1,0:T(8,128)(2,1)S(1)} %bitcast.34), custom_call_target="tpu_custom_call" | custom-call | flops 150994944 | bytes 886276 | tf_op jit(solution)/shard_map/pallas_call | solution.py:40
  107.5 2.0 %collective-permute-start.7 = (bf16[4,208,128]{2,1,0:T(8,128)(2,1)}, bf16[4,208,128]{2,1,0:T(8,128)(2,1)S(1)}, u32[]{:S(2)}, u32[]{:S(2)}) collective-permute-start(bf16[4,208,128]{2,1,0:T(8,128)(2,1)} %get-tuple-element.36), channel_id=1, source_target_pairs={{0,1},{1,0},{2,3},{3,2},{4,5},{5,4},{6,7},{7,6},{8,9},{9,8},{10,11... | collective-permute-start | bytes 638984 | tf_op jit(solution)/shard_map/ppermute | solution.py:286
  109.5 1.3 collective-permute-done.7.got_ref
  110.8 0.1 collective-permute-start.8
  110.9 3.0 %collective-permute-start.9 = (bf16[208,128]{1,0:T(8,128)(2,1)S(1)}, bf16[208,128]{1,0:T(8,128)(2,1)S(1)}, u32[]{:S(2)}, u32[]{:S(2)}) collective-permute-start(bf16[208,128]{1,0:T(8,128)(2,1)S(1)} %get-tuple-element.39), channel_id=1, source_target_pairs={{0,8},{2,10},{4,12},{6,14},{8,0},{10,2},{12,4},{14,6},{1,9},{3,11}... | collective-permute-start | bytes 159752 | tf_op jit(solution)/shard_map/ppermute | solution.py:289
  113.9 2.1 %collective-permute-done.8.refs_1_ = bf16[208,128]{1,0:T(8,128)(2,1)S(1)} collective-permute-done((bf16[208,128]{1,0:T(8,128)(2,1)S(1)}, bf16[208,128]{1,0:T(8,128)(2,1)S(1)}, u32[]{:S(2)}, u32[]{:S(2)}) %collective-permute-start.8) | collective-permute-done | bytes 53280 | tf_op jit(solution)/shard_map/ppermute | solution.py:289
  116.0 1.3 %collective-permute-start.10 = (bf16[208,128]{1,0:T(8,128)(2,1)S(1)}, bf16[208,128]{1,0:T(8,128)(2,1)S(1)}, u32[]{:S(2)}, u32[]{:S(2)}) collective-permute-start(bf16[208,128]{1,0:T(8,128)(2,1)S(1)} %get-tuple-element.40), channel_id=1, source_target_pairs={{0,12},{2,14},{4,0},{6,2},{8,4},{10,6},{12,8},{14,10},{1,13},{3,15... | collective-permute-start | bytes 159752 | tf_op jit(solution)/shard_map/ppermute | solution.py:289
  117.4 0.5 collective-permute-done.9.refs_2_
  117.9 3.2 %collective-permute-done.10.refs_3_ = bf16[208,128]{1,0:T(8,128)(2,1)S(1)} collective-permute-done((bf16[208,128]{1,0:T(8,128)(2,1)S(1)}, bf16[208,128]{1,0:T(8,128)(2,1)S(1)}, u32[]{:S(2)}, u32[]{:S(2)}) %collective-permute-start.10) | collective-permute-done | bytes 53280 | tf_op jit(solution)/shard_map/ppermute | solution.py:289
  121.1 1.3 %shard_map.118 = (bf16[192,128]{1,0:T(8,128)(2,1)}, f32[2,192]{1,0:T(2,128)}) custom-call(bf16[2,192]{1,0:T(2,128)(2,1)} %bitcast.44, bf16[208,128]{1,0:T(8,128)(2,1)S(1)} %get-tuple-element.37.refs_0_, bf16[208,128]{1,0:T(8,128)(2,1)S(1)} %collective-permute-done.8.refs_1_, bf16[208,128]{1,0:T(8,128)(2,1)S(1)} %collective-permute-done.9.refs_2_, ...), custom_call_target="tpu_custom_call" | custom-call | bytes 213760 | tf_op jit(solution)/shard_map/pallas_call | solution.py:40
  122.4 0.0 collective-permute-done.11.refs_0_
  122.4 0.0 collective-permute-done.12.refs_1_
  122.4 0.0 collective-permute-done.13.refs_2_
  122.4 0.0 copy-start.1
  122.4 1.0 copy-done.1
  123.4 7.9 %shard_map.120 = (bf16[448,2048]{1,0:T(8,128)(2,1)}, bf16[448,2048]{1,0:T(8,128)(2,1)}, bf16[448,2048]{1,0:T(8,128)(2,1)}) custom-call(s32[1]{0:T(128)} %bitcast.4.par_ref, bf16[384,1024]{1,0:T(8,128)(2,1)S(1)} %bitcast.33, bf16[192,1024]{1,0:T(8,128)(2,1)S(1)} %collective-permute-done.low_ref, bf16[192,1024]{1,0:T(8,128)(2,1)S(1)} %copy-done.1, ...), custom_call_target="tpu_custom_call" | custom-call | flops 2113929216 | bytes 10715140 | tf_op jit(solution)/shard_map/pallas_call | solution.py:40
  (1 shorter events, 0.0 us)
Async XLA Ops:
  3.6 20.8 %all-to-all-start.1 = ((bf16[16,24,1024]{2,1,0:T(8,128)(2,1)}), bf16[16,24,1024]{2,1,0:T(8,128)(2,1)S(1)}, u32[]{:S(2)}, u32[]{:S(2)}) async-start(bf16[16,24,1024]{2,1,0:T(8,128)(2,1)} %bitcast.37), calls=%async_computation.1 | async-start | bytes 1572864 | tf_op jit(solution)/shard_map/all_to_all | solution.py:292
  11.2 29.9 %collective-permute-start.2 = (bf16[448,2048]{1,0:T(8,128)(2,1)}, bf16[448,2048]{1,0:T(8,128)(2,1)}, u32[]{:S(2)}, u32[]{:S(2)}) collective-permute-start(bf16[448,2048]{1,0:T(8,128)(2,1)} %bitcast.12.refs_0_.refs_5_), channel_id=1, source_target_pairs={{0,1},{1,0},{2,3},{3,2},{4,5},{5,4},{6,7},{7,6},{8,9},{9,8},{10,11... | collective-permute-start | bytes 5505032 | tf_op jit(solution)/shard_map/ppermute | solution.py:286
  12.2 28.9 %collective-permute-start.3 = (bf16[448,2048]{1,0:T(8,128)(2,1)}, bf16[448,2048]{1,0:T(8,128)(2,1)}, u32[]{:S(2)}, u32[]{:S(2)}) collective-permute-start(bf16[448,2048]{1,0:T(8,128)(2,1)} %bitcast.14.refs_1_.refs_6_), channel_id=1, source_target_pairs={{0,1},{1,0},{2,3},{3,2},{4,5},{5,4},{6,7},{7,6},{8,9},{9,8},{10,11... | collective-permute-start | bytes 5505032 | tf_op jit(solution)/shard_map/ppermute | solution.py:286
  12.3 36.2 %collective-permute-start.4 = (bf16[448,2048]{1,0:T(8,128)(2,1)}, bf16[448,2048]{1,0:T(8,128)(2,1)}, u32[]{:S(2)}, u32[]{:S(2)}) collective-permute-start(bf16[448,2048]{1,0:T(8,128)(2,1)} %bitcast.17.refs_3_), channel_id=1, source_target_pairs={{0,1},{1,0},{2,3},{3,2},{4,5},{5,4},{6,7},{7,6},{8,9},{9,8},{10,11... | collective-permute-start | bytes 5505032 | tf_op jit(solution)/shard_map/ppermute | solution.py:286
  24.4 24.1 %all-to-all-start = ((bf16[16,24,2048]{2,1,0:T(8,128)(2,1)}), bf16[16,24,2048]{2,1,0:T(8,128)(2,1)S(1)}, u32[]{:S(2)}, u32[]{:S(2)}) async-start(bf16[16,24,2048]{2,1,0:T(8,128)(2,1)} %bitcast.35), calls=%async_computation | async-start | bytes 3145728 | tf_op jit(solution)/shard_map/all_to_all | solution.py:292
  28.2 12.9 %collective-permute-start = (bf16[192,1024]{1,0:T(8,128)(2,1)S(1)}, bf16[192,1024]{1,0:T(8,128)(2,1)S(1)}, u32[]{:S(2)}, u32[]{:S(2)}) collective-permute-start(bf16[192,1024]{1,0:T(8,128)(2,1)S(1)} %bitcast.39), channel_id=1, source_target_pairs={{0,2},{2,4},{4,6},{6,8},{8,10},{10,12},{12,14},{14,0},{1,3},{3,5},... | collective-permute-start | bytes 1179656 | tf_op jit(solution)/shard_map/ppermute | solution.py:289
  29.9 11.2 %collective-permute-start.1 = (bf16[192,1024]{1,0:T(8,128)(2,1)S(1)}, bf16[192,1024]{1,0:T(8,128)(2,1)S(1)}, u32[]{:S(2)}, u32[]{:S(2)}) collective-permute-start(bf16[192,1024]{1,0:T(8,128)(2,1)S(1)} %bitcast.38), channel_id=1, source_target_pairs={{0,14},{2,0},{4,2},{6,4},{8,6},{10,8},{12,10},{14,12},{1,15},{3,1}... | collective-permute-start | bytes 1179656 | tf_op jit(solution)/shard_map/ppermute | solution.py:289
  41.1 16.3 %copy-start = (bf16[192,1024]{1,0:T(8,128)(2,1)}, bf16[192,1024]{1,0:T(8,128)(2,1)S(1)}, u32[]{:S(2)}) copy-start(bf16[192,1024]{1,0:T(8,128)(2,1)S(1)} %collective-permute-done.1.high_ref) | copy-start | bytes 1179652
  63.7 58.7 %collective-permute-start.11 = (bf16[448,2048]{1,0:T(8,128)(2,1)}, bf16[448,2048]{1,0:T(8,128)(2,1)}, u32[]{:S(2)}, u32[]{:S(2)}) collective-permute-start(bf16[448,2048]{1,0:T(8,128)(2,1)} %get-tuple-element.43), channel_id=1, source_target_pairs={{0,1},{1,0},{2,3},{3,2},{4,5},{5,4},{6,7},{7,6},{8,9},{9,8},{10,11... | collective-permute-start | bytes 5505032 | tf_op jit(solution)/shard_map/ppermute | solution.py:286
  67.7 54.7 %collective-permute-start.12 = (bf16[448,2048]{1,0:T(8,128)(2,1)}, bf16[448,2048]{1,0:T(8,128)(2,1)}, u32[]{:S(2)}, u32[]{:S(2)}) collective-permute-start(bf16[448,2048]{1,0:T(8,128)(2,1)} %get-tuple-element.44), channel_id=1, source_target_pairs={{0,1},{1,0},{2,3},{3,2},{4,5},{5,4},{6,7},{7,6},{8,9},{9,8},{10,11... | collective-permute-start | bytes 5505032 | tf_op jit(solution)/shard_map/ppermute | solution.py:286
  67.7 54.7 %collective-permute-start.13 = (bf16[448,2048]{1,0:T(8,128)(2,1)}, bf16[448,2048]{1,0:T(8,128)(2,1)}, u32[]{:S(2)}, u32[]{:S(2)}) collective-permute-start(bf16[448,2048]{1,0:T(8,128)(2,1)} %get-tuple-element.45), channel_id=1, source_target_pairs={{0,1},{1,0},{2,3},{3,2},{4,5},{5,4},{6,7},{7,6},{8,9},{9,8},{10,11... | collective-permute-start | bytes 5505032 | tf_op jit(solution)/shard_map/ppermute | solution.py:286
  68.2 15.1 %collective-permute-start.5 = (bf16[192,1152]{1,0:T(8,128)(2,1)S(1)}, bf16[192,1152]{1,0:T(8,128)(2,1)S(1)}, u32[]{:S(2)}, u32[]{:S(2)}) collective-permute-start(bf16[192,1152]{1,0:T(8,128)(2,1)S(1)} %get-tuple-element.33), channel_id=1, source_target_pairs={{0,14},{2,0},{4,2},{6,4},{8,6},{10,8},{12,10},{14,12},{1,15},{3,1}... | collective-permute-start | bytes 1327112 | tf_op jit(solution)/shard_map/ppermute | solution.py:289
  73.8 12.7 %collective-permute-start.6 = (bf16[192,1152]{1,0:T(8,128)(2,1)S(1)}, bf16[192,1152]{1,0:T(8,128)(2,1)S(1)}, u32[]{:S(2)}, u32[]{:S(2)}) collective-permute-start(bf16[192,1152]{1,0:T(8,128)(2,1)S(1)} %get-tuple-element.34), channel_id=1, source_target_pairs={{0,2},{2,4},{4,6},{6,8},{8,10},{10,12},{12,14},{14,0},{1,3},{3,5},... | collective-permute-start | bytes 1327112 | tf_op jit(solution)/shard_map/ppermute | solution.py:289
  107.5 3.3 %collective-permute-start.7 = (bf16[4,208,128]{2,1,0:T(8,128)(2,1)}, bf16[4,208,128]{2,1,0:T(8,128)(2,1)S(1)}, u32[]{:S(2)}, u32[]{:S(2)}) collective-permute-start(bf16[4,208,128]{2,1,0:T(8,128)(2,1)} %get-tuple-element.36), channel_id=1, source_target_pairs={{0,1},{1,0},{2,3},{3,2},{4,5},{5,4},{6,7},{7,6},{8,9},{9,8},{10,11... | collective-permute-start | bytes 638984 | tf_op jit(solution)/shard_map/ppermute | solution.py:286
  110.8 5.2 %collective-permute-start.8 = (bf16[208,128]{1,0:T(8,128)(2,1)S(1)}, bf16[208,128]{1,0:T(8,128)(2,1)S(1)}, u32[]{:S(2)}, u32[]{:S(2)}) collective-permute-start(bf16[208,128]{1,0:T(8,128)(2,1)S(1)} %get-tuple-element.38), channel_id=1, source_target_pairs={{0,4},{2,6},{4,8},{6,10},{8,12},{10,14},{12,0},{14,2},{1,5},{3,7},... | collective-permute-start | bytes 159752 | tf_op jit(solution)/shard_map/ppermute | solution.py:289
  110.9 7.0 %collective-permute-start.9 = (bf16[208,128]{1,0:T(8,128)(2,1)S(1)}, bf16[208,128]{1,0:T(8,128)(2,1)S(1)}, u32[]{:S(2)}, u32[]{:S(2)}) collective-permute-start(bf16[208,128]{1,0:T(8,128)(2,1)S(1)} %get-tuple-element.39), channel_id=1, source_target_pairs={{0,8},{2,10},{4,12},{6,14},{8,0},{10,2},{12,4},{14,6},{1,9},{3,11}... | collective-permute-start | bytes 159752 | tf_op jit(solution)/shard_map/ppermute | solution.py:289
  116.0 5.0 %collective-permute-start.10 = (bf16[208,128]{1,0:T(8,128)(2,1)S(1)}, bf16[208,128]{1,0:T(8,128)(2,1)S(1)}, u32[]{:S(2)}, u32[]{:S(2)}) collective-permute-start(bf16[208,128]{1,0:T(8,128)(2,1)S(1)} %get-tuple-element.40), channel_id=1, source_target_pairs={{0,12},{2,14},{4,0},{6,2},{8,4},{10,6},{12,8},{14,10},{1,13},{3,15... | collective-permute-start | bytes 159752 | tf_op jit(solution)/shard_map/ppermute | solution.py:289
  122.4 1.0 copy-start.1

commit v4 on v3

v4 whole, which is shorter than its diff:
```python
import functools

import jax
import jax.numpy as jnp
from jax import lax
from jax.experimental import pallas as pl
from jax.experimental.pallas import tpu as pltpu
from jax.sharding import PartitionSpec as P


EP = ("y", "x")
Z = ("zh", "zl")
LANES = 128
BF16 = jnp.bfloat16
F32 = jnp.float32
NN = (((1,), (0,)), ((), ()))
NT = (((1,), (1,)), ((), ()))
TN = (((0,), (0,)), ((), ()))
IN_VMEM = pl.BlockSpec(memory_space=pltpu.VMEM)
IN_HBM = pl.BlockSpec(memory_space=pltpu.HBM)
IN_SMEM = pl.BlockSpec(memory_space=pltpu.SMEM)


def dot(a, b, dims):
    return lax.dot_general(a, b, dims, preferred_element_type=F32)


def call(kernel, outs, *args, scratch=(), flops=0, mib=24):
    place = {"v": pltpu.VMEM, "h": pltpu.HBM, "w": pltpu.HBM}
    spec = {"v": IN_VMEM, "w": IN_VMEM, "h": IN_HBM, "s": IN_SMEM}
    moved = sum(a.size * a.dtype.itemsize for a, _ in args)
    kernel_call = pl.pallas_call(
        kernel,
        out_shape=[place[m](shape, dtype) for shape, dtype, m in outs],
        in_specs=[spec[m] for _, m in args],
        out_specs=[spec[m] for _, _, m in outs],
        scratch_shapes=list(scratch),
        cost_estimate=pl.CostEstimate(flops=flops, bytes_accessed=moved, transcendentals=0),
        compiler_params=pltpu.CompilerParams(vmem_limit_bytes=mib * 1024 * 1024),
    )
    return kernel_call(
        *(a if m == "s" else pltpu.with_memory_space_constraint(a, place[m]) for a, m in args)
    )


def slots_of(core, routes, experts, half):
    top_k, rows = routes.shape
    expert = lax.broadcasted_iota(jnp.int32, (experts, rows), 0)
    hits = [routes[k : k + 1, :] == expert for k in range(top_k)]
    named = functools.reduce(jnp.logical_or, hits)
    before = lax.broadcasted_iota(jnp.int32, (rows, rows), 0) < lax.broadcasted_iota(
        jnp.int32, (rows, rows), 1
    )
    ones = lambda mask: jnp.where(mask, 1.0, 0.0).astype(BF16)
    count = dot(ones(named), ones(before), NN)
    slots = []
    for k in range(top_k):
        place = jnp.sum(jnp.where(hits[k], count, 0.0), axis=0, keepdims=True).astype(jnp.int32)
        place = place - core * half
        inside = (place >= 0) & (place < half)
        slots.append(jnp.where(inside, routes[k : k + 1, :] * half + place, -1))
    return slots


def masks_of(slots, count):
    row = lax.broadcasted_iota(jnp.int32, (count, slots[0].shape[1]), 0)
    return [row == s for s in slots]


def pick_of(masks):
    hit = functools.reduce(jnp.logical_or, masks)
    return jnp.where(hit, 1.0, 0.0).astype(BF16)


def send_tokens(experts, half, core_ref, par_ref, routes_ref, tok_ref, out_ref, tok, sem):
    copies = [
        pltpu.make_async_copy(tok_ref.at[:, cols], tok.at[:, to], sem.at[n])
        for n, (to, cols) in enumerate(side_columns(par_ref[0], tok_ref.shape[1]))
    ]
    for copy in copies:
        copy.start()
    masks = masks_of(slots_of(core_ref[0], routes_ref[...], experts, half), experts * half)
    for copy in copies:
        copy.wait()
    out_ref[...] = dot(pick_of(masks), tok[...], NN).astype(BF16)


def keep_table(experts, half, core_ref, routes_ref, gates_ref, out_ref):
    slots = slots_of(core_ref[0], routes_ref[...], experts, half)
    top_k = len(slots)
    gates = gates_ref[...].astype(F32)
    out_ref[...] = jnp.zeros(out_ref.shape, F32)
    for k in range(top_k):
        out_ref[k : k + 1] = slots[k].astype(F32)
        out_ref[top_k + k : top_k + k + 1] = gates[k : k + 1]


def table_slots(table_ref):
    return [table_ref[k : k + 1].astype(jnp.int32) for k in range(2)]


def send_cotangents(table_ref, cot_ref, out_ref):
    masks = masks_of(table_slots(table_ref), out_ref.shape[0])
    weigh = jnp.zeros(masks[0].shape, F32)
    for k, mask in enumerate(masks):
        weigh = jnp.where(mask, table_ref[2 + k : 3 + k], weigh)
    out_ref[...] = dot(weigh.astype(BF16), cot_ref[...], NN).astype(BF16)


def side_columns(side, width):
    step = width // 8
    return [
        (slice(m * step, (m + 1) * step), pl.ds(pl.multiple_of((2 * m + side) * step, step), step))
        for m in range(4)
    ]


def pack(par_ref, gate_ref, up_ref, out_ref, buf, sem, made, out_sem):
    copies = [pltpu.make_async_copy(w, buf.at[n], sem.at[n]) for n, w in enumerate((gate_ref, up_ref))]
    for copy in copies:
        copy.start()
    done = []
    for n, copy in enumerate(copies):
        copy.wait()
        for k in range(2):
            for to, cols in side_columns(jnp.where(k == 0, par_ref[0], 1 - par_ref[0]), buf.shape[2]):
                made[n, k, :, to] = buf[n, :, cols]
            done.append(pltpu.make_async_copy(made.at[n, k], out_ref.at[n, k], out_sem.at[2 * n + k]))
            done[-1].start()
    for copy in done:
        copy.wait()


def join_rows(low_ref, high_ref, both):
    rows = low_ref.shape[0]
    both[:rows] = low_ref[...]
    both[rows:] = high_ref[...]


def forward(mine_ref, low_ref, high_ref, own_ref, other_ref, out_ref, buf, sem, both, made, out_sem):
    jobs = [(w.at[n, k], buf.at[2 * p + n, k]) for p, w in enumerate((own_ref, other_ref)) for n in range(2) for k in range(2)]
    copies = [pltpu.make_async_copy(a, b, sem.at[i]) for i, (a, b) in enumerate(jobs)]
    for copy in copies[:4]:
        copy.start()
    join_rows(low_ref, high_ref, both)
    done = []

    def product(n):
        copies[2 * n].wait()
        copies[2 * n + 1].wait()
        for copy in copies[2 * n + 4 : 2 * n + 6]:
            copy.start()
        return dot(mine_ref[...], buf[n, 0], NT) + dot(both[...], buf[n, 1], NT)

    for p in range(2):
        pre = product(2 * p)
        up = product(2 * p + 1)
        sig = jax.nn.sigmoid(pre)
        act = pre * sig
        made[p, 0] = (act * up).astype(BF16)
        made[p, 1] = (up * sig * (1.0 + pre * (1.0 - sig))).astype(BF16)
        made[p, 2] = act.astype(BF16)
        done.append(pltpu.make_async_copy(made.at[p], out_ref.at[p], out_sem.at[p]))
        done[-1].start()
    for copy in done:
        copy.wait()


def input_grad(grads, buf):
    total = dot(grads[0, 0], buf[0], NN)
    total += dot(grads[0, 1], buf[1], NN)
    total += dot(grads[1, 0], buf[2], NN)
    return total + dot(grads[1, 1], buf[3], NN)


def fetch_half(k, own_ref, other_ref, buf, sem):
    return [
        pltpu.make_async_copy(w.at[n, k], buf.at[2 * p + n], sem.at[2 * p + n])
        for p, w in enumerate((own_ref, other_ref))
        for n in range(2)
    ]


def backward(cot_ref, mid_ref, down0_ref, down1_ref, own_ref, other_ref, low_ref, high_ref, grads_ref, gate_ref, mid, mid_sem, wd, wd_sem, buf, sem, grads, out_sem):
    rows, width = cot_ref.shape
    mids = [pltpu.make_async_copy(mid_ref.at[p], mid.at[p], mid_sem.at[p]) for p in range(2)]
    downs = [
        pltpu.make_async_copy(w, wd.at[p], wd_sem.at[p]) for p, w in enumerate((down0_ref, down1_ref))
    ]
    columns = fetch_half(1, own_ref, other_ref, buf, sem)
    downs[0].start()
    mids[0].start()
    downs[1].start()
    mids[1].start()
    gate = jnp.zeros((rows, 1), F32)
    done = []
    for p in range(2):
        downs[p].wait()
        for copy in columns[2 * p : 2 * p + 2]:
            copy.start()
        back = dot(cot_ref[...], wd[p], NT)
        mids[p].wait()
        gate = gate + jnp.sum(mid[p, 0].astype(F32) * back, axis=1, keepdims=True)
        grads[p, 0] = (back * mid[p, 1].astype(F32)).astype(BF16)
        grads[p, 1] = (back * mid[p, 2].astype(F32)).astype(BF16)
        done.append(pltpu.make_async_copy(grads.at[p], grads_ref.at[p], out_sem.at[p]))
        done[-1].start()
    wide = jnp.broadcast_to(gate, (rows, LANES))
    gate_ref[...] = wide
    low_ref[:, width // 2 :] = wide[: rows // 2].astype(BF16)
    high_ref[:, width // 2 :] = wide[rows // 2 :].astype(BF16)
    for copy in columns:
        copy.wait()
    total = input_grad(grads, buf).astype(BF16)
    low_ref[:, : width // 2] = total[: rows // 2]
    high_ref[:, : width // 2] = total[rows // 2 :]
    for copy in done:
        copy.wait()


def own_half(grads_ref, gate_ref, own_ref, other_ref, out_ref, grads, grad_sem, buf, sem):
    copies = [pltpu.make_async_copy(grads_ref.at[p], grads.at[p], grad_sem.at[p]) for p in range(2)]
    copies += fetch_half(0, own_ref, other_ref, buf, sem)
    for copy in copies:
        copy.start()
    part = buf.shape[2]
    out_ref[:, part:] = gate_ref[...]
    for copy in copies:
        copy.wait()
    out_ref[:, :part] = input_grad(grads, buf)


def add_pair(own_ref, low_ref, high_ref, out_ref):
    rows = low_ref.shape[0]
    out_ref[:rows] = (own_ref[:rows] + low_ref[...].astype(F32)).astype(BF16)
    out_ref[rows:] = (own_ref[rows:] + high_ref[...].astype(F32)).astype(BF16)


def weight_grads(p, par_ref, mine_ref, low_ref, high_ref, cot_ref, mid_ref, grads_ref, *refs):
    inputs = refs[:3] if p == 0 else ()
    outs, (both, made, out_sem, left, left_sem, *got) = refs[len(inputs) :][:3], refs[len(inputs) + 3 :]
    lefts = [grads_ref.at[p, 0], grads_ref.at[p, 1], mid_ref.at[p, 0]]
    copies = [pltpu.make_async_copy(r, left.at[n], left_sem.at[n]) for n, r in enumerate(lefts)]
    received = [pltpu.make_async_copy(r, got[0].at[n], got[1].at[n]) for n, r in enumerate(inputs)]
    for copy in copies + received:
        copy.start()
    join_rows(low_ref, high_ref, both)
    done = []

    def put(n, cols, grad):
        if p == 0:
            grad += got[0][n, :, cols].astype(F32)
        made[n, :, cols] = grad.astype(BF16)

    for n in range(3):
        copies[n].wait()
        if p == 0:
            received[n].wait()
        if n < 2:
            for side, right in ((par_ref[0], mine_ref), (1 - par_ref[0], both)):
                grad = dot(left[n], right[...], TN)
                for to, cols in side_columns(side, made.shape[2]):
                    put(n, cols, grad[:, to])
        else:
            put(n, slice(None), dot(left[n], cot_ref[...], TN))
        done.append(pltpu.make_async_copy(made.at[n], outs[n], out_sem.at[n]))
        done[-1].start()
    for copy in done:
        copy.wait()


def combine(core_ref, table_ref, x_ref, keep_ref, send_ref):
    blocks, padded, _ = keep_ref.shape
    rows = table_ref.shape[1]
    width = 2 * blocks * LANES
    core = core_ref[0]
    masks = masks_of(table_slots(table_ref), x_ref.shape[0])
    grads = dot(pick_of(masks), x_ref[:, :width], TN)
    gate = x_ref[:, width : width + 1].astype(F32)
    lines = []
    for mask in masks:
        line = jnp.sum(jnp.where(mask, gate, 0.0), axis=0, keepdims=True)
        line = jnp.concatenate([line, jnp.zeros((1, 2 * LANES - rows), F32)], axis=1)
        lines += [line[:, :LANES], line[:, LANES:]]
    lines.append(jnp.zeros((padded - rows - len(lines), LANES), F32))
    tail = jnp.concatenate(lines, axis=0)
    for b in range(blocks):
        first = grads[:, 2 * b * LANES : (2 * b + 1) * LANES]
        second = grads[:, (2 * b + 1) * LANES : (2 * b + 2) * LANES]
        keep_ref[b, :rows, :] = jnp.where(core == 0, first, second)
        send_ref[b, :rows, :] = jnp.where(core == 0, second, first).astype(BF16)
        keep_ref[b, rows:, :] = tail
        send_ref[b, rows:, :] = tail.astype(BF16)


def join(keep_ref, got_ref, out_ref):
    out_ref[...] = (keep_ref[...] + got_ref[...].astype(F32)).astype(BF16)


def finish(table_ref, x_ref, tok_ref, gate_ref):
    top_k, rows = gate_ref.shape
    total = jnp.sum(x_ref[...].astype(F32), axis=0)
    tok_ref[...] = total[:rows].astype(BF16)
    for k in range(top_k):
        line = jnp.concatenate(
            [total[rows + 2 * k : rows + 2 * k + 1], total[rows + 2 * k + 1 : rows + 2 * k + 2]],
            axis=1,
        )
        gate_ref[k : k + 1, :] = line[:, :rows] / table_ref[top_k + k : top_k + k + 1, :]


def local(experts, tokens, cotangent, routing, gate_weights, gate_proj, up_proj, down_proj):
    rows, width = tokens.shape
    top_k = routing.shape[1]
    half = rows * top_k // experts
    count = experts * half
    part = width // 2
    depth = lax.axis_size(Z)
    core = lax.axis_index("c").astype(jnp.int32).reshape(1)
    parity = (lax.axis_index(Z) % 2).astype(jnp.int32).reshape(1)
    routes, gates = routing.T, gate_weights.T

    def swap(v):
        return lax.ppermute(v, "c", [(0, 1), (1, 0)])

    def shift(v, k):
        return lax.ppermute(v, Z, [(i, (i + k) % depth) for i in range(depth)])

    def exchange(v):
        return lax.all_to_all(v, EP, split_axis=0, concat_axis=0, tiled=True)

    dma = lambda n: pltpu.SemaphoreType.DMA((n,))

    ff = gate_proj.shape[2]
    down = down_proj[0]
    down_other = swap(down)
    (own,) = call(
        pack, [((2, 2, ff, part), BF16, "h")],
        (parity, "s"), (gate_proj[0].T, "h"), (up_proj[0].T, "h"),
        scratch=[
            pltpu.VMEM((2, ff, width), BF16), dma(2), pltpu.VMEM((2, 2, ff, part), BF16), dma(4),
        ],
        mib=10,
    )
    other = swap(own)
    (table,) = call(
        functools.partial(keep_table, experts, half), [((8, rows), F32, "v")],
        (core, "s"), (routes, "w"), (gates, "w"), mib=4,
    )

    (tok_out,) = call(
        functools.partial(send_tokens, experts, half),
        [((count, part), BF16, "w")],
        (core, "s"), (parity, "s"), (routes, "w"), (tokens, "h"),
        scratch=[pltpu.VMEM((rows, part), BF16), dma(4)],
        flops=2 * count * rows * part, mib=8,
    )
    mine = exchange(tok_out.reshape(experts, half, part)).reshape(count, part)
    (cot_out,) = call(
        send_cotangents, [((count, width), BF16, "w")],
        (table, "v"), (cotangent, "w"),
        flops=2 * count * rows * width, mib=8,
    )
    cot = exchange(cot_out.reshape(experts, half, width)).reshape(count, width)
    low = shift(mine[: count // 2], 1)
    high = shift(mine[count // 2 :], -1)

    packed = [(own, "h"), (other, "h")]
    mids = pltpu.VMEM((2, 3, count, ff), BF16)
    halves = [pltpu.VMEM((4, ff, part), BF16), dma(4)]
    (mid,) = call(
        forward, [((2, 3, count, ff), BF16, "h")],
        (mine, "v"), (low, "v"), (high, "v"), *packed,
        scratch=[
            pltpu.VMEM((4, 2, ff, part), BF16), dma(8), pltpu.VMEM((count, part), BF16), mids, dma(2),
        ],
        flops=8 * count * width * ff, mib=18,
    )
    message = ((count // 2, part + LANES), BF16, "v")
    to_low, to_high, grads, gate = call(
        backward,
        [message, message, ((2, 2, count, ff), BF16, "h"), ((count, LANES), F32, "v")],
        (cot, "v"), (mid, "h"), (down, "h"), (down_other, "h"), *packed,
        scratch=[
            mids, dma(2), pltpu.VMEM((2, ff, width), BF16), dma(2), *halves,
            pltpu.VMEM((2, 2, count, ff), BF16), dma(2),
        ],
        flops=8 * count * width * ff, mib=20,
    )
    from_low, from_high = shift(to_low, -1), shift(to_high, 1)
    (kept,) = call(
        own_half, [((count, part + LANES), F32, "v")],
        (grads, "h"), (gate, "v"), *packed,
        scratch=[pltpu.VMEM((2, 2, count, ff), BF16), dma(2), *halves],
        flops=4 * count * width * ff, mib=14,
    )
    (pair,) = call(
        add_pair, [((count, part + LANES), BF16, "w")], (kept, "v"), (from_low, "v"), (from_high, "v"), mib=8
    )
    returned = exchange(pair.reshape(experts, half, part + LANES)).reshape(count, part + LANES)

    pieces = [(v, "v") for v in (mine, low, high, cot)] + [(v, "h") for v in (mid, grads)]
    shard = [((ff, width), BF16, "h")] * 3
    whole = pltpu.VMEM((3, ff, width), BF16)
    room = [pltpu.VMEM((count, part), BF16), whole, dma(3), pltpu.VMEM((3, count, ff), BF16), dma(3)]
    theirs = call(
        functools.partial(weight_grads, 1), shard, (parity, "s"), *pieces,
        scratch=room, flops=6 * count * width * ff, mib=14,
    )
    received = [(swap(g), "h") for g in theirs]
    grad_gate, grad_up, grad_down = call(
        functools.partial(weight_grads, 0), shard, (parity, "s"), *pieces, *received,
        scratch=[*room, whole, dma(3)], flops=6 * count * width * ff, mib=20,
    )

    block = (depth // 2, rows + 16, LANES)
    keep, send = call(
        combine, [(block, F32, "v"), (block, BF16, "v")],
        (core, "s"), (table, "v"), (returned, "v"),
        flops=2 * count * rows * part, mib=10,
    )
    (joined,) = call(join, [(block, BF16, "v")], (keep, "v"), (swap(send), "v"), mib=4)
    summed = lax.all_to_all(joined, "zh", split_axis=0, concat_axis=0, tiled=True)
    grad_tokens, grad_gates = call(
        finish,
        [((rows, LANES), BF16, "w"), ((top_k, rows), F32, "w")],
        (table, "v"), (summed, "v"), mib=4,
    )
    return (grad_tokens, grad_gates.T, grad_gate.T[None], grad_up.T[None], grad_down[None])


def solution(mesh):
    devices = mesh.devices.reshape(4, 4, 4, 2, 2)
    inner = jax.sharding.Mesh(devices, (*EP, *Z, "c"))
    ep, tp = EP, (*Z, "c")

    def body(*args):
        return local(16, *args)

    return jax.shard_map(
        body,
        mesh=inner,
        in_specs=(
            P(ep, None),
            P(ep, None),
            P(ep, None),
            P(ep, None),
            P(ep, None, tp),
            P(ep, None, tp),
            P(ep, tp, None),
        ),
        out_specs=(
            P(ep, tp),
            P(ep, None),
            P(ep, None, tp),
            P(ep, None, tp),
            P(ep, tp, None),
        ),
        check_vma=False,
    )
```

time: 132 us -> 135 us (1.023)
  blocking collectives: 18 us -> 29.2 us
  starting transfers between devices: 35.2 us -> 30.4 us
  Pallas kernels: 46.2 us -> 43.4 us
  waiting for transfers between devices: 30.1 us -> 27.5 us
  local copies, waits for them, and re-layouts: 1.05 us -> 3.08 us
    all_to_all x0 -> x1, blocking collectives: none -> 11.3 us  [local(): lax.all_to_all(joined, 'zh', split_axis=0, concat_axis=0, tiled=True)]
    ppermute x7 -> x4, starting transfers between devices: 15.9 us -> 11.5 us  [shift(): return lax.ppermute(v, Z, [(i, (i + k) % depth) for i in range(depth)])]
    ppermute x7 -> x4, waiting for transfers between devices: 20 us -> 16 us  [shift(): return lax.ppermute(v, Z, [(i, (i + k) % depth) for i in range(depth)])]
    pallas_call x11 -> x13, Pallas kernels: 46.2 us -> 43.4 us  [call(): kernel_call(*(a if m == 's' else pltpu.with_memory_space_constraint(a, pl...]
    all_to_all x2, starting transfers between devices: 11.3 us -> 8.77 us  [exchange(): return lax.all_to_all(v, EP, split_axis=0, concat_axis=0, tiled=True)]
    ppermute x7 -> x6, starting transfers between devices: 8.05 us -> 10.1 us  [swap(): return lax.ppermute(v, 'c', [(0, 1), (1, 0)])]
    unnamed x4 -> x6, local copies, waits for them, and re-layouts: 0.99 us -> 3.02 us
    all_to_all x2, waiting for transfers between devices: 8.77 us -> 10.4 us  [exchange(): return lax.all_to_all(v, EP, split_axis=0, concat_axis=0, tiled=True)]
  transfers between devices with their start and end apart: 16 -> 12, of which waited for: 9 -> 6; matrix products, arithmetic and copies ran while one was open for 0% -> 0% of each run, Pallas kernels for 15% -> 15%
where the time goes in v4:
time: 135 us
  Pallas kernels  43.4 us (32%)
  starting transfers between devices  30.4 us (23%)
  blocking collectives  29.2 us (22%)
  waiting for transfers between devices  27.5 us (20%)
  local copies, waits for them, and re-layouts  3.08 us (2%)
    pallas_call x13, Pallas kernels, call(): kernel_call(*(a if m == 's' else pltpu.with_memory_space_constraint(a, pl...  43.4 us
    all_to_all x1, blocking collectives, exchange(): return lax.all_to_all(v, EP, split_axis=0, concat_axis=0, tiled=True)  17.9 us
    ppermute x4, waiting for transfers between devices, shift(): return lax.ppermute(v, Z, [(i, (i + k) % depth) for i in range(depth)])  16 us
    ppermute x4, starting transfers between devices, shift(): return lax.ppermute(v, Z, [(i, (i + k) % depth) for i in range(depth)])  11.5 us
    all_to_all x1, blocking collectives, local(): lax.all_to_all(joined, 'zh', split_axis=0, concat_axis=0, tiled=True)  11.3 us
    all_to_all x2, waiting for transfers between devices, exchange(): return lax.all_to_all(v, EP, split_axis=0, concat_axis=0, tiled=True)  10.4 us
    ppermute x6, starting transfers between devices, swap(): return lax.ppermute(v, 'c', [(0, 1), (1, 0)])  10.1 us
    all_to_all x2, starting transfers between devices, exchange(): return lax.all_to_all(v, EP, split_axis=0, concat_axis=0, tiled=True)  8.77 us
  transfers between devices with their start and end apart: 12, of which 6 were waited for; matrix products, arithmetic and copies ran while one was open for 0% of the time, Pallas kernels for 15%

profile of v4, /device:TPU:1, one launch (start us, length us, event | category | flops | bytes accessed | tf_op | source)
XLA Modules:
  0.0 134.5 jit_solution(16918839587134717327)
XLA Ops:
  0.6 3.5 %shard_map.113.own_ref = bf16[2,2,448,1024]{3,2,1,0:T(8,128)(2,1)} custom-call(s32[1]{0:T(128)} %bitcast.5.par_ref, bf16[448,2048]{1,0:T(8,128)(2,1)} %bitcast.39, bf16[448,2048]{1,0:T(8,128)(2,1)} %bitcast.40), custom_call_target="tpu_custom_call" | custom-call | bytes 3670020 | tf_op jit(solution)/shard_map/pallas_call | solution.py:41
  4.1 3.3 %collective-permute-start.2 = (bf16[2,2,448,1024]{3,2,1,0:T(8,128)(2,1)}, bf16[2,2,448,1024]{3,2,1,0:T(8,128)(2,1)}, u32[]{:S(2)}, u32[]{:S(2)}) collective-permute-start(bf16[2,2,448,1024]{3,2,1,0:T(8,128)(2,1)} %shard_map.113.own_ref), channel_id=1, source_target_pairs={{0,1},{1,0},{2,3},{3,2},{4,5},{5,4},{6,7},{7,6},{8,9},{9,8},{10,11... | collective-permute-start | bytes 11010056 | tf_op jit(solution)/shard_map/ppermute | solution.py:324
  7.4 3.0 %shard_map.112 = bf16[384,1024]{1,0:T(8,128)(2,1)} custom-call(s32[1]{0:T(128)} %bitcast.core_ref, s32[1]{0:T(128)} %bitcast.5.par_ref, s32[2,192]{1,0:T(2,128)} %bitcast.43, bf16[192,2048]{1,0:T(8,128)(2,1)} %tok_ref.1), custom_call_target="tpu_custom_call" | custom-call | flops 150994944 | bytes 787976 | tf_op jit(solution)/shard_map/pallas_call | solution.py:41
  10.4 5.1 %all-to-all-start.1 = ((bf16[16,24,1024]{2,1,0:T(8,128)(2,1)}), bf16[16,24,1024]{2,1,0:T(8,128)(2,1)S(1)}, u32[]{:S(2)}, u32[]{:S(2)}) async-start(bf16[16,24,1024]{2,1,0:T(8,128)(2,1)} %bitcast.36), calls=%async_computation.1 | async-start | bytes 1572864 | tf_op jit(solution)/shard_map/all_to_all | solution.py:330
  15.5 0.4 collective-permute-start.3
  15.9 0.9 shard_map.110.table_ref
  16.8 2.8 %shard_map.111 = bf16[384,2048]{1,0:T(8,128)(2,1)} custom-call(f32[8,192]{1,0:T(8,128)S(1)} %shard_map.110.table_ref, bf16[192,2048]{1,0:T(8,128)(2,1)} %cot_ref.1), custom_call_target="tpu_custom_call" | custom-call | flops 301989888 | bytes 792576 | tf_op jit(solution)/shard_map/pallas_call | solution.py:41
  19.6 9.7 %all-to-all-done.1 = bf16[16,24,1024]{2,1,0:T(8,128)(2,1)S(1)} async-done(((bf16[16,24,1024]{2,1,0:T(8,128)(2,1)}), bf16[16,24,1024]{2,1,0:T(8,128)(2,1)S(1)}, u32[]{:S(2)}, u32[]{:S(2)}) %all-to-all-start.1) | async-done | bytes 786464 | tf_op jit(solution)/shard_map/all_to_all | solution.py:330
  29.4 3.7 %all-to-all-start = ((bf16[16,24,2048]{2,1,0:T(8,128)(2,1)}), bf16[16,24,2048]{2,1,0:T(8,128)(2,1)S(1)}, u32[]{:S(2)}, u32[]{:S(2)}) async-start(bf16[16,24,2048]{2,1,0:T(8,128)(2,1)} %bitcast.34), calls=%async_computation | async-start | bytes 3145728 | tf_op jit(solution)/shard_map/all_to_all | solution.py:330
  33.1 0.1 fusion
  33.1 1.7 %collective-permute-start = (bf16[192,1024]{1,0:T(8,128)(2,1)S(1)}, bf16[192,1024]{1,0:T(8,128)(2,1)S(1)}, u32[]{:S(2)}, u32[]{:S(2)}) collective-permute-start(bf16[192,1024]{1,0:T(8,128)(2,1)S(1)} %bitcast.42), channel_id=1, source_target_pairs={{0,2},{2,4},{4,6},{6,8},{8,10},{10,12},{12,14},{14,0},{1,3},{3,5},... | collective-permute-start | bytes 1179656 | tf_op jit(solution)/shard_map/ppermute | solution.py:327
  34.8 4.2 %collective-permute-start.1 = (bf16[192,1024]{1,0:T(8,128)(2,1)S(1)}, bf16[192,1024]{1,0:T(8,128)(2,1)S(1)}, u32[]{:S(2)}, u32[]{:S(2)}) collective-permute-start(bf16[192,1024]{1,0:T(8,128)(2,1)S(1)} %bitcast.41), channel_id=1, source_target_pairs={{0,14},{2,0},{4,2},{6,4},{8,6},{10,8},{12,10},{14,12},{1,15},{3,1}... | collective-permute-start | bytes 1179656 | tf_op jit(solution)/shard_map/ppermute | solution.py:327
  39.1 7.8 %collective-permute-done.low_ref = bf16[192,1024]{1,0:T(8,128)(2,1)S(1)} collective-permute-done((bf16[192,1024]{1,0:T(8,128)(2,1)S(1)}, bf16[192,1024]{1,0:T(8,128)(2,1)S(1)}, u32[]{:S(2)}, u32[]{:S(2)}) %collective-permute-start) | collective-permute-done | bytes 393248 | tf_op jit(solution)/shard_map/ppermute | solution.py:327
  46.8 0.0 collective-permute-done.1.high_ref
  46.8 0.0 collective-permute-done.2.other_ref
  46.8 6.9 %shard_map.114.mid_ref = bf16[2,3,384,448]{3,2,1,0:T(8,128)(2,1)} custom-call(bf16[384,1024]{1,0:T(8,128)(2,1)S(1)} %bitcast.30, bf16[192,1024]{1,0:T(8,128)(2,1)S(1)} %collective-permute-done.low_ref, bf16[192,1024]{1,0:T(8,128)(2,1)S(1)} %collective-permute-done.1.high_ref, bf16[2,2,448,1024]{3,2,1,0:T(8,128)(2,1)} %shard_map.113.own_ref, ...), custom_call_target="tpu_custom_call" | custom-call | flops 2818572288 | bytes 8912896 | tf_op jit(solution)/shard_map/pallas_call | solution.py:41
  53.8 0.6 all-to-all-done
  54.4 0.0 collective-permute-done.3.down1_ref
  54.4 7.0 %shard_map.115 = (bf16[192,1152]{1,0:T(8,128)(2,1)S(1)}, bf16[192,1152]{1,0:T(8,128)(2,1)S(1)}, bf16[2,2,384,448]{3,2,1,0:T(8,128)(2,1)}, f32[384,128]{1,0:T(8,128)S(1)}) custom-call(bf16[384,2048]{1,0:T(8,128)(2,1)S(1)} %bitcast.27, bf16[2,3,384,448]{3,2,1,0:T(8,128)(2,1)} %shard_map.114.mid_ref, bf16[448,2048]{1,0:T(8,128)(2,1)} %bitcast.38, ...), custom_call_target="tpu_custom_call" | custom-call | flops 2818572288 | bytes 14647296 | tf_op jit(solution)/shard_map/pallas_call | solution.py:41
  61.4 6.0 %shard_map.121 = (bf16[448,2048]{1,0:T(8,128)(2,1)}, bf16[448,2048]{1,0:T(8,128)(2,1)}, bf16[448,2048]{1,0:T(8,128)(2,1)}) custom-call(s32[1]{0:T(128)} %bitcast.5.par_ref, bf16[384,1024]{1,0:T(8,128)(2,1)S(1)} %bitcast.31, bf16[192,1024]{1,0:T(8,128)(2,1)S(1)} %collective-permute-done.low_ref, bf16[192,1024]{1,0:T(8,128)(2,1)S(1)} %collective-permute-done.1.high_ref, ...), custom_call_target="tpu_custom_call" | custom-call | flops 2113929216 | bytes 6586372 | tf_op jit(solution)/shard_map/pallas_call | solution.py:41
  67.4 3.8 %collective-permute-start.7 = (bf16[448,2048]{1,0:T(8,128)(2,1)}, bf16[448,2048]{1,0:T(8,128)(2,1)S(1)}, u32[]{:S(2)}, u32[]{:S(2)}) collective-permute-start(bf16[448,2048]{1,0:T(8,128)(2,1)} %get-tuple-element.27), channel_id=1, source_target_pairs={{0,1},{1,0},{2,3},{3,2},{4,5},{5,4},{6,7},{7,6},{8,9},{9,8},{10,11... | collective-permute-start | bytes 5505032 | tf_op jit(solution)/shard_map/ppermute | solution.py:324
  71.3 0.1 collective-permute-start.8
  71.4 0.4 collective-permute-start.9
  71.8 5.6 %collective-permute-start.4 = (bf16[192,1152]{1,0:T(8,128)(2,1)S(1)}, bf16[192,1152]{1,0:T(8,128)(2,1)S(1)}, u32[]{:S(2)}, u32[]{:S(2)}) collective-permute-start(bf16[192,1152]{1,0:T(8,128)(2,1)S(1)} %get-tuple-element.21), channel_id=1, source_target_pairs={{0,14},{2,0},{4,2},{6,4},{8,6},{10,8},{12,10},{14,12},{1,15},{3,1}... | collective-permute-start | bytes 1327112 | tf_op jit(solution)/shard_map/ppermute | solution.py:327
  77.4 0.0 collective-permute-start.5
  77.4 4.3 %shard_map.116.own_ref = f32[384,1152]{1,0:T(8,128)S(1)} custom-call(bf16[2,2,384,448]{3,2,1,0:T(8,128)(2,1)} %get-tuple-element.19.grads_ref, f32[384,128]{1,0:T(8,128)S(1)} %get-tuple-element.20.gate_ref, bf16[2,2,448,1024]{3,2,1,0:T(8,128)(2,1)} %shard_map.113.own_ref, bf16[2,2,448,1024]{3,2,1,0:T(8,128)(2,1)} %collective-permute-done.2.other_ref), custom_call_target="tpu_custom_call" | custom-call | flops 1409286144 | bytes 8912896 | tf_op jit(solution)/shard_map/pallas_call | solution.py:41
  81.7 5.1 %collective-permute-done.4.low_ref = bf16[192,1152]{1,0:T(8,128)(2,1)S(1)} collective-permute-done((bf16[192,1152]{1,0:T(8,128)(2,1)S(1)}, bf16[192,1152]{1,0:T(8,128)(2,1)S(1)}, u32[]{:S(2)}, u32[]{:S(2)}) %collective-permute-start.4) | collective-permute-done | bytes 442400 | tf_op jit(solution)/shard_map/ppermute | solution.py:327
  86.8 3.1 %collective-permute-done.5.high_ref = bf16[192,1152]{1,0:T(8,128)(2,1)S(1)} collective-permute-done((bf16[192,1152]{1,0:T(8,128)(2,1)S(1)}, bf16[192,1152]{1,0:T(8,128)(2,1)S(1)}, u32[]{:S(2)}, u32[]{:S(2)}) %collective-permute-start.5) | collective-permute-done | bytes 442400 | tf_op jit(solution)/shard_map/ppermute | solution.py:327
  89.9 1.1 shard_map.117
  91.0 17.9 %all_to_all.20 = bf16[16,24,1152]{2,1,0:T(8,128)(2,1)S(1)} all-to-all(bf16[16,24,1152]{2,1,0:T(8,128)(2,1)} %bitcast.35), channel_id=1, replica_groups=mesh['y'=4,'x'=4,'zh'=4,'zl'=2,'c'=2] {'y','x'}, dimensions={0} | all-to-all | bytes 1769472 | tf_op jit(solution)/shard_map/all_to_all | solution.py:330
  108.9 0.4 shard_map.118
  109.4 2.1 %collective-permute-start.6 = (bf16[4,208,128]{2,1,0:T(8,128)(2,1)S(1)}, bf16[4,208,128]{2,1,0:T(8,128)(2,1)S(1)}, u32[]{:S(2)}, u32[]{:S(2)}) collective-permute-start(bf16[4,208,128]{2,1,0:T(8,128)(2,1)S(1)} %get-tuple-element.24), channel_id=1, source_target_pairs={{0,1},{1,0},{2,3},{3,2},{4,5},{5,4},{6,7},{7,6},{8,9},{9,8},{10,11... | collective-permute-start | bytes 638984 | tf_op jit(solution)/shard_map/ppermute | solution.py:324
  111.5 1.1 collective-permute-done.6.got_ref
  112.6 11.3 %all_to_all.21.x_ref = bf16[4,208,128]{2,1,0:T(8,128)(2,1)S(1)} all-to-all(bf16[4,208,128]{2,1,0:T(8,128)(2,1)S(1)} %shard_map.119), channel_id=1, replica_groups=mesh['y'=4,'x'=4,'zh'=4,'zl'=2,'c'=2] {'zh'}, dimensions={0} | all-to-all | bytes 425984 | tf_op jit(solution)/shard_map/all_to_all | solution.py:423
  123.9 0.7 shard_map.120
  124.6 0.0 collective-permute-done.7.refs_0_
  124.6 0.0 copy-start
  124.6 0.0 collective-permute-done.8.refs_1_
  124.6 0.0 copy-start.1
  124.6 0.0 collective-permute-done.9.refs_2_
  124.6 1.2 copy-done
  125.9 0.5 copy-done.1
  126.4 0.0 copy-start.2
  126.4 1.3 copy-done.2
  127.6 6.7 %shard_map.122 = (bf16[448,2048]{1,0:T(8,128)(2,1)}, bf16[448,2048]{1,0:T(8,128)(2,1)}, bf16[448,2048]{1,0:T(8,128)(2,1)}) custom-call(s32[1]{0:T(128)} %bitcast.5.par_ref, bf16[384,1024]{1,0:T(8,128)(2,1)S(1)} %bitcast.32, bf16[192,1024]{1,0:T(8,128)(2,1)S(1)} %collective-permute-done.low_ref, bf16[192,1024]{1,0:T(8,128)(2,1)S(1)} %collective-permute-done.1.high_ref, ...), custom_call_target="tpu_custom_call" | custom-call | flops 2113929216 | bytes 12091396 | tf_op jit(solution)/shard_map/pallas_call | solution.py:41
  (1 shorter events, 0.0 us)
Async XLA Ops:
  4.1 42.7 %collective-permute-start.2 = (bf16[2,2,448,1024]{3,2,1,0:T(8,128)(2,1)}, bf16[2,2,448,1024]{3,2,1,0:T(8,128)(2,1)}, u32[]{:S(2)}, u32[]{:S(2)}) collective-permute-start(bf16[2,2,448,1024]{3,2,1,0:T(8,128)(2,1)} %shard_map.113.own_ref), channel_id=1, source_target_pairs={{0,1},{1,0},{2,3},{3,2},{4,5},{5,4},{6,7},{7,6},{8,9},{9,8},{10,11... | collective-permute-start | bytes 11010056 | tf_op jit(solution)/shard_map/ppermute | solution.py:324
  10.4 18.9 %all-to-all-start.1 = ((bf16[16,24,1024]{2,1,0:T(8,128)(2,1)}), bf16[16,24,1024]{2,1,0:T(8,128)(2,1)S(1)}, u32[]{:S(2)}, u32[]{:S(2)}) async-start(bf16[16,24,1024]{2,1,0:T(8,128)(2,1)} %bitcast.36), calls=%async_computation.1 | async-start | bytes 1572864 | tf_op jit(solution)/shard_map/all_to_all | solution.py:330
  15.5 38.9 %collective-permute-start.3 = (bf16[448,2048]{1,0:T(8,128)(2,1)}, bf16[448,2048]{1,0:T(8,128)(2,1)}, u32[]{:S(2)}, u32[]{:S(2)}) collective-permute-start(bf16[448,2048]{1,0:T(8,128)(2,1)} %bitcast.37), channel_id=1, source_target_pairs={{0,1},{1,0},{2,3},{3,2},{4,5},{5,4},{6,7},{7,6},{8,9},{9,8},{10,11... | collective-permute-start | bytes 5505032 | tf_op jit(solution)/shard_map/ppermute | solution.py:324
  29.4 25.0 %all-to-all-start = ((bf16[16,24,2048]{2,1,0:T(8,128)(2,1)}), bf16[16,24,2048]{2,1,0:T(8,128)(2,1)S(1)}, u32[]{:S(2)}, u32[]{:S(2)}) async-start(bf16[16,24,2048]{2,1,0:T(8,128)(2,1)} %bitcast.34), calls=%async_computation | async-start | bytes 3145728 | tf_op jit(solution)/shard_map/all_to_all | solution.py:330
  33.1 13.7 %collective-permute-start = (bf16[192,1024]{1,0:T(8,128)(2,1)S(1)}, bf16[192,1024]{1,0:T(8,128)(2,1)S(1)}, u32[]{:S(2)}, u32[]{:S(2)}) collective-permute-start(bf16[192,1024]{1,0:T(8,128)(2,1)S(1)} %bitcast.42), channel_id=1, source_target_pairs={{0,2},{2,4},{4,6},{6,8},{8,10},{10,12},{12,14},{14,0},{1,3},{3,5},... | collective-permute-start | bytes 1179656 | tf_op jit(solution)/shard_map/ppermute | solution.py:327
  34.8 12.0 %collective-permute-start.1 = (bf16[192,1024]{1,0:T(8,128)(2,1)S(1)}, bf16[192,1024]{1,0:T(8,128)(2,1)S(1)}, u32[]{:S(2)}, u32[]{:S(2)}) collective-permute-start(bf16[192,1024]{1,0:T(8,128)(2,1)S(1)} %bitcast.41), channel_id=1, source_target_pairs={{0,14},{2,0},{4,2},{6,4},{8,6},{10,8},{12,10},{14,12},{1,15},{3,1}... | collective-permute-start | bytes 1179656 | tf_op jit(solution)/shard_map/ppermute | solution.py:327
  67.4 57.1 %collective-permute-start.7 = (bf16[448,2048]{1,0:T(8,128)(2,1)}, bf16[448,2048]{1,0:T(8,128)(2,1)S(1)}, u32[]{:S(2)}, u32[]{:S(2)}) collective-permute-start(bf16[448,2048]{1,0:T(8,128)(2,1)} %get-tuple-element.27), channel_id=1, source_target_pairs={{0,1},{1,0},{2,3},{3,2},{4,5},{5,4},{6,7},{7,6},{8,9},{9,8},{10,11... | collective-permute-start | bytes 5505032 | tf_op jit(solution)/shard_map/ppermute | solution.py:324
  71.3 53.3 %collective-permute-start.8 = (bf16[448,2048]{1,0:T(8,128)(2,1)}, bf16[448,2048]{1,0:T(8,128)(2,1)S(1)}, u32[]{:S(2)}, u32[]{:S(2)}) collective-permute-start(bf16[448,2048]{1,0:T(8,128)(2,1)} %get-tuple-element.28), channel_id=1, source_target_pairs={{0,1},{1,0},{2,3},{3,2},{4,5},{5,4},{6,7},{7,6},{8,9},{9,8},{10,11... | collective-permute-start | bytes 5505032 | tf_op jit(solution)/shard_map/ppermute | solution.py:324
  71.4 53.2 %collective-permute-start.9 = (bf16[448,2048]{1,0:T(8,128)(2,1)}, bf16[448,2048]{1,0:T(8,128)(2,1)S(1)}, u32[]{:S(2)}, u32[]{:S(2)}) collective-permute-start(bf16[448,2048]{1,0:T(8,128)(2,1)} %get-tuple-element.29), channel_id=1, source_target_pairs={{0,1},{1,0},{2,3},{3,2},{4,5},{5,4},{6,7},{7,6},{8,9},{9,8},{10,11... | collective-permute-start | bytes 5505032 | tf_op jit(solution)/shard_map/ppermute | solution.py:324
  71.8 15.0 %collective-permute-start.4 = (bf16[192,1152]{1,0:T(8,128)(2,1)S(1)}, bf16[192,1152]{1,0:T(8,128)(2,1)S(1)}, u32[]{:S(2)}, u32[]{:S(2)}) collective-permute-start(bf16[192,1152]{1,0:T(8,128)(2,1)S(1)} %get-tuple-element.21), channel_id=1, source_target_pairs={{0,14},{2,0},{4,2},{6,4},{8,6},{10,8},{12,10},{14,12},{1,15},{3,1}... | collective-permute-start | bytes 1327112 | tf_op jit(solution)/shard_map/ppermute | solution.py:327
  77.4 12.6 %collective-permute-start.5 = (bf16[192,1152]{1,0:T(8,128)(2,1)S(1)}, bf16[192,1152]{1,0:T(8,128)(2,1)S(1)}, u32[]{:S(2)}, u32[]{:S(2)}) collective-permute-start(bf16[192,1152]{1,0:T(8,128)(2,1)S(1)} %get-tuple-element.22), channel_id=1, source_target_pairs={{0,2},{2,4},{4,6},{6,8},{8,10},{10,12},{12,14},{14,0},{1,3},{3,5},... | collective-permute-start | bytes 1327112 | tf_op jit(solution)/shard_map/ppermute | solution.py:327
  109.4 3.2 %collective-permute-start.6 = (bf16[4,208,128]{2,1,0:T(8,128)(2,1)S(1)}, bf16[4,208,128]{2,1,0:T(8,128)(2,1)S(1)}, u32[]{:S(2)}, u32[]{:S(2)}) collective-permute-start(bf16[4,208,128]{2,1,0:T(8,128)(2,1)S(1)} %get-tuple-element.24), channel_id=1, source_target_pairs={{0,1},{1,0},{2,3},{3,2},{4,5},{5,4},{6,7},{7,6},{8,9},{9,8},{10,11... | collective-permute-start | bytes 638984 | tf_op jit(solution)/shard_map/ppermute | solution.py:324
  124.6 1.3 copy-start
  124.6 1.8 %copy-start.1 = (bf16[448,2048]{1,0:T(8,128)(2,1)}, bf16[448,2048]{1,0:T(8,128)(2,1)S(1)}, u32[]{:S(2)}) copy-start(bf16[448,2048]{1,0:T(8,128)(2,1)S(1)} %collective-permute-done.8.refs_1_) | copy-start | bytes 5505028
  126.4 1.3 copy-start.2

commit v5 on v4

--- a/solution.py
+++ b/solution.py
@@ -131,18 +131,25 @@
         copy.wait()
 
 
-def join_rows(low_ref, high_ref, both):
+def fetch_rows(low_ref, high_ref, both, sem):
     rows = low_ref.shape[0]
-    both[:rows] = low_ref[...]
-    both[rows:] = high_ref[...]
-
-
-def forward(mine_ref, low_ref, high_ref, own_ref, other_ref, out_ref, buf, sem, both, made, out_sem):
+    copies = [
+        pltpu.make_async_copy(low_ref, both.at[:rows], sem.at[0]),
+        pltpu.make_async_copy(high_ref, both.at[rows:], sem.at[1]),
+    ]
+    for copy in copies:
+        copy.start()
+    return copies
+
+
+def forward(mine_ref, low_ref, high_ref, own_ref, other_ref, out_ref, buf, sem, both, half_sem, made, out_sem):
     jobs = [(w.at[n, k], buf.at[2 * p + n, k]) for p, w in enumerate((own_ref, other_ref)) for n in range(2) for k in range(2)]
     copies = [pltpu.make_async_copy(a, b, sem.at[i]) for i, (a, b) in enumerate(jobs)]
-    for copy in copies[:4]:
-        copy.start()
-    join_rows(low_ref, high_ref, both)
+    for copy in copies[:2]:
+        copy.start()
+    halves = fetch_rows(low_ref, high_ref, both, half_sem)
+    for copy in copies[2:4]:
+        copy.start()
     done = []
 
     def product(n):
@@ -150,7 +157,11 @@
         copies[2 * n + 1].wait()
         for copy in copies[2 * n + 4 : 2 * n + 6]:
             copy.start()
-        return dot(mine_ref[...], buf[n, 0], NT) + dot(both[...], buf[n, 1], NT)
+        total = dot(mine_ref[...], buf[n, 0], NT)
+        if n == 0:
+            for copy in halves:
+                copy.wait()
+        return total + dot(both[...], buf[n, 1], NT)
 
     for p in range(2):
         pre = product(2 * p)
@@ -238,13 +249,13 @@
 
 def weight_grads(p, par_ref, mine_ref, low_ref, high_ref, cot_ref, mid_ref, grads_ref, *refs):
     inputs = refs[:3] if p == 0 else ()
-    outs, (both, made, out_sem, left, left_sem, *got) = refs[len(inputs) :][:3], refs[len(inputs) + 3 :]
+    outs, (both, half_sem, made, out_sem, left, left_sem, *got) = refs[len(inputs) :][:3], refs[len(inputs) + 3 :]
     lefts = [grads_ref.at[p, 0], grads_ref.at[p, 1], mid_ref.at[p, 0]]
     copies = [pltpu.make_async_copy(r, left.at[n], left_sem.at[n]) for n, r in enumerate(lefts)]
     received = [pltpu.make_async_copy(r, got[0].at[n], got[1].at[n]) for n, r in enumerate(inputs)]
+    halves = fetch_rows(low_ref, high_ref, both, half_sem)
     for copy in copies + received:
         copy.start()
-    join_rows(low_ref, high_ref, both)
     done = []
 
     def put(n, cols, grad):
@@ -256,6 +267,9 @@
         copies[n].wait()
         if p == 0:
             received[n].wait()
+        if n == 0:
+            for copy in halves:
+                copy.wait()
         if n < 2:
             for side, right in ((par_ref[0], mine_ref), (1 - par_ref[0], both)):
                 grad = dot(left[n], right[...], TN)
@@ -293,13 +307,16 @@
         send_ref[b, rows:, :] = tail.astype(BF16)
 
 
-def join(keep_ref, got_ref, out_ref):
-    out_ref[...] = (keep_ref[...] + got_ref[...].astype(F32)).astype(BF16)
-
-
-def finish(table_ref, x_ref, tok_ref, gate_ref):
+def join(turn_ref, keep_ref, got_ref, *out_refs):
+    for k, out_ref in enumerate(out_refs):
+        block = lax.rem(turn_ref[0] + k, len(out_refs))
+        out_ref[...] = (keep_ref[block] + got_ref[block].astype(F32)).astype(BF16)
+
+
+def finish(table_ref, *refs):
+    parts, (tok_ref, gate_ref) = refs[:-2], refs[-2:]
     top_k, rows = gate_ref.shape
-    total = jnp.sum(x_ref[...].astype(F32), axis=0)
+    total = functools.reduce(jnp.add, [x[...].astype(F32) for x in parts])
     tok_ref[...] = total[:rows].astype(BF16)
     for k in range(top_k):
         line = jnp.concatenate(
@@ -370,9 +387,9 @@
     halves = [pltpu.VMEM((4, ff, part), BF16), dma(4)]
     (mid,) = call(
         forward, [((2, 3, count, ff), BF16, "h")],
-        (mine, "v"), (low, "v"), (high, "v"), *packed,
+        (mine, "v"), (low, "h"), (high, "h"), *packed,
         scratch=[
-            pltpu.VMEM((4, 2, ff, part), BF16), dma(8), pltpu.VMEM((count, part), BF16), mids, dma(2),
+            pltpu.VMEM((4, 2, ff, part), BF16), dma(8), pltpu.VMEM((count, part), BF16), dma(2), mids, dma(2),
         ],
         flops=8 * count * width * ff, mib=18,
     )
@@ -399,10 +416,10 @@
     )
     returned = exchange(pair.reshape(experts, half, part + LANES)).reshape(count, part + LANES)
 
-    pieces = [(v, "v") for v in (mine, low, high, cot)] + [(v, "h") for v in (mid, grads)]
+    pieces = [(mine, "v"), (low, "h"), (high, "h"), (cot, "v"), (mid, "h"), (grads, "h")]
     shard = [((ff, width), BF16, "h")] * 3
     whole = pltpu.VMEM((3, ff, width), BF16)
-    room = [pltpu.VMEM((count, part), BF16), whole, dma(3), pltpu.VMEM((3, count, ff), BF16), dma(3)]
+    room = [pltpu.VMEM((count, part), BF16), dma(2), whole, dma(3), pltpu.VMEM((3, count, ff), BF16), dma(3)]
     theirs = call(
         functools.partial(weight_grads, 1), shard, (parity, "s"), *pieces,
         scratch=room, flops=6 * count * width * ff, mib=14,
@@ -419,12 +436,17 @@
         (core, "s"), (table, "v"), (returned, "v"),
         flops=2 * count * rows * part, mib=10,
     )
-    (joined,) = call(join, [(block, BF16, "v")], (keep, "v"), (swap(send), "v"), mib=4)
-    summed = lax.all_to_all(joined, "zh", split_axis=0, concat_axis=0, tiled=True)
+    turn = lax.axis_index("zh").astype(jnp.int32).reshape(1)
+    steps = depth // 2
+    parts = call(
+        join, [(block[1:], BF16, "v")] * steps,
+        (turn, "s"), (keep, "v"), (swap(send), "v"), mib=4,
+    )
+    sums = [parts[0]] + [shift(parts[k], 2 * k) for k in range(1, steps)]
     grad_tokens, grad_gates = call(
         finish,
         [((rows, LANES), BF16, "w"), ((top_k, rows), F32, "w")],
-        (table, "v"), (summed, "v"), mib=4,
+        (table, "v"), *((v, "v") for v in sums), mib=4,
     )
     return (grad_tokens, grad_gates.T, grad_gate.T[None], grad_up.T[None], grad_down[None])
 

time: 135 us -> 135 us (level)
  blocking collectives: 29.2 us -> 17.9 us
  waiting for transfers between devices: 27.5 us -> 32.4 us
  starting transfers between devices: 30.4 us -> 34.4 us
  Pallas kernels: 43.4 us -> 45.1 us
    all_to_all x1 -> x0, blocking collectives: 11.3 us -> none  [local(): lax.all_to_all(joined, 'zh', split_axis=0, concat_axis=0, tiled=True)]
    ppermute x4 -> x7, waiting for transfers between devices: 16 us -> 21.5 us  [shift(): return lax.ppermute(v, Z, [(i, (i + k) % depth) for i in range(depth)])]
    ppermute x4 -> x7, starting transfers between devices: 11.5 us -> 16.3 us  [shift(): return lax.ppermute(v, Z, [(i, (i + k) % depth) for i in range(depth)])]
    pallas_call x13, Pallas kernels: 43.4 us -> 45.1 us  [call(): kernel_call(*(a if m == 's' else pltpu.with_memory_space_constraint(a, pl...]
    unnamed x6 -> x10, local copies, waits for them, and re-layouts: 3.02 us -> 3.87 us
  transfers between devices with their start and end apart: 12 -> 15, of which waited for: 6 -> 8; matrix products, arithmetic and copies ran while one was open for 0% -> 0% of each run, Pallas kernels for 15% -> 15%
where the time goes in v5:
time: 135 us
  Pallas kernels  45.1 us (33%)
  starting transfers between devices  34.4 us (25%)
  waiting for transfers between devices  32.4 us (24%)
  blocking collectives  17.9 us (13%)
  local copies, waits for them, and re-layouts  3.93 us (3%)
    pallas_call x13, Pallas kernels, call(): kernel_call(*(a if m == 's' else pltpu.with_memory_space_constraint(a, pl...  45.1 us
    ppermute x7, waiting for transfers between devices, shift(): return lax.ppermute(v, Z, [(i, (i + k) % depth) for i in range(depth)])  21.5 us
    all_to_all x1, blocking collectives, exchange(): return lax.all_to_all(v, EP, split_axis=0, concat_axis=0, tiled=True)  17.9 us
    ppermute x7, starting transfers between devices, shift(): return lax.ppermute(v, Z, [(i, (i + k) % depth) for i in range(depth)])  16.3 us
    all_to_all x2, waiting for transfers between devices, exchange(): return lax.all_to_all(v, EP, split_axis=0, concat_axis=0, tiled=True)  9.75 us
    ppermute x6, starting transfers between devices, swap(): return lax.ppermute(v, 'c', [(0, 1), (1, 0)])  9.34 us
    all_to_all x2, starting transfers between devices, exchange(): return lax.all_to_all(v, EP, split_axis=0, concat_axis=0, tiled=True)  8.77 us
    unnamed x10, local copies, waits for them, and re-layouts  3.87 us
  transfers between devices with their start and end apart: 15, of which 8 were waited for; matrix products, arithmetic and copies ran while one was open for 0% of the time, Pallas kernels for 15%

profile of v5, /device:TPU:1, one launch (start us, length us, event | category | flops | bytes accessed | tf_op | source)
XLA Modules:
  0.0 134.7 jit_solution(16518091170767044712)
XLA Ops:
  0.6 3.5 %shard_map.113.own_ref = bf16[2,2,448,1024]{3,2,1,0:T(8,128)(2,1)} custom-call(s32[1]{0:T(128)} %bitcast.6.par_ref, bf16[448,2048]{1,0:T(8,128)(2,1)} %bitcast.38, bf16[448,2048]{1,0:T(8,128)(2,1)} %bitcast.39), custom_call_target="tpu_custom_call" | custom-call | bytes 3670020 | tf_op jit(solution)/shard_map/pallas_call | solution.py:41
  4.1 3.3 %collective-permute-start.2 = (bf16[2,2,448,1024]{3,2,1,0:T(8,128)(2,1)}, bf16[2,2,448,1024]{3,2,1,0:T(8,128)(2,1)}, u32[]{:S(2)}, u32[]{:S(2)}) collective-permute-start(bf16[2,2,448,1024]{3,2,1,0:T(8,128)(2,1)} %shard_map.113.own_ref), channel_id=1, source_target_pairs={{0,1},{1,0},{2,3},{3,2},{4,5},{5,4},{6,7},{7,6},{8,9},{9,8},{10,11... | collective-permute-start | bytes 11010056 | tf_op jit(solution)/shard_map/ppermute | solution.py:341
  7.4 3.0 %shard_map.112 = bf16[384,1024]{1,0:T(8,128)(2,1)} custom-call(s32[1]{0:T(128)} %bitcast.core_ref, s32[1]{0:T(128)} %bitcast.6.par_ref, s32[2,192]{1,0:T(2,128)} %bitcast.42, bf16[192,2048]{1,0:T(8,128)(2,1)} %tok_ref.1), custom_call_target="tpu_custom_call" | custom-call | flops 150994944 | bytes 787976 | tf_op jit(solution)/shard_map/pallas_call | solution.py:41
  10.4 5.1 %all-to-all-start.1 = ((bf16[16,24,1024]{2,1,0:T(8,128)(2,1)}), bf16[16,24,1024]{2,1,0:T(8,128)(2,1)S(1)}, u32[]{:S(2)}, u32[]{:S(2)}) async-start(bf16[16,24,1024]{2,1,0:T(8,128)(2,1)} %bitcast.37), calls=%async_computation.1 | async-start | bytes 1572864 | tf_op jit(solution)/shard_map/all_to_all | solution.py:347
  15.5 0.4 collective-permute-start.3
  15.9 0.9 shard_map.110.table_ref
  16.8 2.8 %shard_map.111 = bf16[384,2048]{1,0:T(8,128)(2,1)} custom-call(f32[8,192]{1,0:T(8,128)S(1)} %shard_map.110.table_ref, bf16[192,2048]{1,0:T(8,128)(2,1)} %cot_ref.1), custom_call_target="tpu_custom_call" | custom-call | flops 301989888 | bytes 792576 | tf_op jit(solution)/shard_map/pallas_call | solution.py:41
  19.6 9.7 %all-to-all-done.1 = bf16[16,24,1024]{2,1,0:T(8,128)(2,1)S(1)} async-done(((bf16[16,24,1024]{2,1,0:T(8,128)(2,1)}), bf16[16,24,1024]{2,1,0:T(8,128)(2,1)S(1)}, u32[]{:S(2)}, u32[]{:S(2)}) %all-to-all-start.1) | async-done | bytes 786464 | tf_op jit(solution)/shard_map/all_to_all | solution.py:347
  29.4 3.7 %all-to-all-start = ((bf16[16,24,2048]{2,1,0:T(8,128)(2,1)}), bf16[16,24,2048]{2,1,0:T(8,128)(2,1)S(1)}, u32[]{:S(2)}, u32[]{:S(2)}) async-start(bf16[16,24,2048]{2,1,0:T(8,128)(2,1)} %bitcast.35), calls=%async_computation | async-start | bytes 3145728 | tf_op jit(solution)/shard_map/all_to_all | solution.py:347
  33.1 0.1 fusion
  33.1 1.7 %collective-permute-start = (bf16[192,1024]{1,0:T(8,128)(2,1)S(1)}, bf16[192,1024]{1,0:T(8,128)(2,1)S(1)}, u32[]{:S(2)}, u32[]{:S(2)}) collective-permute-start(bf16[192,1024]{1,0:T(8,128)(2,1)S(1)} %bitcast.41), channel_id=1, source_target_pairs={{0,2},{2,4},{4,6},{6,8},{8,10},{10,12},{12,14},{14,0},{1,3},{3,5},... | collective-permute-start | bytes 1179656 | tf_op jit(solution)/shard_map/ppermute | solution.py:344
  34.8 4.2 %collective-permute-start.1 = (bf16[192,1024]{1,0:T(8,128)(2,1)S(1)}, bf16[192,1024]{1,0:T(8,128)(2,1)S(1)}, u32[]{:S(2)}, u32[]{:S(2)}) collective-permute-start(bf16[192,1024]{1,0:T(8,128)(2,1)S(1)} %bitcast.40), channel_id=1, source_target_pairs={{0,14},{2,0},{4,2},{6,4},{8,6},{10,8},{12,10},{14,12},{1,15},{3,1}... | collective-permute-start | bytes 1179656 | tf_op jit(solution)/shard_map/ppermute | solution.py:344
  39.1 7.8 %collective-permute-done.low_ref = bf16[192,1024]{1,0:T(8,128)(2,1)S(1)} collective-permute-done((bf16[192,1024]{1,0:T(8,128)(2,1)S(1)}, bf16[192,1024]{1,0:T(8,128)(2,1)S(1)}, u32[]{:S(2)}, u32[]{:S(2)}) %collective-permute-start) | collective-permute-done | bytes 393248 | tf_op jit(solution)/shard_map/ppermute | solution.py:344
  46.8 0.0 collective-permute-done.1.high_ref
  46.8 0.0 collective-permute-done.2.other_ref
  46.9 0.7 copy-done.3
  47.6 0.1 copy-done.4
  47.7 7.4 %shard_map.114.mid_ref = bf16[2,3,384,448]{3,2,1,0:T(8,128)(2,1)} custom-call(bf16[384,1024]{1,0:T(8,128)(2,1)S(1)} %bitcast.31, bf16[192,1024]{1,0:T(8,128)(2,1)} %copy-done.3, bf16[192,1024]{1,0:T(8,128)(2,1)} %copy-done.4, bf16[2,2,448,1024]{3,2,1,0:T(8,128)(2,1)} %shard_map.113.own_ref, bf16[2,2,448,1024]{3,2,1,0:T(8,128)(2,1)} %collective-permute-done.2.other_ref), custom_call_target="tpu_custom_call" | custom-call | flops 2818572288 | bytes 8912896 | tf_op jit(solution)/shard_map/pallas_call | solution.py:41
  55.1 0.0 all-to-all-done
  55.1 7.0 %shard_map.115 = (bf16[192,1152]{1,0:T(8,128)(2,1)S(1)}, bf16[192,1152]{1,0:T(8,128)(2,1)S(1)}, bf16[2,2,384,448]{3,2,1,0:T(8,128)(2,1)}, f32[384,128]{1,0:T(8,128)S(1)}) custom-call(bf16[384,2048]{1,0:T(8,128)(2,1)S(1)} %bitcast.28, bf16[2,3,384,448]{3,2,1,0:T(8,128)(2,1)} %shard_map.114.mid_ref, bf16[448,2048]{1,0:T(8,128)(2,1)} %bitcast.15.down0_ref, ...), custom_call_target="tpu_custom_call" | custom-call | flops 2818572288 | bytes 14647296 | tf_op jit(solution)/shard_map/pallas_call | solution.py:41
  62.2 6.4 %shard_map.121 = (bf16[448,2048]{1,0:T(8,128)(2,1)}, bf16[448,2048]{1,0:T(8,128)(2,1)}, bf16[448,2048]{1,0:T(8,128)(2,1)}) custom-call(s32[1]{0:T(128)} %bitcast.6.par_ref, bf16[384,1024]{1,0:T(8,128)(2,1)S(1)} %bitcast.32, bf16[192,1024]{1,0:T(8,128)(2,1)} %copy-done.3, bf16[192,1024]{1,0:T(8,128)(2,1)} %copy-done.4, bf16[384,2048]{1,0:T(8,128)(2,1)S(1)} %bitcast.29, ...), custom_call_target="tpu_custom_call" | custom-call | flops 2113929216 | bytes 6586372 | tf_op jit(solution)/shard_map/pallas_call | solution.py:41
  68.6 3.0 %collective-permute-start.10 = (bf16[448,2048]{1,0:T(8,128)(2,1)}, bf16[448,2048]{1,0:T(8,128)(2,1)S(1)}, u32[]{:S(2)}, u32[]{:S(2)}) collective-permute-start(bf16[448,2048]{1,0:T(8,128)(2,1)} %get-tuple-element.35), channel_id=1, source_target_pairs={{0,1},{1,0},{2,3},{3,2},{4,5},{5,4},{6,7},{7,6},{8,9},{9,8},{10,11... | collective-permute-start | bytes 5505032 | tf_op jit(solution)/shard_map/ppermute | solution.py:341
  71.6 0.1 collective-permute-start.11
  71.7 0.4 collective-permute-start.12
  72.1 5.6 %collective-permute-start.4 = (bf16[192,1152]{1,0:T(8,128)(2,1)S(1)}, bf16[192,1152]{1,0:T(8,128)(2,1)S(1)}, u32[]{:S(2)}, u32[]{:S(2)}) collective-permute-start(bf16[192,1152]{1,0:T(8,128)(2,1)S(1)} %get-tuple-element.25), channel_id=1, source_target_pairs={{0,14},{2,0},{4,2},{6,4},{8,6},{10,8},{12,10},{14,12},{1,15},{3,1}... | collective-permute-start | bytes 1327112 | tf_op jit(solution)/shard_map/ppermute | solution.py:344
  77.7 0.0 collective-permute-start.5
  77.7 4.3 %shard_map.116.own_ref = f32[384,1152]{1,0:T(8,128)S(1)} custom-call(bf16[2,2,384,448]{3,2,1,0:T(8,128)(2,1)} %get-tuple-element.23.grads_ref, f32[384,128]{1,0:T(8,128)S(1)} %get-tuple-element.24.gate_ref, bf16[2,2,448,1024]{3,2,1,0:T(8,128)(2,1)} %shard_map.113.own_ref, bf16[2,2,448,1024]{3,2,1,0:T(8,128)(2,1)} %collective-permute-done.2.other_ref), custom_call_target="tpu_custom_call" | custom-call | flops 1409286144 | bytes 8912896 | tf_op jit(solution)/shard_map/pallas_call | solution.py:41
  82.0 5.1 %collective-permute-done.4.low_ref = bf16[192,1152]{1,0:T(8,128)(2,1)S(1)} collective-permute-done((bf16[192,1152]{1,0:T(8,128)(2,1)S(1)}, bf16[192,1152]{1,0:T(8,128)(2,1)S(1)}, u32[]{:S(2)}, u32[]{:S(2)}) %collective-permute-start.4) | collective-permute-done | bytes 442400 | tf_op jit(solution)/shard_map/ppermute | solution.py:344
  87.2 3.1 %collective-permute-done.5.high_ref = bf16[192,1152]{1,0:T(8,128)(2,1)S(1)} collective-permute-done((bf16[192,1152]{1,0:T(8,128)(2,1)S(1)}, bf16[192,1152]{1,0:T(8,128)(2,1)S(1)}, u32[]{:S(2)}, u32[]{:S(2)}) %collective-permute-start.5) | collective-permute-done | bytes 442400 | tf_op jit(solution)/shard_map/ppermute | solution.py:344
  90.3 1.1 shard_map.117
  91.4 17.9 %all_to_all.15 = bf16[16,24,1152]{2,1,0:T(8,128)(2,1)S(1)} all-to-all(bf16[16,24,1152]{2,1,0:T(8,128)(2,1)} %bitcast.36), channel_id=1, replica_groups=mesh['y'=4,'x'=4,'zh'=4,'zl'=2,'c'=2] {'y','x'}, dimensions={0} | all-to-all | bytes 1769472 | tf_op jit(solution)/shard_map/all_to_all | solution.py:347
  109.3 0.4 shard_map.118
  109.7 2.1 %collective-permute-start.6 = (bf16[4,208,128]{2,1,0:T(8,128)(2,1)S(1)}, bf16[4,208,128]{2,1,0:T(8,128)(2,1)S(1)}, u32[]{:S(2)}, u32[]{:S(2)}) collective-permute-start(bf16[4,208,128]{2,1,0:T(8,128)(2,1)S(1)} %get-tuple-element.28), channel_id=1, source_target_pairs={{0,1},{1,0},{2,3},{3,2},{4,5},{5,4},{6,7},{7,6},{8,9},{9,8},{10,11... | collective-permute-start | bytes 638984 | tf_op jit(solution)/shard_map/ppermute | solution.py:341
  111.8 1.1 collective-permute-done.6.got_ref
  112.9 0.1 shard_map.119
  113.0 0.1 collective-permute-start.7
  113.1 3.2 %collective-permute-start.8 = (bf16[208,128]{1,0:T(8,128)(2,1)S(1)}, bf16[208,128]{1,0:T(8,128)(2,1)S(1)}, u32[]{:S(2)}, u32[]{:S(2)}) collective-permute-start(bf16[208,128]{1,0:T(8,128)(2,1)S(1)} %get-tuple-element.31), channel_id=1, source_target_pairs={{0,8},{2,10},{4,12},{6,14},{8,0},{10,2},{12,4},{14,6},{1,9},{3,11}... | collective-permute-start | bytes 159752 | tf_op jit(solution)/shard_map/ppermute | solution.py:344
  116.2 2.0 %collective-permute-done.7.refs_1_ = bf16[208,128]{1,0:T(8,128)(2,1)S(1)} collective-permute-done((bf16[208,128]{1,0:T(8,128)(2,1)S(1)}, bf16[208,128]{1,0:T(8,128)(2,1)S(1)}, u32[]{:S(2)}, u32[]{:S(2)}) %collective-permute-start.7) | collective-permute-done | bytes 53280 | tf_op jit(solution)/shard_map/ppermute | solution.py:344
  118.2 1.5 %collective-permute-start.9 = (bf16[208,128]{1,0:T(8,128)(2,1)S(1)}, bf16[208,128]{1,0:T(8,128)(2,1)S(1)}, u32[]{:S(2)}, u32[]{:S(2)}) collective-permute-start(bf16[208,128]{1,0:T(8,128)(2,1)S(1)} %get-tuple-element.32), channel_id=1, source_target_pairs={{0,12},{2,14},{4,0},{6,2},{8,4},{10,6},{12,8},{14,10},{1,13},{3,15... | collective-permute-start | bytes 159752 | tf_op jit(solution)/shard_map/ppermute | solution.py:344
  119.7 0.5 collective-permute-done.8.refs_2_
  120.2 3.0 %collective-permute-done.9.refs_3_ = bf16[208,128]{1,0:T(8,128)(2,1)S(1)} collective-permute-done((bf16[208,128]{1,0:T(8,128)(2,1)S(1)}, bf16[208,128]{1,0:T(8,128)(2,1)S(1)}, u32[]{:S(2)}, u32[]{:S(2)}) %collective-permute-start.9) | collective-permute-done | bytes 53280 | tf_op jit(solution)/shard_map/ppermute | solution.py:344
  123.2 0.7 shard_map.120
  123.9 0.0 collective-permute-done.10.refs_0_
  123.9 0.0 collective-permute-done.12.refs_2_
  123.9 1.2 copy-done
  125.2 0.5 copy-done.1
  125.7 1.2 copy-done.2
  126.9 7.6 %shard_map.122 = (bf16[448,2048]{1,0:T(8,128)(2,1)}, bf16[448,2048]{1,0:T(8,128)(2,1)}, bf16[448,2048]{1,0:T(8,128)(2,1)}) custom-call(s32[1]{0:T(128)} %bitcast.6.par_ref, bf16[384,1024]{1,0:T(8,128)(2,1)S(1)} %bitcast.33, bf16[192,1024]{1,0:T(8,128)(2,1)} %copy-done.3, bf16[192,1024]{1,0:T(8,128)(2,1)} %copy-done.4, bf16[384,2048]{1,0:T(8,128)(2,1)S(1)} %bitcast.30, ...), custom_call_target="tpu_custom_call" | custom-call | flops 2113929216 | bytes 12091396 | tf_op jit(solution)/shard_map/pallas_call | solution.py:41
  (7 shorter events, 0.0 us)
Async XLA Ops:
  4.1 42.7 %collective-permute-start.2 = (bf16[2,2,448,1024]{3,2,1,0:T(8,128)(2,1)}, bf16[2,2,448,1024]{3,2,1,0:T(8,128)(2,1)}, u32[]{:S(2)}, u32[]{:S(2)}) collective-permute-start(bf16[2,2,448,1024]{3,2,1,0:T(8,128)(2,1)} %shard_map.113.own_ref), channel_id=1, source_target_pairs={{0,1},{1,0},{2,3},{3,2},{4,5},{5,4},{6,7},{7,6},{8,9},{9,8},{10,11... | collective-permute-start | bytes 11010056 | tf_op jit(solution)/shard_map/ppermute | solution.py:341
  10.4 18.9 %all-to-all-start.1 = ((bf16[16,24,1024]{2,1,0:T(8,128)(2,1)}), bf16[16,24,1024]{2,1,0:T(8,128)(2,1)S(1)}, u32[]{:S(2)}, u32[]{:S(2)}) async-start(bf16[16,24,1024]{2,1,0:T(8,128)(2,1)} %bitcast.37), calls=%async_computation.1 | async-start | bytes 1572864 | tf_op jit(solution)/shard_map/all_to_all | solution.py:347
  15.5 39.6 %collective-permute-start.3 = (bf16[448,2048]{1,0:T(8,128)(2,1)}, bf16[448,2048]{1,0:T(8,128)(2,1)}, u32[]{:S(2)}, u32[]{:S(2)}) collective-permute-start(bf16[448,2048]{1,0:T(8,128)(2,1)} %bitcast.15.down0_ref), channel_id=1, source_target_pairs={{0,1},{1,0},{2,3},{3,2},{4,5},{5,4},{6,7},{7,6},{8,9},{9,8},{10,11... | collective-permute-start | bytes 5505032 | tf_op jit(solution)/shard_map/ppermute | solution.py:341
  29.4 25.8 %all-to-all-start = ((bf16[16,24,2048]{2,1,0:T(8,128)(2,1)}), bf16[16,24,2048]{2,1,0:T(8,128)(2,1)S(1)}, u32[]{:S(2)}, u32[]{:S(2)}) async-start(bf16[16,24,2048]{2,1,0:T(8,128)(2,1)} %bitcast.35), calls=%async_computation | async-start | bytes 3145728 | tf_op jit(solution)/shard_map/all_to_all | solution.py:347
  33.1 13.7 %collective-permute-start = (bf16[192,1024]{1,0:T(8,128)(2,1)S(1)}, bf16[192,1024]{1,0:T(8,128)(2,1)S(1)}, u32[]{:S(2)}, u32[]{:S(2)}) collective-permute-start(bf16[192,1024]{1,0:T(8,128)(2,1)S(1)} %bitcast.41), channel_id=1, source_target_pairs={{0,2},{2,4},{4,6},{6,8},{8,10},{10,12},{12,14},{14,0},{1,3},{3,5},... | collective-permute-start | bytes 1179656 | tf_op jit(solution)/shard_map/ppermute | solution.py:344
  34.8 12.0 %collective-permute-start.1 = (bf16[192,1024]{1,0:T(8,128)(2,1)S(1)}, bf16[192,1024]{1,0:T(8,128)(2,1)S(1)}, u32[]{:S(2)}, u32[]{:S(2)}) collective-permute-start(bf16[192,1024]{1,0:T(8,128)(2,1)S(1)} %bitcast.40), channel_id=1, source_target_pairs={{0,14},{2,0},{4,2},{6,4},{8,6},{10,8},{12,10},{14,12},{1,15},{3,1}... | collective-permute-start | bytes 1179656 | tf_op jit(solution)/shard_map/ppermute | solution.py:344
  46.8 0.7 copy-start.3
  46.8 0.9 copy-start.4
  68.6 55.3 %collective-permute-start.10 = (bf16[448,2048]{1,0:T(8,128)(2,1)}, bf16[448,2048]{1,0:T(8,128)(2,1)S(1)}, u32[]{:S(2)}, u32[]{:S(2)}) collective-permute-start(bf16[448,2048]{1,0:T(8,128)(2,1)} %get-tuple-element.35), channel_id=1, source_target_pairs={{0,1},{1,0},{2,3},{3,2},{4,5},{5,4},{6,7},{7,6},{8,9},{9,8},{10,11... | collective-permute-start | bytes 5505032 | tf_op jit(solution)/shard_map/ppermute | solution.py:341
  71.6 52.3 %collective-permute-start.11 = (bf16[448,2048]{1,0:T(8,128)(2,1)}, bf16[448,2048]{1,0:T(8,128)(2,1)S(1)}, u32[]{:S(2)}, u32[]{:S(2)}) collective-permute-start(bf16[448,2048]{1,0:T(8,128)(2,1)} %get-tuple-element.36), channel_id=1, source_target_pairs={{0,1},{1,0},{2,3},{3,2},{4,5},{5,4},{6,7},{7,6},{8,9},{9,8},{10,11... | collective-permute-start | bytes 5505032 | tf_op jit(solution)/shard_map/ppermute | solution.py:341
  71.7 52.2 %collective-permute-start.12 = (bf16[448,2048]{1,0:T(8,128)(2,1)}, bf16[448,2048]{1,0:T(8,128)(2,1)S(1)}, u32[]{:S(2)}, u32[]{:S(2)}) collective-permute-start(bf16[448,2048]{1,0:T(8,128)(2,1)} %get-tuple-element.37), channel_id=1, source_target_pairs={{0,1},{1,0},{2,3},{3,2},{4,5},{5,4},{6,7},{7,6},{8,9},{9,8},{10,11... | collective-permute-start | bytes 5505032 | tf_op jit(solution)/shard_map/ppermute | solution.py:341
  72.1 15.0 %collective-permute-start.4 = (bf16[192,1152]{1,0:T(8,128)(2,1)S(1)}, bf16[192,1152]{1,0:T(8,128)(2,1)S(1)}, u32[]{:S(2)}, u32[]{:S(2)}) collective-permute-start(bf16[192,1152]{1,0:T(8,128)(2,1)S(1)} %get-tuple-element.25), channel_id=1, source_target_pairs={{0,14},{2,0},{4,2},{6,4},{8,6},{10,8},{12,10},{14,12},{1,15},{3,1}... | collective-permute-start | bytes 1327112 | tf_op jit(solution)/shard_map/ppermute | solution.py:344
  77.7 12.6 %collective-permute-start.5 = (bf16[192,1152]{1,0:T(8,128)(2,1)S(1)}, bf16[192,1152]{1,0:T(8,128)(2,1)S(1)}, u32[]{:S(2)}, u32[]{:S(2)}) collective-permute-start(bf16[192,1152]{1,0:T(8,128)(2,1)S(1)} %get-tuple-element.26), channel_id=1, source_target_pairs={{0,2},{2,4},{4,6},{6,8},{8,10},{10,12},{12,14},{14,0},{1,3},{3,5},... | collective-permute-start | bytes 1327112 | tf_op jit(solution)/shard_map/ppermute | solution.py:344
  109.7 3.2 %collective-permute-start.6 = (bf16[4,208,128]{2,1,0:T(8,128)(2,1)S(1)}, bf16[4,208,128]{2,1,0:T(8,128)(2,1)S(1)}, u32[]{:S(2)}, u32[]{:S(2)}) collective-permute-start(bf16[4,208,128]{2,1,0:T(8,128)(2,1)S(1)} %get-tuple-element.28), channel_id=1, source_target_pairs={{0,1},{1,0},{2,3},{3,2},{4,5},{5,4},{6,7},{7,6},{8,9},{9,8},{10,11... | collective-permute-start | bytes 638984 | tf_op jit(solution)/shard_map/ppermute | solution.py:341
  113.0 5.2 %collective-permute-start.7 = (bf16[208,128]{1,0:T(8,128)(2,1)S(1)}, bf16[208,128]{1,0:T(8,128)(2,1)S(1)}, u32[]{:S(2)}, u32[]{:S(2)}) collective-permute-start(bf16[208,128]{1,0:T(8,128)(2,1)S(1)} %get-tuple-element.30), channel_id=1, source_target_pairs={{0,4},{2,6},{4,8},{6,10},{8,12},{10,14},{12,0},{14,2},{1,5},{3,7},... | collective-permute-start | bytes 159752 | tf_op jit(solution)/shard_map/ppermute | solution.py:344
  113.1 7.1 %collective-permute-start.8 = (bf16[208,128]{1,0:T(8,128)(2,1)S(1)}, bf16[208,128]{1,0:T(8,128)(2,1)S(1)}, u32[]{:S(2)}, u32[]{:S(2)}) collective-permute-start(bf16[208,128]{1,0:T(8,128)(2,1)S(1)} %get-tuple-element.31), channel_id=1, source_target_pairs={{0,8},{2,10},{4,12},{6,14},{8,0},{10,2},{12,4},{14,6},{1,9},{3,11}... | collective-permute-start | bytes 159752 | tf_op jit(solution)/shard_map/ppermute | solution.py:344
  118.2 5.0 %collective-permute-start.9 = (bf16[208,128]{1,0:T(8,128)(2,1)S(1)}, bf16[208,128]{1,0:T(8,128)(2,1)S(1)}, u32[]{:S(2)}, u32[]{:S(2)}) collective-permute-start(bf16[208,128]{1,0:T(8,128)(2,1)S(1)} %get-tuple-element.32), channel_id=1, source_target_pairs={{0,12},{2,14},{4,0},{6,2},{8,4},{10,6},{12,8},{14,10},{1,13},{3,15... | collective-permute-start | bytes 159752 | tf_op jit(solution)/shard_map/ppermute | solution.py:344
  123.9 1.3 copy-start
  123.9 1.8 %copy-start.1 = (bf16[448,2048]{1,0:T(8,128)(2,1)}, bf16[448,2048]{1,0:T(8,128)(2,1)S(1)}, u32[]{:S(2)}) copy-start(bf16[448,2048]{1,0:T(8,128)(2,1)S(1)} %collective-permute-done.11.refs_1_) | copy-start | bytes 5505028
  125.7 1.2 copy-start.2

commit v6 on v5

--- a/solution.py
+++ b/solution.py
@@ -72,17 +72,29 @@
     return jnp.where(hit, 1.0, 0.0).astype(BF16)
 
 
-def send_tokens(experts, half, core_ref, par_ref, routes_ref, tok_ref, out_ref, tok, sem):
+def send_tokens(experts, half, core_ref, par_ref, routes_ref, tok_ref, out_ref, routes, route_sem, tok, sem, made, out_sem):
+    route = pltpu.make_async_copy(routes_ref, routes, route_sem)
+    route.start()
     copies = [
         pltpu.make_async_copy(tok_ref.at[:, cols], tok.at[:, to], sem.at[n])
         for n, (to, cols) in enumerate(side_columns(par_ref[0], tok_ref.shape[1]))
     ]
     for copy in copies:
         copy.start()
-    masks = masks_of(slots_of(core_ref[0], routes_ref[...], experts, half), experts * half)
-    for copy in copies:
-        copy.wait()
-    out_ref[...] = dot(pick_of(masks), tok[...], NN).astype(BF16)
+    route.wait()
+    masks = masks_of(slots_of(core_ref[0], routes[...], experts, half), experts * half)
+    for copy in copies:
+        copy.wait()
+    pick = pick_of(masks)
+    part = out_ref.shape[1]
+    done = []
+    for n in range(2):
+        cols = slice(n * part // 2, (n + 1) * part // 2)
+        made[:, cols] = dot(pick, tok[:, cols], NN).astype(BF16)
+        done.append(pltpu.make_async_copy(made.at[:, cols], out_ref.at[:, cols], out_sem.at[n]))
+        done[-1].start()
+    for copy in done:
+        copy.wait()
 
 
 def keep_table(experts, half, core_ref, routes_ref, gates_ref, out_ref):
@@ -131,37 +143,22 @@
         copy.wait()
 
 
-def fetch_rows(low_ref, high_ref, both, sem):
-    rows = low_ref.shape[0]
-    copies = [
-        pltpu.make_async_copy(low_ref, both.at[:rows], sem.at[0]),
-        pltpu.make_async_copy(high_ref, both.at[rows:], sem.at[1]),
-    ]
-    for copy in copies:
-        copy.start()
-    return copies
-
-
-def forward(mine_ref, low_ref, high_ref, own_ref, other_ref, out_ref, buf, sem, both, half_sem, made, out_sem):
+def forward(mine_ref, low_ref, high_ref, own_ref, other_ref, out_ref, both_ref, buf, sem, both, both_sem, made, out_sem):
     jobs = [(w.at[n, k], buf.at[2 * p + n, k]) for p, w in enumerate((own_ref, other_ref)) for n in range(2) for k in range(2)]
     copies = [pltpu.make_async_copy(a, b, sem.at[i]) for i, (a, b) in enumerate(jobs)]
-    for copy in copies[:2]:
-        copy.start()
-    halves = fetch_rows(low_ref, high_ref, both, half_sem)
-    for copy in copies[2:4]:
-        copy.start()
+    for copy in copies:
+        copy.start()
+    rows = low_ref.shape[0]
+    both[:rows] = low_ref[...]
+    both[rows:] = high_ref[...]
+    keep = pltpu.make_async_copy(both, both_ref, both_sem)
+    keep.start()
     done = []
 
     def product(n):
         copies[2 * n].wait()
         copies[2 * n + 1].wait()
-        for copy in copies[2 * n + 4 : 2 * n + 6]:
-            copy.start()
-        total = dot(mine_ref[...], buf[n, 0], NT)
-        if n == 0:
-            for copy in halves:
-                copy.wait()
-        return total + dot(both[...], buf[n, 1], NT)
+        return dot(mine_ref[...], buf[n, 0], NT) + dot(both[...], buf[n, 1], NT)
 
     for p in range(2):
         pre = product(2 * p)
@@ -173,7 +170,7 @@
         made[p, 2] = act.astype(BF16)
         done.append(pltpu.make_async_copy(made.at[p], out_ref.at[p], out_sem.at[p]))
         done[-1].start()
-    for copy in done:
+    for copy in [keep, *done]:
         copy.wait()
 
 
@@ -199,16 +196,12 @@
         pltpu.make_async_copy(w, wd.at[p], wd_sem.at[p]) for p, w in enumerate((down0_ref, down1_ref))
     ]
     columns = fetch_half(1, own_ref, other_ref, buf, sem)
-    downs[0].start()
-    mids[0].start()
-    downs[1].start()
-    mids[1].start()
+    for copy in (downs[0], mids[0], downs[1], mids[1], *columns):
+        copy.start()
     gate = jnp.zeros((rows, 1), F32)
     done = []
     for p in range(2):
         downs[p].wait()
-        for copy in columns[2 * p : 2 * p + 2]:
-            copy.start()
         back = dot(cot_ref[...], wd[p], NT)
         mids[p].wait()
         gate = gate + jnp.sum(mid[p, 0].astype(F32) * back, axis=1, keepdims=True)
@@ -241,46 +234,62 @@
     out_ref[:, :part] = input_grad(grads, buf)
 
 
-def add_pair(own_ref, low_ref, high_ref, out_ref):
+def add_pair(own_ref, low_ref, high_ref, out_ref, made, sem):
     rows = low_ref.shape[0]
-    out_ref[:rows] = (own_ref[:rows] + low_ref[...].astype(F32)).astype(BF16)
-    out_ref[rows:] = (own_ref[rows:] + high_ref[...].astype(F32)).astype(BF16)
-
-
-def weight_grads(p, par_ref, mine_ref, low_ref, high_ref, cot_ref, mid_ref, grads_ref, *refs):
-    inputs = refs[:3] if p == 0 else ()
-    outs, (both, half_sem, made, out_sem, left, left_sem, *got) = refs[len(inputs) :][:3], refs[len(inputs) + 3 :]
-    lefts = [grads_ref.at[p, 0], grads_ref.at[p, 1], mid_ref.at[p, 0]]
-    copies = [pltpu.make_async_copy(r, left.at[n], left_sem.at[n]) for n, r in enumerate(lefts)]
+    done = []
+    for n, other in enumerate((low_ref, high_ref)):
+        span = slice(n * rows, (n + 1) * rows)
+        made[span] = (own_ref[span] + other[...].astype(F32)).astype(BF16)
+        done.append(pltpu.make_async_copy(made.at[span], out_ref.at[span], sem.at[n]))
+        done[-1].start()
+    for copy in done:
+        copy.wait()
+
+
+def row_grads(p, par_ref, mine_ref, both_ref, grads_ref, *refs):
+    inputs = refs[:2] if p == 0 else ()
+    outs, scratch = refs[len(inputs) : len(inputs) + 2], refs[len(inputs) + 2 :]
+    both, both_sem, left, left_sem, made, out_sem, *got = scratch
+    keep = pltpu.make_async_copy(both_ref, both, both_sem)
+    copies = [pltpu.make_async_copy(grads_ref.at[p, n], left.at[n], left_sem.at[n]) for n in range(2)]
     received = [pltpu.make_async_copy(r, got[0].at[n], got[1].at[n]) for n, r in enumerate(inputs)]
-    halves = fetch_rows(low_ref, high_ref, both, half_sem)
-    for copy in copies + received:
+    for copy in (copies[0], keep, copies[1], *received):
         copy.start()
     done = []
-
-    def put(n, cols, grad):
-        if p == 0:
-            grad += got[0][n, :, cols].astype(F32)
-        made[n, :, cols] = grad.astype(BF16)
-
-    for n in range(3):
+    for n in range(2):
         copies[n].wait()
         if p == 0:
             received[n].wait()
-        if n == 0:
-            for copy in halves:
-                copy.wait()
-        if n < 2:
-            for side, right in ((par_ref[0], mine_ref), (1 - par_ref[0], both)):
-                grad = dot(left[n], right[...], TN)
-                for to, cols in side_columns(side, made.shape[2]):
-                    put(n, cols, grad[:, to])
-        else:
-            put(n, slice(None), dot(left[n], cot_ref[...], TN))
+        for side, right in ((par_ref[0], mine_ref), (1 - par_ref[0], both)):
+            if n == 0 and right is both:
+                keep.wait()
+            grad = dot(left[n], right[...], TN)
+            for to, cols in side_columns(side, made.shape[2]):
+                piece = grad[:, to]
+                if p == 0:
+                    piece = piece + got[0][n, :, cols].astype(F32)
+                made[n, :, cols] = piece.astype(BF16)
         done.append(pltpu.make_async_copy(made.at[n], outs[n], out_sem.at[n]))
         done[-1].start()
     for copy in done:
         copy.wait()
+
+
+def down_grads(p, cot_ref, mid_ref, *refs):
+    inputs, (out_ref, left, sem, made, out_sem, *got) = (refs[:1], refs[1:]) if p == 0 else ((), refs)
+    copies = [pltpu.make_async_copy(mid_ref.at[p, 0], left, sem)]
+    copies += [pltpu.make_async_copy(r, got[0], got[1]) for r in inputs]
+    for copy in copies:
+        copy.start()
+    for copy in copies:
+        copy.wait()
+    grad = dot(left[...], cot_ref[...], TN)
+    if p == 0:
+        grad += got[0][...].astype(F32)
+    made[...] = grad.astype(BF16)
+    done = pltpu.make_async_copy(made, out_ref, out_sem)
+    done.start()
+    done.wait()
 
 
 def combine(core_ref, table_ref, x_ref, keep_ref, send_ref):
@@ -367,9 +376,12 @@
 
     (tok_out,) = call(
         functools.partial(send_tokens, experts, half),
-        [((count, part), BF16, "w")],
-        (core, "s"), (parity, "s"), (routes, "w"), (tokens, "h"),
-        scratch=[pltpu.VMEM((rows, part), BF16), dma(4)],
+        [((count, part), BF16, "h")],
+        (core, "s"), (parity, "s"), (routes, "h"), (tokens, "h"),
+        scratch=[
+            pltpu.VMEM((top_k, rows), jnp.int32), pltpu.SemaphoreType.DMA,
+            pltpu.VMEM((rows, part), BF16), dma(4), pltpu.VMEM((count, part), BF16), dma(2),
+        ],
         flops=2 * count * rows * part, mib=8,
     )
     mine = exchange(tok_out.reshape(experts, half, part)).reshape(count, part)
@@ -385,11 +397,12 @@
     packed = [(own, "h"), (other, "h")]
     mids = pltpu.VMEM((2, 3, count, ff), BF16)
     halves = [pltpu.VMEM((4, ff, part), BF16), dma(4)]
-    (mid,) = call(
-        forward, [((2, 3, count, ff), BF16, "h")],
-        (mine, "v"), (low, "h"), (high, "h"), *packed,
+    mid, both = call(
+        forward, [((2, 3, count, ff), BF16, "h"), ((count, part), BF16, "h")],
+        (mine, "v"), (low, "v"), (high, "v"), *packed,
         scratch=[
-            pltpu.VMEM((4, 2, ff, part), BF16), dma(8), pltpu.VMEM((count, part), BF16), dma(2), mids, dma(2),
+            pltpu.VMEM((4, 2, ff, part), BF16), dma(8), pltpu.VMEM((count, part), BF16),
+            pltpu.SemaphoreType.DMA, mids, dma(2),
         ],
         flops=8 * count * width * ff, mib=18,
     )
@@ -412,22 +425,37 @@
         flops=4 * count * width * ff, mib=14,
     )
     (pair,) = call(
-        add_pair, [((count, part + LANES), BF16, "w")], (kept, "v"), (from_low, "v"), (from_high, "v"), mib=8
+        add_pair, [((count, part + LANES), BF16, "h")], (kept, "v"), (from_low, "v"), (from_high, "v"),
+        scratch=[pltpu.VMEM((count, part + LANES), BF16), dma(2)], mib=8,
     )
     returned = exchange(pair.reshape(experts, half, part + LANES)).reshape(count, part + LANES)
 
-    pieces = [(mine, "v"), (low, "h"), (high, "h"), (cot, "v"), (mid, "h"), (grads, "h")]
-    shard = [((ff, width), BF16, "h")] * 3
-    whole = pltpu.VMEM((3, ff, width), BF16)
-    room = [pltpu.VMEM((count, part), BF16), dma(2), whole, dma(3), pltpu.VMEM((3, count, ff), BF16), dma(3)]
+    one = pltpu.SemaphoreType.DMA
+    shard = ((ff, width), BF16, "h")
+    pair_room = pltpu.VMEM((2, ff, width), BF16)
+    row_args = [(parity, "s"), (mine, "v"), (both, "h"), (grads, "h")]
+    row_room = [
+        pltpu.VMEM((count, part), BF16), one, pltpu.VMEM((2, count, ff), BF16), dma(2), pair_room, dma(2),
+    ]
+    down_args = [(cot, "v"), (mid, "h")]
+    down_room = [pltpu.VMEM((count, ff), BF16), one, pltpu.VMEM((ff, width), BF16), one]
+    cost = 2 * count * width * ff
+    (their_down,) = call(
+        functools.partial(down_grads, 1), [shard], *down_args,
+        scratch=down_room, flops=cost, mib=10,
+    )
     theirs = call(
-        functools.partial(weight_grads, 1), shard, (parity, "s"), *pieces,
-        scratch=room, flops=6 * count * width * ff, mib=14,
+        functools.partial(row_grads, 1), [shard] * 2, *row_args,
+        scratch=row_room, flops=2 * cost, mib=14,
+    )
+    (grad_down,) = call(
+        functools.partial(down_grads, 0), [shard], *down_args, (swap(their_down), "h"),
+        scratch=[*down_room, down_room[2], one], flops=cost, mib=12,
     )
     received = [(swap(g), "h") for g in theirs]
-    grad_gate, grad_up, grad_down = call(
-        functools.partial(weight_grads, 0), shard, (parity, "s"), *pieces, *received,
-        scratch=[*room, whole, dma(3)], flops=6 * count * width * ff, mib=20,
+    grad_gate, grad_up = call(
+        functools.partial(row_grads, 0), [shard] * 2, *row_args, *received,
+        scratch=[*row_room, pair_room, dma(2)], flops=2 * cost, mib=18,
     )
 
     block = (depth // 2, rows + 16, LANES)

time: 135 us -> 140 us (1.037)
  waiting for transfers between devices: 32.4 us -> 35.8 us
  Pallas kernels: 45.1 us -> 48 us
  starting transfers between devices: 34.4 us -> 32.7 us
    ppermute x7, waiting for transfers between devices: 21.5 us -> 24.5 us  [shift(): return lax.ppermute(v, Z, [(i, (i + k) % depth) for i in range(depth)])]
    pallas_call x13 -> x15, Pallas kernels: 45.1 us -> 48 us  [call(): kernel_call(*(a if m == 's' else pltpu.with_memory_space_constraint(a, pl...]
    ppermute x7, starting transfers between devices: 16.3 us -> 13.6 us  [shift(): return lax.ppermute(v, Z, [(i, (i + k) % depth) for i in range(depth)])]
    unnamed x10 -> x6, local copies, waits for them, and re-layouts: 3.87 us -> 3.69 us
  transfers between devices with their start and end apart: 15 -> 15, of which waited for: 8 -> 9; matrix products, arithmetic and copies ran while one was open for 0% -> 0% of each run, Pallas kernels for 15% -> 28%
where the time goes in v6:
time: 140 us; the launch traced here: 139 us
  Pallas kernels  48 us (34%)
  waiting for transfers between devices  35.8 us (26%)
  starting transfers between devices  32.7 us (23%)
  blocking collectives  17.9 us (13%)
  local copies, waits for them, and re-layouts  3.75 us (3%)
    pallas_call x15, Pallas kernels, call(): kernel_call(*(a if m == 's' else pltpu.with_memory_space_constraint(a, pl...  48 us
    ppermute x7, waiting for transfers between devices, shift(): return lax.ppermute(v, Z, [(i, (i + k) % depth) for i in range(depth)])  24.5 us
    all_to_all x1, blocking collectives, exchange(): return lax.all_to_all(v, EP, split_axis=0, concat_axis=0, tiled=True)  17.9 us
    ppermute x7, starting transfers between devices, shift(): return lax.ppermute(v, Z, [(i, (i + k) % depth) for i in range(depth)])  13.6 us
    ppermute x6, starting transfers between devices, swap(): return lax.ppermute(v, 'c', [(0, 1), (1, 0)])  10.4 us
    all_to_all x2, waiting for transfers between devices, exchange(): return lax.all_to_all(v, EP, split_axis=0, concat_axis=0, tiled=True)  10.1 us
    all_to_all x2, starting transfers between devices, exchange(): return lax.all_to_all(v, EP, split_axis=0, concat_axis=0, tiled=True)  8.77 us
    unnamed x6, local copies, waits for them, and re-layouts  3.69 us
  transfers between devices with their start and end apart: 15, of which 9 were waited for; matrix products, arithmetic and copies ran while one was open for 0% of the time, Pallas kernels for 28%

profile of v6, /device:TPU:1, one launch (start us, length us, event | category | flops | bytes accessed | tf_op | source)
XLA Modules:
  0.0 139.2 jit_solution(12898278042823986439)
XLA Ops:
  0.6 3.5 %shard_map.113.own_ref = bf16[2,2,448,1024]{3,2,1,0:T(8,128)(2,1)} custom-call(s32[1]{0:T(128)} %bitcast.6.par_ref, bf16[448,2048]{1,0:T(8,128)(2,1)} %bitcast.40, bf16[448,2048]{1,0:T(8,128)(2,1)} %bitcast.41), custom_call_target="tpu_custom_call" | custom-call | bytes 3670020 | tf_op jit(solution)/shard_map/pallas_call | solution.py:41
  4.1 3.3 %collective-permute-start.2 = (bf16[2,2,448,1024]{3,2,1,0:T(8,128)(2,1)}, bf16[2,2,448,1024]{3,2,1,0:T(8,128)(2,1)}, u32[]{:S(2)}, u32[]{:S(2)}) collective-permute-start(bf16[2,2,448,1024]{3,2,1,0:T(8,128)(2,1)} %shard_map.113.own_ref), channel_id=1, source_target_pairs={{0,1},{1,0},{2,3},{3,2},{4,5},{5,4},{6,7},{7,6},{8,9},{9,8},{10,11... | collective-permute-start | bytes 11010056 | tf_op jit(solution)/shard_map/ppermute | solution.py:350
  7.4 2.3 %shard_map.112 = bf16[384,1024]{1,0:T(8,128)(2,1)} custom-call(s32[1]{0:T(128)} %bitcast.core_ref, s32[1]{0:T(128)} %bitcast.6.par_ref, s32[2,192]{1,0:T(2,128)} %bitcast.45, bf16[192,2048]{1,0:T(8,128)(2,1)} %tok_ref.1), custom_call_target="tpu_custom_call" | custom-call | flops 150994944 | bytes 787976 | tf_op jit(solution)/shard_map/pallas_call | solution.py:41
  9.7 5.1 %all-to-all-start.1 = ((bf16[16,24,1024]{2,1,0:T(8,128)(2,1)}), bf16[16,24,1024]{2,1,0:T(8,128)(2,1)S(1)}, u32[]{:S(2)}, u32[]{:S(2)}) async-start(bf16[16,24,1024]{2,1,0:T(8,128)(2,1)} %bitcast.37), calls=%async_computation.1 | async-start | bytes 1572864 | tf_op jit(solution)/shard_map/all_to_all | solution.py:356
  14.8 0.4 collective-permute-start.3
  15.2 0.9 shard_map.110.table_ref
  16.0 2.8 %shard_map.111 = bf16[384,2048]{1,0:T(8,128)(2,1)} custom-call(f32[8,192]{1,0:T(8,128)S(1)} %shard_map.110.table_ref, bf16[192,2048]{1,0:T(8,128)(2,1)} %cot_ref.1), custom_call_target="tpu_custom_call" | custom-call | flops 301989888 | bytes 792576 | tf_op jit(solution)/shard_map/pallas_call | solution.py:41
  18.9 9.7 %all-to-all-done.1 = bf16[16,24,1024]{2,1,0:T(8,128)(2,1)S(1)} async-done(((bf16[16,24,1024]{2,1,0:T(8,128)(2,1)}), bf16[16,24,1024]{2,1,0:T(8,128)(2,1)S(1)}, u32[]{:S(2)}, u32[]{:S(2)}) %all-to-all-start.1) | async-done | bytes 786464 | tf_op jit(solution)/shard_map/all_to_all | solution.py:356
  28.6 3.7 %all-to-all-start = ((bf16[16,24,2048]{2,1,0:T(8,128)(2,1)}), bf16[16,24,2048]{2,1,0:T(8,128)(2,1)S(1)}, u32[]{:S(2)}, u32[]{:S(2)}) async-start(bf16[16,24,2048]{2,1,0:T(8,128)(2,1)} %bitcast.35), calls=%async_computation | async-start | bytes 3145728 | tf_op jit(solution)/shard_map/all_to_all | solution.py:356
  32.3 0.1 fusion
  32.4 1.7 %collective-permute-start = (bf16[192,1024]{1,0:T(8,128)(2,1)S(1)}, bf16[192,1024]{1,0:T(8,128)(2,1)S(1)}, u32[]{:S(2)}, u32[]{:S(2)}) collective-permute-start(bf16[192,1024]{1,0:T(8,128)(2,1)S(1)} %bitcast.44), channel_id=1, source_target_pairs={{0,2},{2,4},{4,6},{6,8},{8,10},{10,12},{12,14},{14,0},{1,3},{3,5},... | collective-permute-start | bytes 1179656 | tf_op jit(solution)/shard_map/ppermute | solution.py:353
  34.1 4.0 %collective-permute-start.1 = (bf16[192,1024]{1,0:T(8,128)(2,1)S(1)}, bf16[192,1024]{1,0:T(8,128)(2,1)S(1)}, u32[]{:S(2)}, u32[]{:S(2)}) collective-permute-start(bf16[192,1024]{1,0:T(8,128)(2,1)S(1)} %bitcast.43), channel_id=1, source_target_pairs={{0,14},{2,0},{4,2},{6,4},{8,6},{10,8},{12,10},{14,12},{1,15},{3,1}... | collective-permute-start | bytes 1179656 | tf_op jit(solution)/shard_map/ppermute | solution.py:353
  38.1 7.9 %collective-permute-done.low_ref = bf16[192,1024]{1,0:T(8,128)(2,1)S(1)} collective-permute-done((bf16[192,1024]{1,0:T(8,128)(2,1)S(1)}, bf16[192,1024]{1,0:T(8,128)(2,1)S(1)}, u32[]{:S(2)}, u32[]{:S(2)}) %collective-permute-start) | collective-permute-done | bytes 393248 | tf_op jit(solution)/shard_map/ppermute | solution.py:353
  46.1 0.0 collective-permute-done.1.high_ref
  46.1 0.0 collective-permute-done.2.other_ref
  46.1 7.2 %shard_map.114 = (bf16[2,3,384,448]{3,2,1,0:T(8,128)(2,1)}, bf16[384,1024]{1,0:T(8,128)(2,1)}) custom-call(bf16[384,1024]{1,0:T(8,128)(2,1)S(1)} %bitcast.31, bf16[192,1024]{1,0:T(8,128)(2,1)S(1)} %collective-permute-done.low_ref, bf16[192,1024]{1,0:T(8,128)(2,1)S(1)} %collective-permute-done.1.high_ref, bf16[2,2,448,1024]{3,2,1,0:T(8,128)(2,1)} %shard_map.113.own_ref, ...), custom_call_target="tpu_custom_call" | custom-call | flops 2818572288 | bytes 8912896 | tf_op jit(solution)/shard_map/pallas_call | solution.py:41
  53.2 0.4 all-to-all-done
  53.7 3.4 %shard_map.123 = bf16[448,2048]{1,0:T(8,128)(2,1)} custom-call(bf16[384,2048]{1,0:T(8,128)(2,1)S(1)} %bitcast.28, bf16[2,3,384,448]{3,2,1,0:T(8,128)(2,1)} %get-tuple-element.23.mid_ref), custom_call_target="tpu_custom_call" | custom-call | flops 704643072 | bytes 3637248 | tf_op jit(solution)/shard_map/pallas_call | solution.py:41
  57.0 4.0 %collective-permute-start.12 = (bf16[448,2048]{1,0:T(8,128)(2,1)}, bf16[448,2048]{1,0:T(8,128)(2,1)S(1)}, u32[]{:S(2)}, u32[]{:S(2)}) collective-permute-start(bf16[448,2048]{1,0:T(8,128)(2,1)} %shard_map.123), channel_id=1, source_target_pairs={{0,1},{1,0},{2,3},{3,2},{4,5},{5,4},{6,7},{7,6},{8,9},{9,8},{10,11... | collective-permute-start | bytes 5505032 | tf_op jit(solution)/shard_map/ppermute | solution.py:350
  61.0 0.0 collective-permute-done.3.down1_ref
  61.0 6.7 %shard_map.115 = (bf16[192,1152]{1,0:T(8,128)(2,1)S(1)}, bf16[192,1152]{1,0:T(8,128)(2,1)S(1)}, bf16[2,2,384,448]{3,2,1,0:T(8,128)(2,1)}, f32[384,128]{1,0:T(8,128)S(1)}) custom-call(bf16[384,2048]{1,0:T(8,128)(2,1)S(1)} %bitcast.29, bf16[2,3,384,448]{3,2,1,0:T(8,128)(2,1)} %get-tuple-element.23.mid_ref, bf16[448,2048]{1,0:T(8,128)(2,1)} %bitcast.39, ...), custom_call_target="tpu_custom_call" | custom-call | flops 2818572288 | bytes 14647296 | tf_op jit(solution)/shard_map/pallas_call | solution.py:41
  67.8 5.0 %shard_map.121 = (bf16[448,2048]{1,0:T(8,128)(2,1)}, bf16[448,2048]{1,0:T(8,128)(2,1)}) custom-call(s32[1]{0:T(128)} %bitcast.6.par_ref, bf16[384,1024]{1,0:T(8,128)(2,1)S(1)} %bitcast.32, bf16[384,1024]{1,0:T(8,128)(2,1)} %get-tuple-element.36.both_ref, bf16[2,2,384,448]{3,2,1,0:T(8,128)(2,1)} %get-tuple-element.24.grads_ref), custom_call_target="tpu_custom_call" | custom-call | flops 1409286144 | bytes 2949124 | tf_op jit(solution)/shard_map/pallas_call | solution.py:41
  72.8 0.1 collective-permute-start.10
  72.9 0.5 collective-permute-start.11
  73.4 5.6 %collective-permute-start.4 = (bf16[192,1152]{1,0:T(8,128)(2,1)S(1)}, bf16[192,1152]{1,0:T(8,128)(2,1)S(1)}, u32[]{:S(2)}, u32[]{:S(2)}) collective-permute-start(bf16[192,1152]{1,0:T(8,128)(2,1)S(1)} %get-tuple-element.26), channel_id=1, source_target_pairs={{0,14},{2,0},{4,2},{6,4},{8,6},{10,8},{12,10},{14,12},{1,15},{3,1}... | collective-permute-start | bytes 1327112 | tf_op jit(solution)/shard_map/ppermute | solution.py:353
  79.0 0.0 collective-permute-start.5
  79.0 4.3 %shard_map.116.own_ref = f32[384,1152]{1,0:T(8,128)S(1)} custom-call(bf16[2,2,384,448]{3,2,1,0:T(8,128)(2,1)} %get-tuple-element.24.grads_ref, f32[384,128]{1,0:T(8,128)S(1)} %get-tuple-element.25.gate_ref, bf16[2,2,448,1024]{3,2,1,0:T(8,128)(2,1)} %shard_map.113.own_ref, bf16[2,2,448,1024]{3,2,1,0:T(8,128)(2,1)} %collective-permute-done.2.other_ref), custom_call_target="tpu_custom_call" | custom-call | flops 1409286144 | bytes 8912896 | tf_op jit(solution)/shard_map/pallas_call | solution.py:41
  83.3 5.1 %collective-permute-done.4.low_ref = bf16[192,1152]{1,0:T(8,128)(2,1)S(1)} collective-permute-done((bf16[192,1152]{1,0:T(8,128)(2,1)S(1)}, bf16[192,1152]{1,0:T(8,128)(2,1)S(1)}, u32[]{:S(2)}, u32[]{:S(2)}) %collective-permute-start.4) | collective-permute-done | bytes 442400 | tf_op jit(solution)/shard_map/ppermute | solution.py:353
  88.4 3.1 %collective-permute-done.5.high_ref = bf16[192,1152]{1,0:T(8,128)(2,1)S(1)} collective-permute-done((bf16[192,1152]{1,0:T(8,128)(2,1)S(1)}, bf16[192,1152]{1,0:T(8,128)(2,1)S(1)}, u32[]{:S(2)}, u32[]{:S(2)}) %collective-permute-start.5) | collective-permute-done | bytes 442400 | tf_op jit(solution)/shard_map/ppermute | solution.py:353
  91.5 1.0 shard_map.117
  92.6 17.9 %all_to_all.15 = bf16[16,24,1152]{2,1,0:T(8,128)(2,1)S(1)} all-to-all(bf16[16,24,1152]{2,1,0:T(8,128)(2,1)} %bitcast.36), channel_id=1, replica_groups=mesh['y'=4,'x'=4,'zh'=4,'zl'=2,'c'=2] {'y','x'}, dimensions={0} | all-to-all | bytes 1769472 | tf_op jit(solution)/shard_map/all_to_all | solution.py:356
  110.5 0.4 shard_map.118
  111.0 2.1 %collective-permute-start.6 = (bf16[4,208,128]{2,1,0:T(8,128)(2,1)S(1)}, bf16[4,208,128]{2,1,0:T(8,128)(2,1)S(1)}, u32[]{:S(2)}, u32[]{:S(2)}) collective-permute-start(bf16[4,208,128]{2,1,0:T(8,128)(2,1)S(1)} %get-tuple-element.29), channel_id=1, source_target_pairs={{0,1},{1,0},{2,3},{3,2},{4,5},{5,4},{6,7},{7,6},{8,9},{9,8},{10,11... | collective-permute-start | bytes 638984 | tf_op jit(solution)/shard_map/ppermute | solution.py:350
  113.1 1.1 collective-permute-done.6.got_ref
  114.2 0.1 shard_map.119
  114.2 0.1 collective-permute-start.7
  114.3 2.2 %collective-permute-start.8 = (bf16[208,128]{1,0:T(8,128)(2,1)S(1)}, bf16[208,128]{1,0:T(8,128)(2,1)S(1)}, u32[]{:S(2)}, u32[]{:S(2)}) collective-permute-start(bf16[208,128]{1,0:T(8,128)(2,1)S(1)} %get-tuple-element.32), channel_id=1, source_target_pairs={{0,8},{2,10},{4,12},{6,14},{8,0},{10,2},{12,4},{14,6},{1,9},{3,11}... | collective-permute-start | bytes 159752 | tf_op jit(solution)/shard_map/ppermute | solution.py:353
  116.5 4.5 %collective-permute-done.7.refs_1_ = bf16[208,128]{1,0:T(8,128)(2,1)S(1)} collective-permute-done((bf16[208,128]{1,0:T(8,128)(2,1)S(1)}, bf16[208,128]{1,0:T(8,128)(2,1)S(1)}, u32[]{:S(2)}, u32[]{:S(2)}) %collective-permute-start.7) | collective-permute-done | bytes 53280 | tf_op jit(solution)/shard_map/ppermute | solution.py:353
  121.0 0.0 collective-permute-start.9
  121.0 0.4 collective-permute-done.8.refs_2_
  121.4 3.5 %collective-permute-done.9.refs_3_ = bf16[208,128]{1,0:T(8,128)(2,1)S(1)} collective-permute-done((bf16[208,128]{1,0:T(8,128)(2,1)S(1)}, bf16[208,128]{1,0:T(8,128)(2,1)S(1)}, u32[]{:S(2)}, u32[]{:S(2)}) %collective-permute-start.9) | collective-permute-done | bytes 53280 | tf_op jit(solution)/shard_map/ppermute | solution.py:353
  124.9 0.7 shard_map.120
  125.5 1.2 copy-done
  126.8 4.0 %shard_map.124 = bf16[448,2048]{1,0:T(8,128)(2,1)} custom-call(bf16[384,2048]{1,0:T(8,128)(2,1)S(1)} %bitcast.30, bf16[2,3,384,448]{3,2,1,0:T(8,128)(2,1)} %get-tuple-element.23.mid_ref, bf16[448,2048]{1,0:T(8,128)(2,1)} %copy-done), custom_call_target="tpu_custom_call" | custom-call | flops 704643072 | bytes 5472256 | tf_op jit(solution)/shard_map/pallas_call | solution.py:41
  130.9 0.0 collective-permute-done.11.refs_1_
  130.9 1.2 copy-done.1
  132.1 1.2 copy-done.2
  133.3 5.7 %shard_map.122 = (bf16[448,2048]{1,0:T(8,128)(2,1)}, bf16[448,2048]{1,0:T(8,128)(2,1)}) custom-call(s32[1]{0:T(128)} %bitcast.6.par_ref, bf16[384,1024]{1,0:T(8,128)(2,1)S(1)} %bitcast.33, bf16[384,1024]{1,0:T(8,128)(2,1)} %get-tuple-element.36.both_ref, bf16[2,2,384,448]{3,2,1,0:T(8,128)(2,1)} %get-tuple-element.24.grads_ref, bf16[448,2048]{1,0:T(8,128)(2,1)} %copy-done.1, ...), custom_call_target="tpu_custom_call" | custom-call | flops 1409286144 | bytes 6619140 | tf_op jit(solution)/shard_map/pallas_call | solution.py:41
  (5 shorter events, 0.0 us)
Async XLA Ops:
  4.1 42.0 %collective-permute-start.2 = (bf16[2,2,448,1024]{3,2,1,0:T(8,128)(2,1)}, bf16[2,2,448,1024]{3,2,1,0:T(8,128)(2,1)}, u32[]{:S(2)}, u32[]{:S(2)}) collective-permute-start(bf16[2,2,448,1024]{3,2,1,0:T(8,128)(2,1)} %shard_map.113.own_ref), channel_id=1, source_target_pairs={{0,1},{1,0},{2,3},{3,2},{4,5},{5,4},{6,7},{7,6},{8,9},{9,8},{10,11... | collective-permute-start | bytes 11010056 | tf_op jit(solution)/shard_map/ppermute | solution.py:350
  9.7 18.9 %all-to-all-start.1 = ((bf16[16,24,1024]{2,1,0:T(8,128)(2,1)}), bf16[16,24,1024]{2,1,0:T(8,128)(2,1)S(1)}, u32[]{:S(2)}, u32[]{:S(2)}) async-start(bf16[16,24,1024]{2,1,0:T(8,128)(2,1)} %bitcast.37), calls=%async_computation.1 | async-start | bytes 1572864 | tf_op jit(solution)/shard_map/all_to_all | solution.py:356
  14.8 46.3 %collective-permute-start.3 = (bf16[448,2048]{1,0:T(8,128)(2,1)}, bf16[448,2048]{1,0:T(8,128)(2,1)}, u32[]{:S(2)}, u32[]{:S(2)}) collective-permute-start(bf16[448,2048]{1,0:T(8,128)(2,1)} %bitcast.38), channel_id=1, source_target_pairs={{0,1},{1,0},{2,3},{3,2},{4,5},{5,4},{6,7},{7,6},{8,9},{9,8},{10,11... | collective-permute-start | bytes 5505032 | tf_op jit(solution)/shard_map/ppermute | solution.py:350
  28.6 25.0 %all-to-all-start = ((bf16[16,24,2048]{2,1,0:T(8,128)(2,1)}), bf16[16,24,2048]{2,1,0:T(8,128)(2,1)S(1)}, u32[]{:S(2)}, u32[]{:S(2)}) async-start(bf16[16,24,2048]{2,1,0:T(8,128)(2,1)} %bitcast.35), calls=%async_computation | async-start | bytes 3145728 | tf_op jit(solution)/shard_map/all_to_all | solution.py:356
  32.4 13.7 %collective-permute-start = (bf16[192,1024]{1,0:T(8,128)(2,1)S(1)}, bf16[192,1024]{1,0:T(8,128)(2,1)S(1)}, u32[]{:S(2)}, u32[]{:S(2)}) collective-permute-start(bf16[192,1024]{1,0:T(8,128)(2,1)S(1)} %bitcast.44), channel_id=1, source_target_pairs={{0,2},{2,4},{4,6},{6,8},{8,10},{10,12},{12,14},{14,0},{1,3},{3,5},... | collective-permute-start | bytes 1179656 | tf_op jit(solution)/shard_map/ppermute | solution.py:353
  34.1 12.0 %collective-permute-start.1 = (bf16[192,1024]{1,0:T(8,128)(2,1)S(1)}, bf16[192,1024]{1,0:T(8,128)(2,1)S(1)}, u32[]{:S(2)}, u32[]{:S(2)}) collective-permute-start(bf16[192,1024]{1,0:T(8,128)(2,1)S(1)} %bitcast.43), channel_id=1, source_target_pairs={{0,14},{2,0},{4,2},{6,4},{8,6},{10,8},{12,10},{14,12},{1,15},{3,1}... | collective-permute-start | bytes 1179656 | tf_op jit(solution)/shard_map/ppermute | solution.py:353
  57.0 68.5 %collective-permute-start.12 = (bf16[448,2048]{1,0:T(8,128)(2,1)}, bf16[448,2048]{1,0:T(8,128)(2,1)S(1)}, u32[]{:S(2)}, u32[]{:S(2)}) collective-permute-start(bf16[448,2048]{1,0:T(8,128)(2,1)} %shard_map.123), channel_id=1, source_target_pairs={{0,1},{1,0},{2,3},{3,2},{4,5},{5,4},{6,7},{7,6},{8,9},{9,8},{10,11... | collective-permute-start | bytes 5505032 | tf_op jit(solution)/shard_map/ppermute | solution.py:350
  72.8 58.0 %collective-permute-start.10 = (bf16[448,2048]{1,0:T(8,128)(2,1)}, bf16[448,2048]{1,0:T(8,128)(2,1)S(1)}, u32[]{:S(2)}, u32[]{:S(2)}) collective-permute-start(bf16[448,2048]{1,0:T(8,128)(2,1)} %get-tuple-element.37), channel_id=1, source_target_pairs={{0,1},{1,0},{2,3},{3,2},{4,5},{5,4},{6,7},{7,6},{8,9},{9,8},{10,11... | collective-permute-start | bytes 5505032 | tf_op jit(solution)/shard_map/ppermute | solution.py:350
  72.9 57.9 %collective-permute-start.11 = (bf16[448,2048]{1,0:T(8,128)(2,1)}, bf16[448,2048]{1,0:T(8,128)(2,1)S(1)}, u32[]{:S(2)}, u32[]{:S(2)}) collective-permute-start(bf16[448,2048]{1,0:T(8,128)(2,1)} %get-tuple-element.38), channel_id=1, source_target_pairs={{0,1},{1,0},{2,3},{3,2},{4,5},{5,4},{6,7},{7,6},{8,9},{9,8},{10,11... | collective-permute-start | bytes 5505032 | tf_op jit(solution)/shard_map/ppermute | solution.py:350
  73.4 15.0 %collective-permute-start.4 = (bf16[192,1152]{1,0:T(8,128)(2,1)S(1)}, bf16[192,1152]{1,0:T(8,128)(2,1)S(1)}, u32[]{:S(2)}, u32[]{:S(2)}) collective-permute-start(bf16[192,1152]{1,0:T(8,128)(2,1)S(1)} %get-tuple-element.26), channel_id=1, source_target_pairs={{0,14},{2,0},{4,2},{6,4},{8,6},{10,8},{12,10},{14,12},{1,15},{3,1}... | collective-permute-start | bytes 1327112 | tf_op jit(solution)/shard_map/ppermute | solution.py:353
  79.0 12.6 %collective-permute-start.5 = (bf16[192,1152]{1,0:T(8,128)(2,1)S(1)}, bf16[192,1152]{1,0:T(8,128)(2,1)S(1)}, u32[]{:S(2)}, u32[]{:S(2)}) collective-permute-start(bf16[192,1152]{1,0:T(8,128)(2,1)S(1)} %get-tuple-element.27), channel_id=1, source_target_pairs={{0,2},{2,4},{4,6},{6,8},{8,10},{10,12},{12,14},{14,0},{1,3},{3,5},... | collective-permute-start | bytes 1327112 | tf_op jit(solution)/shard_map/ppermute | solution.py:353
  111.0 3.2 %collective-permute-start.6 = (bf16[4,208,128]{2,1,0:T(8,128)(2,1)S(1)}, bf16[4,208,128]{2,1,0:T(8,128)(2,1)S(1)}, u32[]{:S(2)}, u32[]{:S(2)}) collective-permute-start(bf16[4,208,128]{2,1,0:T(8,128)(2,1)S(1)} %get-tuple-element.29), channel_id=1, source_target_pairs={{0,1},{1,0},{2,3},{3,2},{4,5},{5,4},{6,7},{7,6},{8,9},{9,8},{10,11... | collective-permute-start | bytes 638984 | tf_op jit(solution)/shard_map/ppermute | solution.py:350
  114.2 6.8 %collective-permute-start.7 = (bf16[208,128]{1,0:T(8,128)(2,1)S(1)}, bf16[208,128]{1,0:T(8,128)(2,1)S(1)}, u32[]{:S(2)}, u32[]{:S(2)}) collective-permute-start(bf16[208,128]{1,0:T(8,128)(2,1)S(1)} %get-tuple-element.31), channel_id=1, source_target_pairs={{0,4},{2,6},{4,8},{6,10},{8,12},{10,14},{12,0},{14,2},{1,5},{3,7},... | collective-permute-start | bytes 159752 | tf_op jit(solution)/shard_map/ppermute | solution.py:353
  114.3 7.1 %collective-permute-start.8 = (bf16[208,128]{1,0:T(8,128)(2,1)S(1)}, bf16[208,128]{1,0:T(8,128)(2,1)S(1)}, u32[]{:S(2)}, u32[]{:S(2)}) collective-permute-start(bf16[208,128]{1,0:T(8,128)(2,1)S(1)} %get-tuple-element.32), channel_id=1, source_target_pairs={{0,8},{2,10},{4,12},{6,14},{8,0},{10,2},{12,4},{14,6},{1,9},{3,11}... | collective-permute-start | bytes 159752 | tf_op jit(solution)/shard_map/ppermute | solution.py:353
  121.0 3.9 %collective-permute-start.9 = (bf16[208,128]{1,0:T(8,128)(2,1)S(1)}, bf16[208,128]{1,0:T(8,128)(2,1)S(1)}, u32[]{:S(2)}, u32[]{:S(2)}) collective-permute-start(bf16[208,128]{1,0:T(8,128)(2,1)S(1)} %get-tuple-element.33), channel_id=1, source_target_pairs={{0,12},{2,14},{4,0},{6,2},{8,4},{10,6},{12,8},{14,10},{1,13},{3,15... | collective-permute-start | bytes 159752 | tf_op jit(solution)/shard_map/ppermute | solution.py:353
  125.5 1.3 copy-start
  130.8 1.3 copy-start.1
  132.1 1.2 copy-start.2

commit v7 on v6

--- a/solution.py
+++ b/solution.py
@@ -143,7 +143,7 @@
         copy.wait()
 
 
-def forward(mine_ref, low_ref, high_ref, own_ref, other_ref, out_ref, both_ref, buf, sem, both, both_sem, made, out_sem):
+def forward(mine_ref, low_ref, high_ref, own_ref, other_ref, out_ref, rows_ref, buf, sem, both, keep_sem, made, out_sem):
     jobs = [(w.at[n, k], buf.at[2 * p + n, k]) for p, w in enumerate((own_ref, other_ref)) for n in range(2) for k in range(2)]
     copies = [pltpu.make_async_copy(a, b, sem.at[i]) for i, (a, b) in enumerate(jobs)]
     for copy in copies:
@@ -151,8 +151,12 @@
     rows = low_ref.shape[0]
     both[:rows] = low_ref[...]
     both[rows:] = high_ref[...]
-    keep = pltpu.make_async_copy(both, both_ref, both_sem)
-    keep.start()
+    keep = [
+        pltpu.make_async_copy(side, rows_ref.at[n], keep_sem.at[n])
+        for n, side in enumerate((mine_ref, both))
+    ]
+    for copy in keep:
+        copy.start()
     done = []
 
     def product(n):
@@ -170,8 +174,14 @@
         made[p, 2] = act.astype(BF16)
         done.append(pltpu.make_async_copy(made.at[p], out_ref.at[p], out_sem.at[p]))
         done[-1].start()
-    for copy in [keep, *done]:
-        copy.wait()
+    for copy in keep + done:
+        copy.wait()
+
+
+def hold(down_ref, out_ref, sem):
+    copy = pltpu.make_async_copy(down_ref, out_ref, sem)
+    copy.start()
+    copy.wait()
 
 
 def input_grad(grads, buf):
@@ -192,17 +202,16 @@
 def backward(cot_ref, mid_ref, down0_ref, down1_ref, own_ref, other_ref, low_ref, high_ref, grads_ref, gate_ref, mid, mid_sem, wd, wd_sem, buf, sem, grads, out_sem):
     rows, width = cot_ref.shape
     mids = [pltpu.make_async_copy(mid_ref.at[p], mid.at[p], mid_sem.at[p]) for p in range(2)]
-    downs = [
-        pltpu.make_async_copy(w, wd.at[p], wd_sem.at[p]) for p, w in enumerate((down0_ref, down1_ref))
-    ]
+    second = pltpu.make_async_copy(down1_ref, wd, wd_sem)
     columns = fetch_half(1, own_ref, other_ref, buf, sem)
-    for copy in (downs[0], mids[0], downs[1], mids[1], *columns):
+    for copy in (mids[0], second, mids[1], *columns):
         copy.start()
     gate = jnp.zeros((rows, 1), F32)
     done = []
     for p in range(2):
-        downs[p].wait()
-        back = dot(cot_ref[...], wd[p], NT)
+        if p == 1:
+            second.wait()
+        back = dot(cot_ref[...], (down0_ref, wd)[p][...], NT)
         mids[p].wait()
         gate = gate + jnp.sum(mid[p, 0].astype(F32) * back, axis=1, keepdims=True)
         grads[p, 0] = (back * mid[p, 1].astype(F32)).astype(BF16)
@@ -246,24 +255,24 @@
         copy.wait()
 
 
-def row_grads(p, par_ref, mine_ref, both_ref, grads_ref, *refs):
+def row_grads(p, par_ref, sides_ref, grads_ref, *refs):
     inputs = refs[:2] if p == 0 else ()
     outs, scratch = refs[len(inputs) : len(inputs) + 2], refs[len(inputs) + 2 :]
-    both, both_sem, left, left_sem, made, out_sem, *got = scratch
-    keep = pltpu.make_async_copy(both_ref, both, both_sem)
+    sides, side_sem, left, left_sem, made, out_sem, *got = scratch
+    keep = [pltpu.make_async_copy(sides_ref.at[k], sides.at[k], side_sem.at[k]) for k in range(2)]
     copies = [pltpu.make_async_copy(grads_ref.at[p, n], left.at[n], left_sem.at[n]) for n in range(2)]
     received = [pltpu.make_async_copy(r, got[0].at[n], got[1].at[n]) for n, r in enumerate(inputs)]
-    for copy in (copies[0], keep, copies[1], *received):
+    for copy in (copies[0], *keep, copies[1], *received):
         copy.start()
     done = []
     for n in range(2):
         copies[n].wait()
         if p == 0:
             received[n].wait()
-        for side, right in ((par_ref[0], mine_ref), (1 - par_ref[0], both)):
-            if n == 0 and right is both:
-                keep.wait()
-            grad = dot(left[n], right[...], TN)
+        for k, side in enumerate((par_ref[0], 1 - par_ref[0])):
+            if n == 0:
+                keep[k].wait()
+            grad = dot(left[n], sides[k], TN)
             for to, cols in side_columns(side, made.shape[2]):
                 piece = grad[:, to]
                 if p == 0:
@@ -397,22 +406,26 @@
     packed = [(own, "h"), (other, "h")]
     mids = pltpu.VMEM((2, 3, count, ff), BF16)
     halves = [pltpu.VMEM((4, ff, part), BF16), dma(4)]
-    mid, both = call(
-        forward, [((2, 3, count, ff), BF16, "h"), ((count, part), BF16, "h")],
+    mid, sides = call(
+        forward, [((2, 3, count, ff), BF16, "h"), ((2, count, part), BF16, "h")],
         (mine, "v"), (low, "v"), (high, "v"), *packed,
         scratch=[
             pltpu.VMEM((4, 2, ff, part), BF16), dma(8), pltpu.VMEM((count, part), BF16),
-            pltpu.SemaphoreType.DMA, mids, dma(2),
+            dma(2), mids, dma(2),
         ],
         flops=8 * count * width * ff, mib=18,
+    )
+    (held,) = call(
+        hold, [((ff, width), BF16, "v")], (down, "h"),
+        scratch=[pltpu.SemaphoreType.DMA], mib=4,
     )
     message = ((count // 2, part + LANES), BF16, "v")
     to_low, to_high, grads, gate = call(
         backward,
         [message, message, ((2, 2, count, ff), BF16, "h"), ((count, LANES), F32, "v")],
-        (cot, "v"), (mid, "h"), (down, "h"), (down_other, "h"), *packed,
+        (cot, "v"), (mid, "h"), (held, "v"), (down_other, "h"), *packed,
         scratch=[
-            mids, dma(2), pltpu.VMEM((2, ff, width), BF16), dma(2), *halves,
+            mids, dma(2), pltpu.VMEM((ff, width), BF16), pltpu.SemaphoreType.DMA, *halves,
             pltpu.VMEM((2, 2, count, ff), BF16), dma(2),
         ],
         flops=8 * count * width * ff, mib=20,
@@ -433,9 +446,9 @@
     one = pltpu.SemaphoreType.DMA
     shard = ((ff, width), BF16, "h")
     pair_room = pltpu.VMEM((2, ff, width), BF16)
-    row_args = [(parity, "s"), (mine, "v"), (both, "h"), (grads, "h")]
+    row_args = [(parity, "s"), (sides, "h"), (grads, "h")]
     row_room = [
-        pltpu.VMEM((count, part), BF16), one, pltpu.VMEM((2, count, ff), BF16), dma(2), pair_room, dma(2),
+        pltpu.VMEM((2, count, part), BF16), dma(2), pltpu.VMEM((2, count, ff), BF16), dma(2), pair_room, dma(2),
     ]
     down_args = [(cot, "v"), (mid, "h")]
     down_room = [pltpu.VMEM((count, ff), BF16), one, pltpu.VMEM((ff, width), BF16), one]

time: 140 us -> 140 us (level)
  waiting for transfers between devices: 35.8 us -> 33.8 us
  Pallas kernels: 48 us -> 49.5 us
    ppermute x7, waiting for transfers between devices: 24.5 us -> 22.8 us  [shift(): return lax.ppermute(v, Z, [(i, (i + k) % depth) for i in range(depth)])]
    pallas_call x15 -> x16, Pallas kernels: 48 us -> 49.5 us  [call(): kernel_call(*(a if m == 's' else pltpu.with_memory_space_constraint(a, pl...]
    unnamed x6 -> x10, local copies, waits for them, and re-layouts: 3.69 us -> 3.7 us
  transfers between devices with their start and end apart: 15 -> 15, of which waited for: 9 -> 9; matrix products, arithmetic and copies ran while one was open for 0% -> 0% of each run, Pallas kernels for 28% -> 29%
where the time goes in v7:
time: 140 us; the launch traced here: 139 us
  Pallas kernels  49.5 us (35%)
  waiting for transfers between devices  33.8 us (24%)
  starting transfers between devices  33.1 us (24%)
  blocking collectives  17.9 us (13%)
  local copies, waits for them, and re-layouts  3.76 us (3%)
    pallas_call x16, Pallas kernels, call(): kernel_call(*(a if m == 's' else pltpu.with_memory_space_constraint(a, pl...  49.5 us
    ppermute x7, waiting for transfers between devices, shift(): return lax.ppermute(v, Z, [(i, (i + k) % depth) for i in range(depth)])  22.8 us
    all_to_all x1, blocking collectives, exchange(): return lax.all_to_all(v, EP, split_axis=0, concat_axis=0, tiled=True)  17.9 us
    ppermute x7, starting transfers between devices, shift(): return lax.ppermute(v, Z, [(i, (i + k) % depth) for i in range(depth)])  13.9 us
    ppermute x6, starting transfers between devices, swap(): return lax.ppermute(v, 'c', [(0, 1), (1, 0)])  10.4 us
    all_to_all x2, waiting for transfers between devices, exchange(): return lax.all_to_all(v, EP, split_axis=0, concat_axis=0, tiled=True)  9.84 us
    all_to_all x2, starting transfers between devices, exchange(): return lax.all_to_all(v, EP, split_axis=0, concat_axis=0, tiled=True)  8.77 us
    unnamed x10, local copies, waits for them, and re-layouts  3.7 us
  transfers between devices with their start and end apart: 15, of which 9 were waited for; matrix products, arithmetic and copies ran while one was open for 0% of the time, Pallas kernels for 29%

profile of v7, /device:TPU:1, one launch (start us, length us, event | category | flops | bytes accessed | tf_op | source)
XLA Modules:
  0.0 139.0 jit_solution(1365279967989443565)
XLA Ops:
  0.6 3.5 %shard_map.113.own_ref = bf16[2,2,448,1024]{3,2,1,0:T(8,128)(2,1)} custom-call(s32[1]{0:T(128)} %bitcast.6.par_ref, bf16[448,2048]{1,0:T(8,128)(2,1)} %bitcast.38, bf16[448,2048]{1,0:T(8,128)(2,1)} %bitcast.39), custom_call_target="tpu_custom_call" | custom-call | bytes 3670020 | tf_op jit(solution)/shard_map/pallas_call | solution.py:41
  4.1 3.3 %collective-permute-start.2 = (bf16[2,2,448,1024]{3,2,1,0:T(8,128)(2,1)}, bf16[2,2,448,1024]{3,2,1,0:T(8,128)(2,1)}, u32[]{:S(2)}, u32[]{:S(2)}) collective-permute-start(bf16[2,2,448,1024]{3,2,1,0:T(8,128)(2,1)} %shard_map.113.own_ref), channel_id=1, source_target_pairs={{0,1},{1,0},{2,3},{3,2},{4,5},{5,4},{6,7},{7,6},{8,9},{9,8},{10,11... | collective-permute-start | bytes 11010056 | tf_op jit(solution)/shard_map/ppermute | solution.py:359
  7.4 2.3 %shard_map.112 = bf16[384,1024]{1,0:T(8,128)(2,1)} custom-call(s32[1]{0:T(128)} %bitcast.core_ref, s32[1]{0:T(128)} %bitcast.6.par_ref, s32[2,192]{1,0:T(2,128)} %bitcast.43, bf16[192,2048]{1,0:T(8,128)(2,1)} %tok_ref.1), custom_call_target="tpu_custom_call" | custom-call | flops 150994944 | bytes 787976 | tf_op jit(solution)/shard_map/pallas_call | solution.py:41
  9.7 5.1 %all-to-all-start.1 = ((bf16[16,24,1024]{2,1,0:T(8,128)(2,1)}), bf16[16,24,1024]{2,1,0:T(8,128)(2,1)S(1)}, u32[]{:S(2)}, u32[]{:S(2)}) async-start(bf16[16,24,1024]{2,1,0:T(8,128)(2,1)} %bitcast.35), calls=%async_computation.1 | async-start | bytes 1572864 | tf_op jit(solution)/shard_map/all_to_all | solution.py:365
  14.8 0.4 collective-permute-start.3
  15.2 0.9 shard_map.110.table_ref
  16.0 2.8 %shard_map.111 = bf16[384,2048]{1,0:T(8,128)(2,1)} custom-call(f32[8,192]{1,0:T(8,128)S(1)} %shard_map.110.table_ref, bf16[192,2048]{1,0:T(8,128)(2,1)} %cot_ref.1), custom_call_target="tpu_custom_call" | custom-call | flops 301989888 | bytes 792576 | tf_op jit(solution)/shard_map/pallas_call | solution.py:41
  18.9 9.7 %all-to-all-done.1 = bf16[16,24,1024]{2,1,0:T(8,128)(2,1)S(1)} async-done(((bf16[16,24,1024]{2,1,0:T(8,128)(2,1)}), bf16[16,24,1024]{2,1,0:T(8,128)(2,1)S(1)}, u32[]{:S(2)}, u32[]{:S(2)}) %all-to-all-start.1) | async-done | bytes 786464 | tf_op jit(solution)/shard_map/all_to_all | solution.py:365
  28.6 3.7 %all-to-all-start = ((bf16[16,24,2048]{2,1,0:T(8,128)(2,1)}), bf16[16,24,2048]{2,1,0:T(8,128)(2,1)S(1)}, u32[]{:S(2)}, u32[]{:S(2)}) async-start(bf16[16,24,2048]{2,1,0:T(8,128)(2,1)} %bitcast.33), calls=%async_computation | async-start | bytes 3145728 | tf_op jit(solution)/shard_map/all_to_all | solution.py:365
  32.3 0.1 fusion
  32.4 1.7 %collective-permute-start = (bf16[192,1024]{1,0:T(8,128)(2,1)S(1)}, bf16[192,1024]{1,0:T(8,128)(2,1)S(1)}, u32[]{:S(2)}, u32[]{:S(2)}) collective-permute-start(bf16[192,1024]{1,0:T(8,128)(2,1)S(1)} %bitcast.42), channel_id=1, source_target_pairs={{0,2},{2,4},{4,6},{6,8},{8,10},{10,12},{12,14},{14,0},{1,3},{3,5},... | collective-permute-start | bytes 1179656 | tf_op jit(solution)/shard_map/ppermute | solution.py:362
  34.1 4.0 %collective-permute-start.1 = (bf16[192,1024]{1,0:T(8,128)(2,1)S(1)}, bf16[192,1024]{1,0:T(8,128)(2,1)S(1)}, u32[]{:S(2)}, u32[]{:S(2)}) collective-permute-start(bf16[192,1024]{1,0:T(8,128)(2,1)S(1)} %bitcast.41), channel_id=1, source_target_pairs={{0,14},{2,0},{4,2},{6,4},{8,6},{10,8},{12,10},{14,12},{1,15},{3,1}... | collective-permute-start | bytes 1179656 | tf_op jit(solution)/shard_map/ppermute | solution.py:362
  38.2 1.5 %shard_map.115.down0_ref = bf16[448,2048]{1,0:T(8,128)(2,1)S(1)} custom-call(bf16[448,2048]{1,0:T(8,128)(2,1)} %bitcast.37), custom_call_target="tpu_custom_call" | custom-call | bytes 1835008 | tf_op jit(solution)/shard_map/pallas_call | solution.py:41
  39.7 6.4 %collective-permute-done.low_ref = bf16[192,1024]{1,0:T(8,128)(2,1)S(1)} collective-permute-done((bf16[192,1024]{1,0:T(8,128)(2,1)S(1)}, bf16[192,1024]{1,0:T(8,128)(2,1)S(1)}, u32[]{:S(2)}, u32[]{:S(2)}) %collective-permute-start) | collective-permute-done | bytes 393248 | tf_op jit(solution)/shard_map/ppermute | solution.py:362
  46.1 0.0 collective-permute-done.2.other_ref
  46.1 7.4 %shard_map.114 = (bf16[2,3,384,448]{3,2,1,0:T(8,128)(2,1)}, bf16[2,384,1024]{2,1,0:T(8,128)(2,1)}) custom-call(bf16[384,1024]{1,0:T(8,128)(2,1)S(1)} %bitcast.32, bf16[192,1024]{1,0:T(8,128)(2,1)S(1)} %collective-permute-done.low_ref, bf16[192,1024]{1,0:T(8,128)(2,1)S(1)} %collective-permute-done.1.high_ref, bf16[2,2,448,1024]{3,2,1,0:T(8,128)(2,1)} %shard_map.113.own_ref, ...), custom_call_target="tpu_custom_call" | custom-call | flops 2818572288 | bytes 8912896 | tf_op jit(solution)/shard_map/pallas_call | solution.py:41
  53.6 0.1 all-to-all-done
  53.7 3.4 %shard_map.124 = bf16[448,2048]{1,0:T(8,128)(2,1)} custom-call(bf16[384,2048]{1,0:T(8,128)(2,1)S(1)} %bitcast.28, bf16[2,3,384,448]{3,2,1,0:T(8,128)(2,1)} %get-tuple-element.23.mid_ref), custom_call_target="tpu_custom_call" | custom-call | flops 704643072 | bytes 3637248 | tf_op jit(solution)/shard_map/pallas_call | solution.py:41
  57.1 4.0 %collective-permute-start.12 = (bf16[448,2048]{1,0:T(8,128)(2,1)}, bf16[448,2048]{1,0:T(8,128)(2,1)S(1)}, u32[]{:S(2)}, u32[]{:S(2)}) collective-permute-start(bf16[448,2048]{1,0:T(8,128)(2,1)} %shard_map.124), channel_id=1, source_target_pairs={{0,1},{1,0},{2,3},{3,2},{4,5},{5,4},{6,7},{7,6},{8,9},{9,8},{10,11... | collective-permute-start | bytes 5505032 | tf_op jit(solution)/shard_map/ppermute | solution.py:359
  61.1 6.0 %shard_map.116 = (bf16[192,1152]{1,0:T(8,128)(2,1)S(1)}, bf16[192,1152]{1,0:T(8,128)(2,1)S(1)}, bf16[2,2,384,448]{3,2,1,0:T(8,128)(2,1)}, f32[384,128]{1,0:T(8,128)S(1)}) custom-call(bf16[384,2048]{1,0:T(8,128)(2,1)S(1)} %bitcast.29, bf16[2,3,384,448]{3,2,1,0:T(8,128)(2,1)} %get-tuple-element.23.mid_ref, bf16[448,2048]{1,0:T(8,128)(2,1)S(1)} %shard_map.115.down0_ref, ...), custom_call_target="tpu_custom_call" | custom-call | flops 2818572288 | bytes 14647296 | tf_op jit(solution)/shard_map/pallas_call | solution.py:41
  67.0 5.3 %shard_map.122 = (bf16[448,2048]{1,0:T(8,128)(2,1)}, bf16[448,2048]{1,0:T(8,128)(2,1)}) custom-call(s32[1]{0:T(128)} %bitcast.6.par_ref, bf16[2,384,1024]{2,1,0:T(8,128)(2,1)} %get-tuple-element.36.sides_ref, bf16[2,2,384,448]{3,2,1,0:T(8,128)(2,1)} %get-tuple-element.24.grads_ref), custom_call_target="tpu_custom_call" | custom-call | flops 1409286144 | bytes 2949124 | tf_op jit(solution)/shard_map/pallas_call | solution.py:41
  72.3 0.1 collective-permute-start.10
  72.4 0.5 collective-permute-start.11
  72.9 5.6 %collective-permute-start.4 = (bf16[192,1152]{1,0:T(8,128)(2,1)S(1)}, bf16[192,1152]{1,0:T(8,128)(2,1)S(1)}, u32[]{:S(2)}, u32[]{:S(2)}) collective-permute-start(bf16[192,1152]{1,0:T(8,128)(2,1)S(1)} %get-tuple-element.26), channel_id=1, source_target_pairs={{0,14},{2,0},{4,2},{6,4},{8,6},{10,8},{12,10},{14,12},{1,15},{3,1}... | collective-permute-start | bytes 1327112 | tf_op jit(solution)/shard_map/ppermute | solution.py:362
  78.5 0.0 collective-permute-start.5
  78.5 4.3 %shard_map.117.own_ref = f32[384,1152]{1,0:T(8,128)S(1)} custom-call(bf16[2,2,384,448]{3,2,1,0:T(8,128)(2,1)} %get-tuple-element.24.grads_ref, f32[384,128]{1,0:T(8,128)S(1)} %get-tuple-element.25.gate_ref, bf16[2,2,448,1024]{3,2,1,0:T(8,128)(2,1)} %shard_map.113.own_ref, bf16[2,2,448,1024]{3,2,1,0:T(8,128)(2,1)} %collective-permute-done.2.other_ref), custom_call_target="tpu_custom_call" | custom-call | flops 1409286144 | bytes 8912896 | tf_op jit(solution)/shard_map/pallas_call | solution.py:41
  82.8 5.1 %collective-permute-done.4.low_ref = bf16[192,1152]{1,0:T(8,128)(2,1)S(1)} collective-permute-done((bf16[192,1152]{1,0:T(8,128)(2,1)S(1)}, bf16[192,1152]{1,0:T(8,128)(2,1)S(1)}, u32[]{:S(2)}, u32[]{:S(2)}) %collective-permute-start.4) | collective-permute-done | bytes 442400 | tf_op jit(solution)/shard_map/ppermute | solution.py:362
  87.9 3.1 %collective-permute-done.5.high_ref = bf16[192,1152]{1,0:T(8,128)(2,1)S(1)} collective-permute-done((bf16[192,1152]{1,0:T(8,128)(2,1)S(1)}, bf16[192,1152]{1,0:T(8,128)(2,1)S(1)}, u32[]{:S(2)}, u32[]{:S(2)}) %collective-permute-start.5) | collective-permute-done | bytes 442400 | tf_op jit(solution)/shard_map/ppermute | solution.py:362
  91.1 1.0 shard_map.118
  92.1 17.9 %all_to_all.15 = bf16[16,24,1152]{2,1,0:T(8,128)(2,1)S(1)} all-to-all(bf16[16,24,1152]{2,1,0:T(8,128)(2,1)} %bitcast.34), channel_id=1, replica_groups=mesh['y'=4,'x'=4,'zh'=4,'zl'=2,'c'=2] {'y','x'}, dimensions={0} | all-to-all | bytes 1769472 | tf_op jit(solution)/shard_map/all_to_all | solution.py:365
  110.0 0.4 shard_map.119
  110.5 2.1 %collective-permute-start.6 = (bf16[4,208,128]{2,1,0:T(8,128)(2,1)S(1)}, bf16[4,208,128]{2,1,0:T(8,128)(2,1)S(1)}, u32[]{:S(2)}, u32[]{:S(2)}) collective-permute-start(bf16[4,208,128]{2,1,0:T(8,128)(2,1)S(1)} %get-tuple-element.29), channel_id=1, source_target_pairs={{0,1},{1,0},{2,3},{3,2},{4,5},{5,4},{6,7},{7,6},{8,9},{9,8},{10,11... | collective-permute-start | bytes 638984 | tf_op jit(solution)/shard_map/ppermute | solution.py:359
  112.6 1.1 collective-permute-done.6.got_ref
  113.7 0.1 shard_map.120
  113.7 0.1 collective-permute-start.7
  113.8 2.5 %collective-permute-start.8 = (bf16[208,128]{1,0:T(8,128)(2,1)S(1)}, bf16[208,128]{1,0:T(8,128)(2,1)S(1)}, u32[]{:S(2)}, u32[]{:S(2)}) collective-permute-start(bf16[208,128]{1,0:T(8,128)(2,1)S(1)} %get-tuple-element.32), channel_id=1, source_target_pairs={{0,8},{2,10},{4,12},{6,14},{8,0},{10,2},{12,4},{14,6},{1,9},{3,11}... | collective-permute-start | bytes 159752 | tf_op jit(solution)/shard_map/ppermute | solution.py:362
  116.3 4.3 %collective-permute-done.7.refs_1_ = bf16[208,128]{1,0:T(8,128)(2,1)S(1)} collective-permute-done((bf16[208,128]{1,0:T(8,128)(2,1)S(1)}, bf16[208,128]{1,0:T(8,128)(2,1)S(1)}, u32[]{:S(2)}, u32[]{:S(2)}) %collective-permute-start.7) | collective-permute-done | bytes 53280 | tf_op jit(solution)/shard_map/ppermute | solution.py:362
  120.6 0.0 collective-permute-start.9
  120.6 0.3 collective-permute-done.8.refs_2_
  120.9 3.6 %collective-permute-done.9.refs_3_ = bf16[208,128]{1,0:T(8,128)(2,1)S(1)} collective-permute-done((bf16[208,128]{1,0:T(8,128)(2,1)S(1)}, bf16[208,128]{1,0:T(8,128)(2,1)S(1)}, u32[]{:S(2)}, u32[]{:S(2)}) %collective-permute-start.9) | collective-permute-done | bytes 53280 | tf_op jit(solution)/shard_map/ppermute | solution.py:362
  124.5 0.7 shard_map.121
  125.1 0.0 collective-permute-done.12.refs_0_
  125.1 1.2 copy-done.2
  126.4 4.0 %shard_map.125 = bf16[448,2048]{1,0:T(8,128)(2,1)} custom-call(bf16[384,2048]{1,0:T(8,128)(2,1)S(1)} %bitcast.30, bf16[2,3,384,448]{3,2,1,0:T(8,128)(2,1)} %get-tuple-element.23.mid_ref, bf16[448,2048]{1,0:T(8,128)(2,1)} %copy-done.2), custom_call_target="tpu_custom_call" | custom-call | flops 704643072 | bytes 5472256 | tf_op jit(solution)/shard_map/pallas_call | solution.py:41
  130.4 0.0 collective-permute-done.10.refs_0_
  130.5 1.2 copy-done.3
  131.7 1.2 copy-done.4
  132.9 5.9 %shard_map.123 = (bf16[448,2048]{1,0:T(8,128)(2,1)}, bf16[448,2048]{1,0:T(8,128)(2,1)}) custom-call(s32[1]{0:T(128)} %bitcast.6.par_ref, bf16[2,384,1024]{2,1,0:T(8,128)(2,1)} %get-tuple-element.36.sides_ref, bf16[2,2,384,448]{3,2,1,0:T(8,128)(2,1)} %get-tuple-element.24.grads_ref, bf16[448,2048]{1,0:T(8,128)(2,1)} %copy-done.3, bf16[448,2048]{1,0:T(8,128)(2,1)} %copy-done.4), custom_call_target="tpu_custom_call" | custom-call | flops 1409286144 | bytes 6619140 | tf_op jit(solution)/shard_map/pallas_call | solution.py:41
  (10 shorter events, 0.0 us)
Async XLA Ops:
  4.1 42.0 %collective-permute-start.2 = (bf16[2,2,448,1024]{3,2,1,0:T(8,128)(2,1)}, bf16[2,2,448,1024]{3,2,1,0:T(8,128)(2,1)}, u32[]{:S(2)}, u32[]{:S(2)}) collective-permute-start(bf16[2,2,448,1024]{3,2,1,0:T(8,128)(2,1)} %shard_map.113.own_ref), channel_id=1, source_target_pairs={{0,1},{1,0},{2,3},{3,2},{4,5},{5,4},{6,7},{7,6},{8,9},{9,8},{10,11... | collective-permute-start | bytes 11010056 | tf_op jit(solution)/shard_map/ppermute | solution.py:359
  9.7 18.9 %all-to-all-start.1 = ((bf16[16,24,1024]{2,1,0:T(8,128)(2,1)}), bf16[16,24,1024]{2,1,0:T(8,128)(2,1)S(1)}, u32[]{:S(2)}, u32[]{:S(2)}) async-start(bf16[16,24,1024]{2,1,0:T(8,128)(2,1)} %bitcast.35), calls=%async_computation.1 | async-start | bytes 1572864 | tf_op jit(solution)/shard_map/all_to_all | solution.py:365
  14.8 46.3 %collective-permute-start.3 = (bf16[448,2048]{1,0:T(8,128)(2,1)}, bf16[448,2048]{1,0:T(8,128)(2,1)}, u32[]{:S(2)}, u32[]{:S(2)}) collective-permute-start(bf16[448,2048]{1,0:T(8,128)(2,1)} %bitcast.36), channel_id=1, source_target_pairs={{0,1},{1,0},{2,3},{3,2},{4,5},{5,4},{6,7},{7,6},{8,9},{9,8},{10,11... | collective-permute-start | bytes 5505032 | tf_op jit(solution)/shard_map/ppermute | solution.py:359
  28.6 3.8 %copy-start = (bf16[16,24,1024]{2,1,0:T(8,128)(2,1)}, bf16[16,24,1024]{2,1,0:T(8,128)(2,1)S(1)}, u32[]{:S(2)}) copy-start(bf16[16,24,1024]{2,1,0:T(8,128)(2,1)S(1)} %all-to-all-done.1) | copy-start | bytes 2359300
  28.6 25.1 %all-to-all-start = ((bf16[16,24,2048]{2,1,0:T(8,128)(2,1)}), bf16[16,24,2048]{2,1,0:T(8,128)(2,1)S(1)}, u32[]{:S(2)}, u32[]{:S(2)}) async-start(bf16[16,24,2048]{2,1,0:T(8,128)(2,1)} %bitcast.33), calls=%async_computation | async-start | bytes 3145728 | tf_op jit(solution)/shard_map/all_to_all | solution.py:365
  32.4 13.7 %collective-permute-start = (bf16[192,1024]{1,0:T(8,128)(2,1)S(1)}, bf16[192,1024]{1,0:T(8,128)(2,1)S(1)}, u32[]{:S(2)}, u32[]{:S(2)}) collective-permute-start(bf16[192,1024]{1,0:T(8,128)(2,1)S(1)} %bitcast.42), channel_id=1, source_target_pairs={{0,2},{2,4},{4,6},{6,8},{8,10},{10,12},{12,14},{14,0},{1,3},{3,5},... | collective-permute-start | bytes 1179656 | tf_op jit(solution)/shard_map/ppermute | solution.py:362
  34.1 12.0 %copy-start.1 = (bf16[16,24,1024]{2,1,0:T(8,128)(2,1)S(1)}, bf16[16,24,1024]{2,1,0:T(8,128)(2,1)}, u32[]{:S(2)}) copy-start(bf16[16,24,1024]{2,1,0:T(8,128)(2,1)} %copy-done) | copy-start | bytes 2359300
  34.1 12.0 %collective-permute-start.1 = (bf16[192,1024]{1,0:T(8,128)(2,1)S(1)}, bf16[192,1024]{1,0:T(8,128)(2,1)S(1)}, u32[]{:S(2)}, u32[]{:S(2)}) collective-permute-start(bf16[192,1024]{1,0:T(8,128)(2,1)S(1)} %bitcast.41), channel_id=1, source_target_pairs={{0,14},{2,0},{4,2},{6,4},{8,6},{10,8},{12,10},{14,12},{1,15},{3,1}... | collective-permute-start | bytes 1179656 | tf_op jit(solution)/shard_map/ppermute | solution.py:362
  57.1 68.1 %collective-permute-start.12 = (bf16[448,2048]{1,0:T(8,128)(2,1)}, bf16[448,2048]{1,0:T(8,128)(2,1)S(1)}, u32[]{:S(2)}, u32[]{:S(2)}) collective-permute-start(bf16[448,2048]{1,0:T(8,128)(2,1)} %shard_map.124), channel_id=1, source_target_pairs={{0,1},{1,0},{2,3},{3,2},{4,5},{5,4},{6,7},{7,6},{8,9},{9,8},{10,11... | collective-permute-start | bytes 5505032 | tf_op jit(solution)/shard_map/ppermute | solution.py:359
  72.3 58.1 %collective-permute-start.10 = (bf16[448,2048]{1,0:T(8,128)(2,1)}, bf16[448,2048]{1,0:T(8,128)(2,1)S(1)}, u32[]{:S(2)}, u32[]{:S(2)}) collective-permute-start(bf16[448,2048]{1,0:T(8,128)(2,1)} %get-tuple-element.37), channel_id=1, source_target_pairs={{0,1},{1,0},{2,3},{3,2},{4,5},{5,4},{6,7},{7,6},{8,9},{9,8},{10,11... | collective-permute-start | bytes 5505032 | tf_op jit(solution)/shard_map/ppermute | solution.py:359
  72.4 58.0 %collective-permute-start.11 = (bf16[448,2048]{1,0:T(8,128)(2,1)}, bf16[448,2048]{1,0:T(8,128)(2,1)S(1)}, u32[]{:S(2)}, u32[]{:S(2)}) collective-permute-start(bf16[448,2048]{1,0:T(8,128)(2,1)} %get-tuple-element.38), channel_id=1, source_target_pairs={{0,1},{1,0},{2,3},{3,2},{4,5},{5,4},{6,7},{7,6},{8,9},{9,8},{10,11... | collective-permute-start | bytes 5505032 | tf_op jit(solution)/shard_map/ppermute | solution.py:359
  72.9 15.0 %collective-permute-start.4 = (bf16[192,1152]{1,0:T(8,128)(2,1)S(1)}, bf16[192,1152]{1,0:T(8,128)(2,1)S(1)}, u32[]{:S(2)}, u32[]{:S(2)}) collective-permute-start(bf16[192,1152]{1,0:T(8,128)(2,1)S(1)} %get-tuple-element.26), channel_id=1, source_target_pairs={{0,14},{2,0},{4,2},{6,4},{8,6},{10,8},{12,10},{14,12},{1,15},{3,1}... | collective-permute-start | bytes 1327112 | tf_op jit(solution)/shard_map/ppermute | solution.py:362
  78.5 12.6 %collective-permute-start.5 = (bf16[192,1152]{1,0:T(8,128)(2,1)S(1)}, bf16[192,1152]{1,0:T(8,128)(2,1)S(1)}, u32[]{:S(2)}, u32[]{:S(2)}) collective-permute-start(bf16[192,1152]{1,0:T(8,128)(2,1)S(1)} %get-tuple-element.27), channel_id=1, source_target_pairs={{0,2},{2,4},{4,6},{6,8},{8,10},{10,12},{12,14},{14,0},{1,3},{3,5},... | collective-permute-start | bytes 1327112 | tf_op jit(solution)/shard_map/ppermute | solution.py:362
  110.5 3.2 %collective-permute-start.6 = (bf16[4,208,128]{2,1,0:T(8,128)(2,1)S(1)}, bf16[4,208,128]{2,1,0:T(8,128)(2,1)S(1)}, u32[]{:S(2)}, u32[]{:S(2)}) collective-permute-start(bf16[4,208,128]{2,1,0:T(8,128)(2,1)S(1)} %get-tuple-element.29), channel_id=1, source_target_pairs={{0,1},{1,0},{2,3},{3,2},{4,5},{5,4},{6,7},{7,6},{8,9},{9,8},{10,11... | collective-permute-start | bytes 638984 | tf_op jit(solution)/shard_map/ppermute | solution.py:359
  113.7 6.9 %collective-permute-start.7 = (bf16[208,128]{1,0:T(8,128)(2,1)S(1)}, bf16[208,128]{1,0:T(8,128)(2,1)S(1)}, u32[]{:S(2)}, u32[]{:S(2)}) collective-permute-start(bf16[208,128]{1,0:T(8,128)(2,1)S(1)} %get-tuple-element.31), channel_id=1, source_target_pairs={{0,4},{2,6},{4,8},{6,10},{8,12},{10,14},{12,0},{14,2},{1,5},{3,7},... | collective-permute-start | bytes 159752 | tf_op jit(solution)/shard_map/ppermute | solution.py:362
  113.8 7.1 %collective-permute-start.8 = (bf16[208,128]{1,0:T(8,128)(2,1)S(1)}, bf16[208,128]{1,0:T(8,128)(2,1)S(1)}, u32[]{:S(2)}, u32[]{:S(2)}) collective-permute-start(bf16[208,128]{1,0:T(8,128)(2,1)S(1)} %get-tuple-element.32), channel_id=1, source_target_pairs={{0,8},{2,10},{4,12},{6,14},{8,0},{10,2},{12,4},{14,6},{1,9},{3,11}... | collective-permute-start | bytes 159752 | tf_op jit(solution)/shard_map/ppermute | solution.py:362
  120.6 3.9 %collective-permute-start.9 = (bf16[208,128]{1,0:T(8,128)(2,1)S(1)}, bf16[208,128]{1,0:T(8,128)(2,1)S(1)}, u32[]{:S(2)}, u32[]{:S(2)}) collective-permute-start(bf16[208,128]{1,0:T(8,128)(2,1)S(1)} %get-tuple-element.33), channel_id=1, source_target_pairs={{0,12},{2,14},{4,0},{6,2},{8,4},{10,6},{12,8},{14,10},{1,13},{3,15... | collective-permute-start | bytes 159752 | tf_op jit(solution)/shard_map/ppermute | solution.py:362
  125.1 1.2 copy-start.2
  130.4 1.2 copy-start.3
  131.7 1.2 copy-start.4

commit v8 on v7

--- a/solution.py
+++ b/solution.py
@@ -255,19 +255,28 @@
         copy.wait()
 
 
-def row_grads(p, par_ref, sides_ref, grads_ref, *refs):
-    inputs = refs[:2] if p == 0 else ()
-    outs, scratch = refs[len(inputs) : len(inputs) + 2], refs[len(inputs) + 2 :]
-    sides, side_sem, left, left_sem, made, out_sem, *got = scratch
+def start_all(copies):
+    for copy in copies:
+        copy.start()
+    return copies
+
+
+def start_rows(p, sides_ref, grads_ref, inputs, scratch):
+    sides, side_sem, left, left_sem, _, _, *got = scratch
     keep = [pltpu.make_async_copy(sides_ref.at[k], sides.at[k], side_sem.at[k]) for k in range(2)]
     copies = [pltpu.make_async_copy(grads_ref.at[p, n], left.at[n], left_sem.at[n]) for n in range(2)]
     received = [pltpu.make_async_copy(r, got[0].at[n], got[1].at[n]) for n, r in enumerate(inputs)]
-    for copy in (copies[0], *keep, copies[1], *received):
-        copy.start()
+    start_all([copies[0], *keep, copies[1], *received])
+    return keep, copies, received
+
+
+def finish_rows(par_ref, started, outs, scratch):
+    keep, copies, received = started
+    sides, _, left, _, made, out_sem, *got = scratch
     done = []
     for n in range(2):
         copies[n].wait()
-        if p == 0:
+        if received:
             received[n].wait()
         for k, side in enumerate((par_ref[0], 1 - par_ref[0])):
             if n == 0:
@@ -275,30 +284,49 @@
             grad = dot(left[n], sides[k], TN)
             for to, cols in side_columns(side, made.shape[2]):
                 piece = grad[:, to]
-                if p == 0:
+                if received:
                     piece = piece + got[0][n, :, cols].astype(F32)
                 made[n, :, cols] = piece.astype(BF16)
-        done.append(pltpu.make_async_copy(made.at[n], outs[n], out_sem.at[n]))
-        done[-1].start()
-    for copy in done:
-        copy.wait()
-
-
-def down_grads(p, cot_ref, mid_ref, *refs):
-    inputs, (out_ref, left, sem, made, out_sem, *got) = (refs[:1], refs[1:]) if p == 0 else ((), refs)
+        done += start_all([pltpu.make_async_copy(made.at[n], outs[n], out_sem.at[n])])
+    return done
+
+
+def start_down(p, mid_ref, inputs, scratch):
+    left, sem, _, _, *got = scratch
     copies = [pltpu.make_async_copy(mid_ref.at[p, 0], left, sem)]
-    copies += [pltpu.make_async_copy(r, got[0], got[1]) for r in inputs]
-    for copy in copies:
-        copy.start()
-    for copy in copies:
+    return start_all(copies + [pltpu.make_async_copy(r, got[0], got[1]) for r in inputs])
+
+
+def finish_down(cot_ref, started, out_ref, scratch):
+    left, _, made, out_sem, *got = scratch
+    for copy in started:
         copy.wait()
     grad = dot(left[...], cot_ref[...], TN)
-    if p == 0:
+    if got:
         grad += got[0][...].astype(F32)
     made[...] = grad.astype(BF16)
-    done = pltpu.make_async_copy(made, out_ref, out_sem)
-    done.start()
-    done.wait()
+    return start_all([pltpu.make_async_copy(made, out_ref, out_sem)])
+
+
+def their_down_grads(cot_ref, mid_ref, out_ref, *scratch):
+    for copy in finish_down(cot_ref, start_down(1, mid_ref, (), scratch), out_ref, scratch):
+        copy.wait()
+
+
+def middle_grads(par_ref, sides_ref, grads_ref, cot_ref, mid_ref, got_ref, gate_ref, up_ref, down_ref, *scratch):
+    rows, down = scratch[:6], scratch[6:]
+    started = start_rows(1, sides_ref, grads_ref, (), rows)
+    down_started = start_down(0, mid_ref, (got_ref,), down)
+    done = finish_rows(par_ref, started, (gate_ref, up_ref), rows)
+    done += finish_down(cot_ref, down_started, down_ref, down)
+    for copy in done:
+        copy.wait()
+
+
+def own_row_grads(par_ref, sides_ref, grads_ref, got0_ref, got1_ref, gate_ref, up_ref, *scratch):
+    started = start_rows(0, sides_ref, grads_ref, (got0_ref, got1_ref), scratch)
+    for copy in finish_rows(par_ref, started, (gate_ref, up_ref), scratch):
+        copy.wait()
 
 
 def combine(core_ref, table_ref, x_ref, keep_ref, send_ref):
@@ -453,21 +481,14 @@
     down_args = [(cot, "v"), (mid, "h")]
     down_room = [pltpu.VMEM((count, ff), BF16), one, pltpu.VMEM((ff, width), BF16), one]
     cost = 2 * count * width * ff
-    (their_down,) = call(
-        functools.partial(down_grads, 1), [shard], *down_args,
-        scratch=down_room, flops=cost, mib=10,
-    )
-    theirs = call(
-        functools.partial(row_grads, 1), [shard] * 2, *row_args,
-        scratch=row_room, flops=2 * cost, mib=14,
-    )
-    (grad_down,) = call(
-        functools.partial(down_grads, 0), [shard], *down_args, (swap(their_down), "h"),
-        scratch=[*down_room, down_room[2], one], flops=cost, mib=12,
+    (their_down,) = call(their_down_grads, [shard], *down_args, scratch=down_room, flops=cost, mib=10)
+    *theirs, grad_down = call(
+        middle_grads, [shard] * 3, *row_args, *down_args, (swap(their_down), "h"),
+        scratch=[*row_room, *down_room, down_room[2], one], flops=3 * cost, mib=20,
     )
     received = [(swap(g), "h") for g in theirs]
     grad_gate, grad_up = call(
-        functools.partial(row_grads, 0), [shard] * 2, *row_args, *received,
+        own_row_grads, [shard] * 2, *row_args, *received,
         scratch=[*row_room, pair_room, dma(2)], flops=2 * cost, mib=18,
     )
 

time: 140 us -> 138 us (0.986)
  starting transfers between devices: 33.1 us -> 37.9 us
  waiting for transfers between devices: 33.8 us -> 30.5 us
  Pallas kernels: 49.5 us -> 46.6 us
    ppermute x7, waiting for transfers between devices: 22.8 us -> 19.2 us  [shift(): return lax.ppermute(v, Z, [(i, (i + k) % depth) for i in range(depth)])]
    ppermute x7, starting transfers between devices: 13.9 us -> 17.4 us  [shift(): return lax.ppermute(v, Z, [(i, (i + k) % depth) for i in range(depth)])]
    pallas_call x16 -> x15, Pallas kernels: 49.5 us -> 46.6 us  [call(): kernel_call(*(a if m == 's' else pltpu.with_memory_space_constraint(a, pl...]
    unnamed x10 -> x6, local copies, waits for them, and re-layouts: 3.7 us -> 3.68 us
  transfers between devices with their start and end apart: 15 -> 15, of which waited for: 9 -> 9; matrix products, arithmetic and copies ran while one was open for 0% -> 0% of each run, Pallas kernels for 29% -> 22%
where the time goes in v8:
time: 138 us
  Pallas kernels  46.6 us (34%)
  starting transfers between devices  37.9 us (27%)
  waiting for transfers between devices  30.5 us (22%)
  blocking collectives  17.9 us (13%)
  local copies, waits for them, and re-layouts  3.73 us (3%)
    pallas_call x15, Pallas kernels, call(): kernel_call(*(a if m == 's' else pltpu.with_memory_space_constraint(a, pl...  46.6 us
    ppermute x7, waiting for transfers between devices, shift(): return lax.ppermute(v, Z, [(i, (i + k) % depth) for i in range(depth)])  19.2 us
    all_to_all x1, blocking collectives, exchange(): return lax.all_to_all(v, EP, split_axis=0, concat_axis=0, tiled=True)  17.9 us
    ppermute x7, starting transfers between devices, shift(): return lax.ppermute(v, Z, [(i, (i + k) % depth) for i in range(depth)])  17.4 us
    ppermute x6, starting transfers between devices, swap(): return lax.ppermute(v, 'c', [(0, 1), (1, 0)])  11.7 us
    all_to_all x2, waiting for transfers between devices, exchange(): return lax.all_to_all(v, EP, split_axis=0, concat_axis=0, tiled=True)  10.2 us
    all_to_all x2, starting transfers between devices, exchange(): return lax.all_to_all(v, EP, split_axis=0, concat_axis=0, tiled=True)  8.77 us
    unnamed x6, local copies, waits for them, and re-layouts  3.68 us
  transfers between devices with their start and end apart: 15, of which 9 were waited for; matrix products, arithmetic and copies ran while one was open for 0% of the time, Pallas kernels for 22%

profile of v8, /device:TPU:1, one launch (start us, length us, event | category | flops | bytes accessed | tf_op | source)
XLA Modules:
  0.0 137.7 jit_solution(13723880378726718741)
XLA Ops:
  0.6 3.5 %shard_map.113.own_ref = bf16[2,2,448,1024]{3,2,1,0:T(8,128)(2,1)} custom-call(s32[1]{0:T(128)} %bitcast.6.par_ref, bf16[448,2048]{1,0:T(8,128)(2,1)} %bitcast.38, bf16[448,2048]{1,0:T(8,128)(2,1)} %bitcast.39), custom_call_target="tpu_custom_call" | custom-call | bytes 3670020 | tf_op jit(solution)/shard_map/pallas_call | solution.py:41
  4.1 3.3 %collective-permute-start.2 = (bf16[2,2,448,1024]{3,2,1,0:T(8,128)(2,1)}, bf16[2,2,448,1024]{3,2,1,0:T(8,128)(2,1)}, u32[]{:S(2)}, u32[]{:S(2)}) collective-permute-start(bf16[2,2,448,1024]{3,2,1,0:T(8,128)(2,1)} %shard_map.113.own_ref), channel_id=1, source_target_pairs={{0,1},{1,0},{2,3},{3,2},{4,5},{5,4},{6,7},{7,6},{8,9},{9,8},{10,11... | collective-permute-start | bytes 11010056 | tf_op jit(solution)/shard_map/ppermute | solution.py:387
  7.4 2.3 %shard_map.112 = bf16[384,1024]{1,0:T(8,128)(2,1)} custom-call(s32[1]{0:T(128)} %bitcast.core_ref, s32[1]{0:T(128)} %bitcast.6.par_ref, s32[2,192]{1,0:T(2,128)} %bitcast.42, bf16[192,2048]{1,0:T(8,128)(2,1)} %tok_ref.1), custom_call_target="tpu_custom_call" | custom-call | flops 150994944 | bytes 787976 | tf_op jit(solution)/shard_map/pallas_call | solution.py:41
  9.7 5.1 %all-to-all-start.1 = ((bf16[16,24,1024]{2,1,0:T(8,128)(2,1)}), bf16[16,24,1024]{2,1,0:T(8,128)(2,1)S(1)}, u32[]{:S(2)}, u32[]{:S(2)}) async-start(bf16[16,24,1024]{2,1,0:T(8,128)(2,1)} %bitcast.35), calls=%async_computation.1 | async-start | bytes 1572864 | tf_op jit(solution)/shard_map/all_to_all | solution.py:393
  14.8 0.9 shard_map.110.table_ref
  15.6 2.8 %shard_map.111 = bf16[384,2048]{1,0:T(8,128)(2,1)} custom-call(f32[8,192]{1,0:T(8,128)S(1)} %shard_map.110.table_ref, bf16[192,2048]{1,0:T(8,128)(2,1)} %cot_ref.1), custom_call_target="tpu_custom_call" | custom-call | flops 301989888 | bytes 792576 | tf_op jit(solution)/shard_map/pallas_call | solution.py:41
  18.5 10.1 %all-to-all-done.1 = bf16[16,24,1024]{2,1,0:T(8,128)(2,1)S(1)} async-done(((bf16[16,24,1024]{2,1,0:T(8,128)(2,1)}), bf16[16,24,1024]{2,1,0:T(8,128)(2,1)S(1)}, u32[]{:S(2)}, u32[]{:S(2)}) %all-to-all-start.1) | async-done | bytes 786464 | tf_op jit(solution)/shard_map/all_to_all | solution.py:393
  28.6 3.7 %all-to-all-start = ((bf16[16,24,2048]{2,1,0:T(8,128)(2,1)}), bf16[16,24,2048]{2,1,0:T(8,128)(2,1)S(1)}, u32[]{:S(2)}, u32[]{:S(2)}) async-start(bf16[16,24,2048]{2,1,0:T(8,128)(2,1)} %bitcast.33), calls=%async_computation | async-start | bytes 3145728 | tf_op jit(solution)/shard_map/all_to_all | solution.py:393
  32.3 0.1 fusion
  32.4 1.7 %collective-permute-start = (bf16[192,1024]{1,0:T(8,128)(2,1)S(1)}, bf16[192,1024]{1,0:T(8,128)(2,1)S(1)}, u32[]{:S(2)}, u32[]{:S(2)}) collective-permute-start(bf16[192,1024]{1,0:T(8,128)(2,1)S(1)} %bitcast.41), channel_id=1, source_target_pairs={{0,2},{2,4},{4,6},{6,8},{8,10},{10,12},{12,14},{14,0},{1,3},{3,5},... | collective-permute-start | bytes 1179656 | tf_op jit(solution)/shard_map/ppermute | solution.py:390
  34.1 4.0 %collective-permute-start.1 = (bf16[192,1024]{1,0:T(8,128)(2,1)S(1)}, bf16[192,1024]{1,0:T(8,128)(2,1)S(1)}, u32[]{:S(2)}, u32[]{:S(2)}) collective-permute-start(bf16[192,1024]{1,0:T(8,128)(2,1)S(1)} %bitcast.40), channel_id=1, source_target_pairs={{0,14},{2,0},{4,2},{6,4},{8,6},{10,8},{12,10},{14,12},{1,15},{3,1}... | collective-permute-start | bytes 1179656 | tf_op jit(solution)/shard_map/ppermute | solution.py:390
  38.1 1.7 %collective-permute-start.3 = (bf16[448,2048]{1,0:T(8,128)(2,1)}, bf16[448,2048]{1,0:T(8,128)(2,1)}, u32[]{:S(2)}, u32[]{:S(2)}) collective-permute-start(bf16[448,2048]{1,0:T(8,128)(2,1)} %bitcast.36), channel_id=1, source_target_pairs={{0,1},{1,0},{2,3},{3,2},{4,5},{5,4},{6,7},{7,6},{8,9},{9,8},{10,11... | collective-permute-start | bytes 5505032 | tf_op jit(solution)/shard_map/ppermute | solution.py:387
  39.9 6.2 %collective-permute-done.low_ref = bf16[192,1024]{1,0:T(8,128)(2,1)S(1)} collective-permute-done((bf16[192,1024]{1,0:T(8,128)(2,1)S(1)}, bf16[192,1024]{1,0:T(8,128)(2,1)S(1)}, u32[]{:S(2)}, u32[]{:S(2)}) %collective-permute-start) | collective-permute-done | bytes 393248 | tf_op jit(solution)/shard_map/ppermute | solution.py:390
  46.1 0.0 collective-permute-done.1.high_ref
  46.1 0.0 collective-permute-done.2.other_ref
  46.1 7.4 %shard_map.114 = (bf16[2,3,384,448]{3,2,1,0:T(8,128)(2,1)}, bf16[2,384,1024]{2,1,0:T(8,128)(2,1)}) custom-call(bf16[384,1024]{1,0:T(8,128)(2,1)S(1)} %bitcast.32, bf16[192,1024]{1,0:T(8,128)(2,1)S(1)} %collective-permute-done.low_ref, bf16[192,1024]{1,0:T(8,128)(2,1)S(1)} %collective-permute-done.1.high_ref, bf16[2,2,448,1024]{3,2,1,0:T(8,128)(2,1)} %shard_map.113.own_ref, ...), custom_call_target="tpu_custom_call" | custom-call | flops 2818572288 | bytes 8912896 | tf_op jit(solution)/shard_map/pallas_call | solution.py:41
  53.5 0.1 all-to-all-done
  53.7 3.4 %shard_map.122 = bf16[448,2048]{1,0:T(8,128)(2,1)} custom-call(bf16[384,2048]{1,0:T(8,128)(2,1)S(1)} %bitcast.28, bf16[2,3,384,448]{3,2,1,0:T(8,128)(2,1)} %get-tuple-element.24.mid_ref), custom_call_target="tpu_custom_call" | custom-call | flops 704643072 | bytes 3637248 | tf_op jit(solution)/shard_map/pallas_call | solution.py:41
  57.0 4.0 %collective-permute-start.10 = (bf16[448,2048]{1,0:T(8,128)(2,1)}, bf16[448,2048]{1,0:T(8,128)(2,1)S(1)}, u32[]{:S(2)}, u32[]{:S(2)}) collective-permute-start(bf16[448,2048]{1,0:T(8,128)(2,1)} %shard_map.122), channel_id=1, source_target_pairs={{0,1},{1,0},{2,3},{3,2},{4,5},{5,4},{6,7},{7,6},{8,9},{9,8},{10,11... | collective-permute-start | bytes 5505032 | tf_op jit(solution)/shard_map/ppermute | solution.py:387
  61.0 1.5 %shard_map.115.down0_ref = bf16[448,2048]{1,0:T(8,128)(2,1)S(1)} custom-call(bf16[448,2048]{1,0:T(8,128)(2,1)} %bitcast.37), custom_call_target="tpu_custom_call" | custom-call | bytes 1835008 | tf_op jit(solution)/shard_map/pallas_call | solution.py:41
  62.6 6.0 %shard_map.116 = (bf16[192,1152]{1,0:T(8,128)(2,1)S(1)}, bf16[192,1152]{1,0:T(8,128)(2,1)S(1)}, bf16[2,2,384,448]{3,2,1,0:T(8,128)(2,1)}, f32[384,128]{1,0:T(8,128)S(1)}) custom-call(bf16[384,2048]{1,0:T(8,128)(2,1)S(1)} %bitcast.29, bf16[2,3,384,448]{3,2,1,0:T(8,128)(2,1)} %get-tuple-element.24.mid_ref, bf16[448,2048]{1,0:T(8,128)(2,1)S(1)} %shard_map.115.down0_ref, ...), custom_call_target="tpu_custom_call" | custom-call | flops 2818572288 | bytes 14647296 | tf_op jit(solution)/shard_map/pallas_call | solution.py:41
  68.5 0.0 collective-permute-done.10.got_ref
  68.5 0.0 copy-start.2
  68.6 1.2 copy-done.2
  69.8 6.5 %shard_map.123 = (bf16[448,2048]{1,0:T(8,128)(2,1)}, bf16[448,2048]{1,0:T(8,128)(2,1)}, bf16[448,2048]{1,0:T(8,128)(2,1)}) custom-call(s32[1]{0:T(128)} %bitcast.6.par_ref, bf16[2,384,1024]{2,1,0:T(8,128)(2,1)} %get-tuple-element.37.sides_ref, bf16[2,2,384,448]{3,2,1,0:T(8,128)(2,1)} %get-tuple-element.25.grads_ref, bf16[384,2048]{1,0:T(8,128)(2,1)S(1)} %bitcast.30, ...), custom_call_target="tpu_custom_call" | custom-call | flops 2113929216 | bytes 8421380 | tf_op jit(solution)/shard_map/pallas_call | solution.py:41
  76.2 0.1 collective-permute-start.11
  76.4 0.5 collective-permute-start.12
  76.8 5.6 %collective-permute-start.4 = (bf16[192,1152]{1,0:T(8,128)(2,1)S(1)}, bf16[192,1152]{1,0:T(8,128)(2,1)S(1)}, u32[]{:S(2)}, u32[]{:S(2)}) collective-permute-start(bf16[192,1152]{1,0:T(8,128)(2,1)S(1)} %get-tuple-element.27), channel_id=1, source_target_pairs={{0,14},{2,0},{4,2},{6,4},{8,6},{10,8},{12,10},{14,12},{1,15},{3,1}... | collective-permute-start | bytes 1327112 | tf_op jit(solution)/shard_map/ppermute | solution.py:390
  82.5 4.3 %shard_map.117.own_ref = f32[384,1152]{1,0:T(8,128)S(1)} custom-call(bf16[2,2,384,448]{3,2,1,0:T(8,128)(2,1)} %get-tuple-element.25.grads_ref, f32[384,128]{1,0:T(8,128)S(1)} %get-tuple-element.26.gate_ref, bf16[2,2,448,1024]{3,2,1,0:T(8,128)(2,1)} %shard_map.113.own_ref, bf16[2,2,448,1024]{3,2,1,0:T(8,128)(2,1)} %collective-permute-done.2.other_ref), custom_call_target="tpu_custom_call" | custom-call | flops 1409286144 | bytes 8912896 | tf_op jit(solution)/shard_map/pallas_call | solution.py:41
  86.8 5.1 %collective-permute-done.4.low_ref = bf16[192,1152]{1,0:T(8,128)(2,1)S(1)} collective-permute-done((bf16[192,1152]{1,0:T(8,128)(2,1)S(1)}, bf16[192,1152]{1,0:T(8,128)(2,1)S(1)}, u32[]{:S(2)}, u32[]{:S(2)}) %collective-permute-start.4) | collective-permute-done | bytes 442400 | tf_op jit(solution)/shard_map/ppermute | solution.py:390
  91.9 3.1 %collective-permute-done.5.high_ref = bf16[192,1152]{1,0:T(8,128)(2,1)S(1)} collective-permute-done((bf16[192,1152]{1,0:T(8,128)(2,1)S(1)}, bf16[192,1152]{1,0:T(8,128)(2,1)S(1)}, u32[]{:S(2)}, u32[]{:S(2)}) %collective-permute-start.5) | collective-permute-done | bytes 442400 | tf_op jit(solution)/shard_map/ppermute | solution.py:390
  95.0 1.0 shard_map.118
  96.0 17.9 %all_to_all.15 = bf16[16,24,1152]{2,1,0:T(8,128)(2,1)S(1)} all-to-all(bf16[16,24,1152]{2,1,0:T(8,128)(2,1)} %bitcast.34), channel_id=1, replica_groups=mesh['y'=4,'x'=4,'zh'=4,'zl'=2,'c'=2] {'y','x'}, dimensions={0} | all-to-all | bytes 1769472 | tf_op jit(solution)/shard_map/all_to_all | solution.py:393
  114.0 0.4 shard_map.119
  114.4 2.1 %collective-permute-start.6 = (bf16[4,208,128]{2,1,0:T(8,128)(2,1)S(1)}, bf16[4,208,128]{2,1,0:T(8,128)(2,1)S(1)}, u32[]{:S(2)}, u32[]{:S(2)}) collective-permute-start(bf16[4,208,128]{2,1,0:T(8,128)(2,1)S(1)} %get-tuple-element.30), channel_id=1, source_target_pairs={{0,1},{1,0},{2,3},{3,2},{4,5},{5,4},{6,7},{7,6},{8,9},{9,8},{10,11... | collective-permute-start | bytes 638984 | tf_op jit(solution)/shard_map/ppermute | solution.py:387
  116.5 1.1 collective-permute-done.6.got_ref
  117.6 0.1 shard_map.120
  117.7 0.1 collective-permute-start.7
  117.8 2.7 %collective-permute-start.8 = (bf16[208,128]{1,0:T(8,128)(2,1)S(1)}, bf16[208,128]{1,0:T(8,128)(2,1)S(1)}, u32[]{:S(2)}, u32[]{:S(2)}) collective-permute-start(bf16[208,128]{1,0:T(8,128)(2,1)S(1)} %get-tuple-element.33), channel_id=1, source_target_pairs={{0,8},{2,10},{4,12},{6,14},{8,0},{10,2},{12,4},{14,6},{1,9},{3,11}... | collective-permute-start | bytes 159752 | tf_op jit(solution)/shard_map/ppermute | solution.py:390
  120.4 3.3 %collective-permute-start.9 = (bf16[208,128]{1,0:T(8,128)(2,1)S(1)}, bf16[208,128]{1,0:T(8,128)(2,1)S(1)}, u32[]{:S(2)}, u32[]{:S(2)}) collective-permute-start(bf16[208,128]{1,0:T(8,128)(2,1)S(1)} %get-tuple-element.34), channel_id=1, source_target_pairs={{0,12},{2,14},{4,0},{6,2},{8,4},{10,6},{12,8},{14,10},{1,13},{3,15... | collective-permute-start | bytes 159752 | tf_op jit(solution)/shard_map/ppermute | solution.py:390
  123.7 0.9 collective-permute-done.7.refs_1_
  124.6 0.4 collective-permute-done.8.refs_2_
  125.1 3.4 %collective-permute-done.9.refs_3_ = bf16[208,128]{1,0:T(8,128)(2,1)S(1)} collective-permute-done((bf16[208,128]{1,0:T(8,128)(2,1)S(1)}, bf16[208,128]{1,0:T(8,128)(2,1)S(1)}, u32[]{:S(2)}, u32[]{:S(2)}) %collective-permute-start.9) | collective-permute-done | bytes 53280 | tf_op jit(solution)/shard_map/ppermute | solution.py:390
  128.5 0.7 shard_map.121
  129.1 0.0 collective-permute-done.11.got0_ref
  129.1 1.2 copy-done
  130.4 1.2 copy-done.1
  131.6 5.9 %shard_map.124 = (bf16[448,2048]{1,0:T(8,128)(2,1)}, bf16[448,2048]{1,0:T(8,128)(2,1)}) custom-call(s32[1]{0:T(128)} %bitcast.6.par_ref, bf16[2,384,1024]{2,1,0:T(8,128)(2,1)} %get-tuple-element.37.sides_ref, bf16[2,2,384,448]{3,2,1,0:T(8,128)(2,1)} %get-tuple-element.25.grads_ref, bf16[448,2048]{1,0:T(8,128)(2,1)} %copy-done, bf16[448,2048]{1,0:T(8,128)(2,1)} %copy-done.1), custom_call_target="tpu_custom_call" | custom-call | flops 1409286144 | bytes 6619140 | tf_op jit(solution)/shard_map/pallas_call | solution.py:41
  (5 shorter events, 0.0 us)
Async XLA Ops:
  4.1 42.0 %collective-permute-start.2 = (bf16[2,2,448,1024]{3,2,1,0:T(8,128)(2,1)}, bf16[2,2,448,1024]{3,2,1,0:T(8,128)(2,1)}, u32[]{:S(2)}, u32[]{:S(2)}) collective-permute-start(bf16[2,2,448,1024]{3,2,1,0:T(8,128)(2,1)} %shard_map.113.own_ref), channel_id=1, source_target_pairs={{0,1},{1,0},{2,3},{3,2},{4,5},{5,4},{6,7},{7,6},{8,9},{9,8},{10,11... | collective-permute-start | bytes 11010056 | tf_op jit(solution)/shard_map/ppermute | solution.py:387
  9.7 18.9 %all-to-all-start.1 = ((bf16[16,24,1024]{2,1,0:T(8,128)(2,1)}), bf16[16,24,1024]{2,1,0:T(8,128)(2,1)S(1)}, u32[]{:S(2)}, u32[]{:S(2)}) async-start(bf16[16,24,1024]{2,1,0:T(8,128)(2,1)} %bitcast.35), calls=%async_computation.1 | async-start | bytes 1572864 | tf_op jit(solution)/shard_map/all_to_all | solution.py:393
  28.6 25.0 %all-to-all-start = ((bf16[16,24,2048]{2,1,0:T(8,128)(2,1)}), bf16[16,24,2048]{2,1,0:T(8,128)(2,1)S(1)}, u32[]{:S(2)}, u32[]{:S(2)}) async-start(bf16[16,24,2048]{2,1,0:T(8,128)(2,1)} %bitcast.33), calls=%async_computation | async-start | bytes 3145728 | tf_op jit(solution)/shard_map/all_to_all | solution.py:393
  32.4 13.7 %collective-permute-start = (bf16[192,1024]{1,0:T(8,128)(2,1)S(1)}, bf16[192,1024]{1,0:T(8,128)(2,1)S(1)}, u32[]{:S(2)}, u32[]{:S(2)}) collective-permute-start(bf16[192,1024]{1,0:T(8,128)(2,1)S(1)} %bitcast.41), channel_id=1, source_target_pairs={{0,2},{2,4},{4,6},{6,8},{8,10},{10,12},{12,14},{14,0},{1,3},{3,5},... | collective-permute-start | bytes 1179656 | tf_op jit(solution)/shard_map/ppermute | solution.py:390
  34.1 12.0 %collective-permute-start.1 = (bf16[192,1024]{1,0:T(8,128)(2,1)S(1)}, bf16[192,1024]{1,0:T(8,128)(2,1)S(1)}, u32[]{:S(2)}, u32[]{:S(2)}) collective-permute-start(bf16[192,1024]{1,0:T(8,128)(2,1)S(1)} %bitcast.40), channel_id=1, source_target_pairs={{0,14},{2,0},{4,2},{6,4},{8,6},{10,8},{12,10},{14,12},{1,15},{3,1}... | collective-permute-start | bytes 1179656 | tf_op jit(solution)/shard_map/ppermute | solution.py:390
  38.1 24.4 %collective-permute-start.3 = (bf16[448,2048]{1,0:T(8,128)(2,1)}, bf16[448,2048]{1,0:T(8,128)(2,1)}, u32[]{:S(2)}, u32[]{:S(2)}) collective-permute-start(bf16[448,2048]{1,0:T(8,128)(2,1)} %bitcast.36), channel_id=1, source_target_pairs={{0,1},{1,0},{2,3},{3,2},{4,5},{5,4},{6,7},{7,6},{8,9},{9,8},{10,11... | collective-permute-start | bytes 5505032 | tf_op jit(solution)/shard_map/ppermute | solution.py:387
  57.0 11.5 %collective-permute-start.10 = (bf16[448,2048]{1,0:T(8,128)(2,1)}, bf16[448,2048]{1,0:T(8,128)(2,1)S(1)}, u32[]{:S(2)}, u32[]{:S(2)}) collective-permute-start(bf16[448,2048]{1,0:T(8,128)(2,1)} %shard_map.122), channel_id=1, source_target_pairs={{0,1},{1,0},{2,3},{3,2},{4,5},{5,4},{6,7},{7,6},{8,9},{9,8},{10,11... | collective-permute-start | bytes 5505032 | tf_op jit(solution)/shard_map/ppermute | solution.py:387
  68.5 1.2 copy-start.2
  76.2 52.9 %collective-permute-start.11 = (bf16[448,2048]{1,0:T(8,128)(2,1)}, bf16[448,2048]{1,0:T(8,128)(2,1)S(1)}, u32[]{:S(2)}, u32[]{:S(2)}) collective-permute-start(bf16[448,2048]{1,0:T(8,128)(2,1)} %get-tuple-element.38), channel_id=1, source_target_pairs={{0,1},{1,0},{2,3},{3,2},{4,5},{5,4},{6,7},{7,6},{8,9},{9,8},{10,11... | collective-permute-start | bytes 5505032 | tf_op jit(solution)/shard_map/ppermute | solution.py:387
  76.4 52.8 %collective-permute-start.12 = (bf16[448,2048]{1,0:T(8,128)(2,1)}, bf16[448,2048]{1,0:T(8,128)(2,1)S(1)}, u32[]{:S(2)}, u32[]{:S(2)}) collective-permute-start(bf16[448,2048]{1,0:T(8,128)(2,1)} %get-tuple-element.39), channel_id=1, source_target_pairs={{0,1},{1,0},{2,3},{3,2},{4,5},{5,4},{6,7},{7,6},{8,9},{9,8},{10,11... | collective-permute-start | bytes 5505032 | tf_op jit(solution)/shard_map/ppermute | solution.py:387
  76.8 15.1 %collective-permute-start.4 = (bf16[192,1152]{1,0:T(8,128)(2,1)S(1)}, bf16[192,1152]{1,0:T(8,128)(2,1)S(1)}, u32[]{:S(2)}, u32[]{:S(2)}) collective-permute-start(bf16[192,1152]{1,0:T(8,128)(2,1)S(1)} %get-tuple-element.27), channel_id=1, source_target_pairs={{0,14},{2,0},{4,2},{6,4},{8,6},{10,8},{12,10},{14,12},{1,15},{3,1}... | collective-permute-start | bytes 1327112 | tf_op jit(solution)/shard_map/ppermute | solution.py:390
  82.5 12.6 %collective-permute-start.5 = (bf16[192,1152]{1,0:T(8,128)(2,1)S(1)}, bf16[192,1152]{1,0:T(8,128)(2,1)S(1)}, u32[]{:S(2)}, u32[]{:S(2)}) collective-permute-start(bf16[192,1152]{1,0:T(8,128)(2,1)S(1)} %get-tuple-element.28), channel_id=1, source_target_pairs={{0,2},{2,4},{4,6},{6,8},{8,10},{10,12},{12,14},{14,0},{1,3},{3,5},... | collective-permute-start | bytes 1327112 | tf_op jit(solution)/shard_map/ppermute | solution.py:390
  114.4 3.2 %collective-permute-start.6 = (bf16[4,208,128]{2,1,0:T(8,128)(2,1)S(1)}, bf16[4,208,128]{2,1,0:T(8,128)(2,1)S(1)}, u32[]{:S(2)}, u32[]{:S(2)}) collective-permute-start(bf16[4,208,128]{2,1,0:T(8,128)(2,1)S(1)} %get-tuple-element.30), channel_id=1, source_target_pairs={{0,1},{1,0},{2,3},{3,2},{4,5},{5,4},{6,7},{7,6},{8,9},{9,8},{10,11... | collective-permute-start | bytes 638984 | tf_op jit(solution)/shard_map/ppermute | solution.py:387
  117.7 6.9 %collective-permute-start.7 = (bf16[208,128]{1,0:T(8,128)(2,1)S(1)}, bf16[208,128]{1,0:T(8,128)(2,1)S(1)}, u32[]{:S(2)}, u32[]{:S(2)}) collective-permute-start(bf16[208,128]{1,0:T(8,128)(2,1)S(1)} %get-tuple-element.32), channel_id=1, source_target_pairs={{0,4},{2,6},{4,8},{6,10},{8,12},{10,14},{12,0},{14,2},{1,5},{3,7},... | collective-permute-start | bytes 159752 | tf_op jit(solution)/shard_map/ppermute | solution.py:390
  117.8 7.3 %collective-permute-start.8 = (bf16[208,128]{1,0:T(8,128)(2,1)S(1)}, bf16[208,128]{1,0:T(8,128)(2,1)S(1)}, u32[]{:S(2)}, u32[]{:S(2)}) collective-permute-start(bf16[208,128]{1,0:T(8,128)(2,1)S(1)} %get-tuple-element.33), channel_id=1, source_target_pairs={{0,8},{2,10},{4,12},{6,14},{8,0},{10,2},{12,4},{14,6},{1,9},{3,11}... | collective-permute-start | bytes 159752 | tf_op jit(solution)/shard_map/ppermute | solution.py:390
  120.4 8.0 %collective-permute-start.9 = (bf16[208,128]{1,0:T(8,128)(2,1)S(1)}, bf16[208,128]{1,0:T(8,128)(2,1)S(1)}, u32[]{:S(2)}, u32[]{:S(2)}) collective-permute-start(bf16[208,128]{1,0:T(8,128)(2,1)S(1)} %get-tuple-element.34), channel_id=1, source_target_pairs={{0,12},{2,14},{4,0},{6,2},{8,4},{10,6},{12,8},{14,10},{1,13},{3,15... | collective-permute-start | bytes 159752 | tf_op jit(solution)/shard_map/ppermute | solution.py:390
  129.1 1.3 copy-start
  130.4 1.2 copy-start.1

commit v9 on v7

--- a/solution.py
+++ b/solution.py
@@ -143,7 +143,7 @@
         copy.wait()
 
 
-def forward(mine_ref, low_ref, high_ref, own_ref, other_ref, out_ref, rows_ref, buf, sem, both, keep_sem, made, out_sem):
+def forward(mine_ref, low_ref, high_ref, own_ref, other_ref, out_ref, rows_ref, hid_ref, buf, sem, both, keep_sem, made, out_sem):
     jobs = [(w.at[n, k], buf.at[2 * p + n, k]) for p, w in enumerate((own_ref, other_ref)) for n in range(2) for k in range(2)]
     copies = [pltpu.make_async_copy(a, b, sem.at[i]) for i, (a, b) in enumerate(jobs)]
     for copy in copies:
@@ -174,6 +174,8 @@
         made[p, 2] = act.astype(BF16)
         done.append(pltpu.make_async_copy(made.at[p], out_ref.at[p], out_sem.at[p]))
         done[-1].start()
+    done.append(pltpu.make_async_copy(made.at[1, 0], hid_ref, out_sem.at[2]))
+    done[-1].start()
     for copy in keep + done:
         copy.wait()
 
@@ -199,7 +201,7 @@
     ]
 
 
-def backward(cot_ref, mid_ref, down0_ref, down1_ref, own_ref, other_ref, low_ref, high_ref, grads_ref, gate_ref, mid, mid_sem, wd, wd_sem, buf, sem, grads, out_sem):
+def backward(cot_ref, mid_ref, down0_ref, down1_ref, own_ref, other_ref, low_ref, high_ref, grads_ref, theirs_ref, gate_ref, mid, mid_sem, wd, wd_sem, buf, sem, grads, out_sem, wide_grads):
     rows, width = cot_ref.shape
     mids = [pltpu.make_async_copy(mid_ref.at[p], mid.at[p], mid_sem.at[p]) for p in range(2)]
     second = pltpu.make_async_copy(down1_ref, wd, wd_sem)
@@ -216,8 +218,15 @@
         gate = gate + jnp.sum(mid[p, 0].astype(F32) * back, axis=1, keepdims=True)
         grads[p, 0] = (back * mid[p, 1].astype(F32)).astype(BF16)
         grads[p, 1] = (back * mid[p, 2].astype(F32)).astype(BF16)
-        done.append(pltpu.make_async_copy(grads.at[p], grads_ref.at[p], out_sem.at[p]))
-        done[-1].start()
+        for n in range(2):
+            if p == 0:
+                source, to = grads.at[0, n], grads_ref.at[n]
+            else:
+                wide_grads[n] = jnp.zeros(wide_grads.shape[1:], BF16)
+                wide_grads[n, :, : grads.shape[3]] = grads[1, n]
+                source, to = wide_grads.at[n], theirs_ref.at[n * rows : (n + 1) * rows]
+            done.append(pltpu.make_async_copy(source, to, out_sem.at[2 * p + n]))
+            done[-1].start()
     wide = jnp.broadcast_to(gate, (rows, LANES))
     gate_ref[...] = wide
     low_ref[:, width // 2 :] = wide[: rows // 2].astype(BF16)
@@ -231,8 +240,13 @@
         copy.wait()
 
 
-def own_half(grads_ref, gate_ref, own_ref, other_ref, out_ref, grads, grad_sem, buf, sem):
-    copies = [pltpu.make_async_copy(grads_ref.at[p], grads.at[p], grad_sem.at[p]) for p in range(2)]
+def own_half(grads_ref, theirs_ref, gate_ref, own_ref, other_ref, out_ref, grads, grad_sem, buf, sem, wide):
+    rows = gate_ref.shape[0]
+    copies = [pltpu.make_async_copy(grads_ref, grads.at[0], grad_sem.at[2])]
+    copies += [
+        pltpu.make_async_copy(theirs_ref.at[n * rows : (n + 1) * rows], wide.at[n], grad_sem.at[n])
+        for n in range(2)
+    ]
     copies += fetch_half(0, own_ref, other_ref, buf, sem)
     for copy in copies:
         copy.start()
@@ -240,6 +254,8 @@
     out_ref[:, part:] = gate_ref[...]
     for copy in copies:
         copy.wait()
+    for n in range(2):
+        grads[1, n] = wide[n, :, : grads.shape[3]]
     out_ref[:, :part] = input_grad(grads, buf)
 
 
@@ -255,47 +271,58 @@
         copy.wait()
 
 
-def row_grads(p, par_ref, sides_ref, grads_ref, *refs):
-    inputs = refs[:2] if p == 0 else ()
-    outs, scratch = refs[len(inputs) : len(inputs) + 2], refs[len(inputs) + 2 :]
-    sides, side_sem, left, left_sem, made, out_sem, *got = scratch
-    keep = [pltpu.make_async_copy(sides_ref.at[k], sides.at[k], side_sem.at[k]) for k in range(2)]
-    copies = [pltpu.make_async_copy(grads_ref.at[p, n], left.at[n], left_sem.at[n]) for n in range(2)]
-    received = [pltpu.make_async_copy(r, got[0].at[n], got[1].at[n]) for n, r in enumerate(inputs)]
-    for copy in (copies[0], *keep, copies[1], *received):
-        copy.start()
+def start_all(copies):
+    for copy in copies:
+        copy.start()
+    return copies
+
+
+def row_grads(par_ref, *refs):
+    inputs, outs, (sides, side_sem, left, left_sem, made, out_sem, wide) = refs[:4], refs[4:6], refs[6:]
+    rows, ff = left.shape[1:]
+    sources = [
+        [inputs[2].at[n] for n in range(2)],
+        [inputs[3].at[n * rows : (n + 1) * rows] for n in range(2)],
+    ]
+    lefts = [
+        [pltpu.make_async_copy(sources[q][n], (left, wide)[q].at[n], left_sem.at[2 * q + n]) for n in range(2)]
+        for q in range(2)
+    ]
+    rights = [
+        [pltpu.make_async_copy(inputs[q].at[k], sides.at[q, k], side_sem.at[2 * q + k]) for k in range(2)]
+        for q in range(2)
+    ]
+    for q in range(2):
+        start_all([lefts[q][0], *rights[q], lefts[q][1]])
     done = []
     for n in range(2):
-        copies[n].wait()
-        if p == 0:
-            received[n].wait()
         for k, side in enumerate((par_ref[0], 1 - par_ref[0])):
-            if n == 0:
-                keep[k].wait()
-            grad = dot(left[n], sides[k], TN)
+            total = 0.0
+            for q in range(2):
+                if k == 0:
+                    lefts[q][n].wait()
+                if n == 0:
+                    rights[q][k].wait()
+                side_left = left[n] if q == 0 else wide[n, :, :ff]
+                total = total + dot(side_left, sides[q, k], TN)
             for to, cols in side_columns(side, made.shape[2]):
-                piece = grad[:, to]
-                if p == 0:
-                    piece = piece + got[0][n, :, cols].astype(F32)
-                made[n, :, cols] = piece.astype(BF16)
-        done.append(pltpu.make_async_copy(made.at[n], outs[n], out_sem.at[n]))
-        done[-1].start()
+                made[n, :, cols] = total[:, to].astype(BF16)
+        done += start_all([pltpu.make_async_copy(made.at[n], outs[n], out_sem.at[n])])
     for copy in done:
         copy.wait()
 
 
-def down_grads(p, cot_ref, mid_ref, *refs):
-    inputs, (out_ref, left, sem, made, out_sem, *got) = (refs[:1], refs[1:]) if p == 0 else ((), refs)
-    copies = [pltpu.make_async_copy(mid_ref.at[p, 0], left, sem)]
-    copies += [pltpu.make_async_copy(r, got[0], got[1]) for r in inputs]
-    for copy in copies:
-        copy.start()
-    for copy in copies:
-        copy.wait()
-    grad = dot(left[...], cot_ref[...], TN)
-    if p == 0:
-        grad += got[0][...].astype(F32)
-    made[...] = grad.astype(BF16)
+def down_grads(cot_ref, mid_ref, cot1_ref, hid1_ref, out_ref, left, left_sem, cot1, cot_sem, made, out_sem):
+    copies = start_all([
+        pltpu.make_async_copy(mid_ref.at[0, 0], left.at[0], left_sem.at[0]),
+        pltpu.make_async_copy(cot1_ref, cot1, cot_sem),
+        pltpu.make_async_copy(hid1_ref, left.at[1], left_sem.at[1]),
+    ])
+    copies[0].wait()
+    total = dot(left[0], cot_ref[...], TN)
+    copies[1].wait()
+    copies[2].wait()
+    made[...] = (total + dot(left[1], cot1[...], TN)).astype(BF16)
     done = pltpu.make_async_copy(made, out_ref, out_sem)
     done.start()
     done.wait()
@@ -406,12 +433,13 @@
     packed = [(own, "h"), (other, "h")]
     mids = pltpu.VMEM((2, 3, count, ff), BF16)
     halves = [pltpu.VMEM((4, ff, part), BF16), dma(4)]
-    mid, sides = call(
-        forward, [((2, 3, count, ff), BF16, "h"), ((2, count, part), BF16, "h")],
+    mid, sides, hid = call(
+        forward,
+        [((2, 3, count, ff), BF16, "h"), ((2, count, part), BF16, "h"), ((count, ff), BF16, "h")],
         (mine, "v"), (low, "v"), (high, "v"), *packed,
         scratch=[
             pltpu.VMEM((4, 2, ff, part), BF16), dma(8), pltpu.VMEM((count, part), BF16),
-            dma(2), mids, dma(2),
+            dma(2), mids, dma(3),
         ],
         flops=8 * count * width * ff, mib=18,
     )
@@ -419,22 +447,26 @@
         hold, [((ff, width), BF16, "v")], (down, "h"),
         scratch=[pltpu.SemaphoreType.DMA], mib=4,
     )
+    padded = (ff + LANES - 1) // LANES * LANES
     message = ((count // 2, part + LANES), BF16, "v")
-    to_low, to_high, grads, gate = call(
+    to_low, to_high, grads, theirs, gate = call(
         backward,
-        [message, message, ((2, 2, count, ff), BF16, "h"), ((count, LANES), F32, "v")],
+        [
+            message, message, ((2, count, ff), BF16, "h"), ((2 * count, padded), BF16, "h"),
+            ((count, LANES), F32, "v"),
+        ],
         (cot, "v"), (mid, "h"), (held, "v"), (down_other, "h"), *packed,
         scratch=[
             mids, dma(2), pltpu.VMEM((ff, width), BF16), pltpu.SemaphoreType.DMA, *halves,
-            pltpu.VMEM((2, 2, count, ff), BF16), dma(2),
+            pltpu.VMEM((2, 2, count, ff), BF16), dma(4), pltpu.VMEM((2, count, padded), BF16),
         ],
         flops=8 * count * width * ff, mib=20,
     )
     from_low, from_high = shift(to_low, -1), shift(to_high, 1)
     (kept,) = call(
         own_half, [((count, part + LANES), F32, "v")],
-        (grads, "h"), (gate, "v"), *packed,
-        scratch=[pltpu.VMEM((2, 2, count, ff), BF16), dma(2), *halves],
+        (grads, "h"), (theirs, "h"), (gate, "v"), *packed,
+        scratch=[pltpu.VMEM((2, 2, count, ff), BF16), dma(3), *halves, pltpu.VMEM((2, count, padded), BF16)],
         flops=4 * count * width * ff, mib=14,
     )
     (pair,) = call(
@@ -445,30 +477,24 @@
 
     one = pltpu.SemaphoreType.DMA
     shard = ((ff, width), BF16, "h")
-    pair_room = pltpu.VMEM((2, ff, width), BF16)
-    row_args = [(parity, "s"), (sides, "h"), (grads, "h")]
-    row_room = [
-        pltpu.VMEM((2, count, part), BF16), dma(2), pltpu.VMEM((2, count, ff), BF16), dma(2), pair_room, dma(2),
-    ]
-    down_args = [(cot, "v"), (mid, "h")]
-    down_room = [pltpu.VMEM((count, ff), BF16), one, pltpu.VMEM((ff, width), BF16), one]
-    cost = 2 * count * width * ff
-    (their_down,) = call(
-        functools.partial(down_grads, 1), [shard], *down_args,
-        scratch=down_room, flops=cost, mib=10,
-    )
-    theirs = call(
-        functools.partial(row_grads, 1), [shard] * 2, *row_args,
-        scratch=row_room, flops=2 * cost, mib=14,
-    )
+    cost = 4 * count * width * ff
     (grad_down,) = call(
-        functools.partial(down_grads, 0), [shard], *down_args, (swap(their_down), "h"),
-        scratch=[*down_room, down_room[2], one], flops=cost, mib=12,
-    )
-    received = [(swap(g), "h") for g in theirs]
+        down_grads, [shard],
+        (cot, "v"), (mid, "h"), (swap(cot), "h"), (swap(hid), "h"),
+        scratch=[
+            pltpu.VMEM((2, count, ff), BF16), dma(2), pltpu.VMEM((count, width), BF16), one,
+            pltpu.VMEM((ff, width), BF16), one,
+        ],
+        flops=cost, mib=12,
+    )
     grad_gate, grad_up = call(
-        functools.partial(row_grads, 0), [shard] * 2, *row_args, *received,
-        scratch=[*row_room, pair_room, dma(2)], flops=2 * cost, mib=18,
+        row_grads, [shard] * 2,
+        (parity, "s"), (sides, "h"), (swap(sides), "h"), (grads, "h"), (swap(theirs), "h"),
+        scratch=[
+            pltpu.VMEM((2, 2, count, part), BF16), dma(4), pltpu.VMEM((2, count, ff), BF16), dma(4),
+            pltpu.VMEM((2, ff, width), BF16), dma(2), pltpu.VMEM((2, count, padded), BF16),
+        ],
+        flops=2 * cost, mib=18,
     )
 
     block = (depth // 2, rows + 16, LANES)

time: 140 us -> 135 us (0.964)
  blocking collectives: 17.9 us -> 0 us
  waiting for transfers between devices: 33.8 us -> 44.9 us
  starting transfers between devices: 33.1 us -> 40.8 us
  Pallas kernels: 49.5 us -> 45.2 us
  local copies, waits for them, and re-layouts: 3.76 us -> 2.06 us
    all_to_all x2 -> x3, waiting for transfers between devices: 9.84 us -> 35.8 us  [exchange(): return lax.all_to_all(v, EP, split_axis=0, concat_axis=0, tiled=True)]
    all_to_all x1 -> x0, blocking collectives: 17.9 us -> none  [exchange(): return lax.all_to_all(v, EP, split_axis=0, concat_axis=0, tiled=True)]
    ppermute x7, waiting for transfers between devices: 22.8 us -> 8.03 us  [shift(): return lax.ppermute(v, Z, [(i, (i + k) % depth) for i in range(depth)])]
    pallas_call x16 -> x14, Pallas kernels: 49.5 us -> 45.2 us  [call(): kernel_call(*(a if m == 's' else pltpu.with_memory_space_constraint(a, pl...]
    all_to_all x2 -> x3, starting transfers between devices: 8.77 us -> 12.4 us  [exchange(): return lax.all_to_all(v, EP, split_axis=0, concat_axis=0, tiled=True)]
    ppermute x7, starting transfers between devices: 13.9 us -> 16.8 us  [shift(): return lax.ppermute(v, Z, [(i, (i + k) % depth) for i in range(depth)])]
    unnamed x10 -> x6, local copies, waits for them, and re-layouts: 3.7 us -> 1.14 us
    ppermute x6 -> x7, starting transfers between devices: 10.4 us -> 11.6 us  [swap(): return lax.ppermute(v, 'c', [(0, 1), (1, 0)])]
  transfers between devices with their start and end apart: 15 -> 17, of which waited for: 9 -> 6; matrix products, arithmetic and copies ran while one was open for 0% -> 1% of each run, Pallas kernels for 29% -> 25%
where the time goes in v9:
time: 135 us; the launch traced here: 134 us
  Pallas kernels  45.2 us (33%)
  waiting for transfers between devices  44.9 us (33%)
  starting transfers between devices  40.8 us (30%)
  local copies, waits for them, and re-layouts  2.06 us (2%)
    pallas_call x14, Pallas kernels, call(): kernel_call(*(a if m == 's' else pltpu.with_memory_space_constraint(a, pl...  45.2 us
    all_to_all x3, waiting for transfers between devices, exchange(): return lax.all_to_all(v, EP, split_axis=0, concat_axis=0, tiled=True)  35.8 us
    ppermute x7, starting transfers between devices, shift(): return lax.ppermute(v, Z, [(i, (i + k) % depth) for i in range(depth)])  16.8 us
    all_to_all x3, starting transfers between devices, exchange(): return lax.all_to_all(v, EP, split_axis=0, concat_axis=0, tiled=True)  12.4 us
    ppermute x7, starting transfers between devices, swap(): return lax.ppermute(v, 'c', [(0, 1), (1, 0)])  11.6 us
    ppermute x7, waiting for transfers between devices, shift(): return lax.ppermute(v, Z, [(i, (i + k) % depth) for i in range(depth)])  8.03 us
  transfers between devices with their start and end apart: 17, of which 6 were waited for; matrix products, arithmetic and copies ran while one was open for 1% of the time, Pallas kernels for 25%

profile of v9, /device:TPU:1, one launch (start us, length us, event | category | flops | bytes accessed | tf_op | source)
XLA Modules:
  0.0 134.0 jit_solution(16477928657788951513)
XLA Ops:
  0.6 3.5 %shard_map.113.own_ref = bf16[2,2,448,1024]{3,2,1,0:T(8,128)(2,1)} custom-call(s32[1]{0:T(128)} %bitcast.6.par_ref, bf16[448,2048]{1,0:T(8,128)(2,1)} %bitcast.38, bf16[448,2048]{1,0:T(8,128)(2,1)} %bitcast.39), custom_call_target="tpu_custom_call" | custom-call | bytes 3670020 | tf_op jit(solution)/shard_map/pallas_call | solution.py:41
  4.1 3.3 %collective-permute-start.2 = (bf16[2,2,448,1024]{3,2,1,0:T(8,128)(2,1)}, bf16[2,2,448,1024]{3,2,1,0:T(8,128)(2,1)}, u32[]{:S(2)}, u32[]{:S(2)}) collective-permute-start(bf16[2,2,448,1024]{3,2,1,0:T(8,128)(2,1)} %shard_map.113.own_ref), channel_id=1, source_target_pairs={{0,1},{1,0},{2,3},{3,2},{4,5},{5,4},{6,7},{7,6},{8,9},{9,8},{10,11... | collective-permute-start | bytes 11010056 | tf_op jit(solution)/shard_map/ppermute | solution.py:386
  7.4 2.3 %shard_map.112 = bf16[384,1024]{1,0:T(8,128)(2,1)} custom-call(s32[1]{0:T(128)} %bitcast.core_ref, s32[1]{0:T(128)} %bitcast.6.par_ref, s32[2,192]{1,0:T(2,128)} %bitcast.41, bf16[192,2048]{1,0:T(8,128)(2,1)} %tok_ref.1), custom_call_target="tpu_custom_call" | custom-call | flops 150994944 | bytes 787976 | tf_op jit(solution)/shard_map/pallas_call | solution.py:41
  9.7 5.1 %all-to-all-start.1 = ((bf16[16,24,1024]{2,1,0:T(8,128)(2,1)}), bf16[16,24,1024]{2,1,0:T(8,128)(2,1)S(1)}, u32[]{:S(2)}, u32[]{:S(2)}) async-start(bf16[16,24,1024]{2,1,0:T(8,128)(2,1)} %bitcast.35), calls=%async_computation.1 | async-start | bytes 1572864 | tf_op jit(solution)/shard_map/all_to_all | solution.py:392
  14.8 0.4 collective-permute-start.3
  15.2 0.9 shard_map.110.table_ref
  16.0 2.8 %shard_map.111 = bf16[384,2048]{1,0:T(8,128)(2,1)} custom-call(f32[8,192]{1,0:T(8,128)S(1)} %shard_map.110.table_ref, bf16[192,2048]{1,0:T(8,128)(2,1)} %cot_ref.1), custom_call_target="tpu_custom_call" | custom-call | flops 301989888 | bytes 792576 | tf_op jit(solution)/shard_map/pallas_call | solution.py:41
  18.9 9.7 %all-to-all-done.1 = bf16[16,24,1024]{2,1,0:T(8,128)(2,1)S(1)} async-done(((bf16[16,24,1024]{2,1,0:T(8,128)(2,1)}), bf16[16,24,1024]{2,1,0:T(8,128)(2,1)S(1)}, u32[]{:S(2)}, u32[]{:S(2)}) %all-to-all-start.1) | async-done | bytes 786464 | tf_op jit(solution)/shard_map/all_to_all | solution.py:392
  28.6 3.7 %all-to-all-start = ((bf16[16,24,2048]{2,1,0:T(8,128)(2,1)}), bf16[16,24,2048]{2,1,0:T(8,128)(2,1)S(1)}, u32[]{:S(2)}, u32[]{:S(2)}) async-start(bf16[16,24,2048]{2,1,0:T(8,128)(2,1)} %bitcast.33), calls=%async_computation | async-start | bytes 3145728 | tf_op jit(solution)/shard_map/all_to_all | solution.py:392
  32.3 0.9 fusion
  33.3 1.7 %collective-permute-start = (bf16[192,1024]{1,0:T(8,128)(2,1)}, bf16[192,1024]{1,0:T(8,128)(2,1)}, u32[]{:S(2)}, u32[]{:S(2)}) collective-permute-start(bf16[192,1024]{1,0:T(8,128)(2,1)} %bitcast.9), channel_id=1, source_target_pairs={{0,2},{2,4},{4,6},{6,8},{8,10},{10,12},{12,14},{14,0},{1,3},{3,5},... | collective-permute-start | bytes 1179656 | tf_op jit(solution)/shard_map/ppermute | solution.py:389
  34.9 3.9 %collective-permute-start.1 = (bf16[192,1024]{1,0:T(8,128)(2,1)}, bf16[192,1024]{1,0:T(8,128)(2,1)}, u32[]{:S(2)}, u32[]{:S(2)}) collective-permute-start(bf16[192,1024]{1,0:T(8,128)(2,1)} %bitcast.10), channel_id=1, source_target_pairs={{0,14},{2,0},{4,2},{6,4},{8,6},{10,8},{12,10},{14,12},{1,15},{3,1}... | collective-permute-start | bytes 1179656 | tf_op jit(solution)/shard_map/ppermute | solution.py:389
  38.9 1.5 %shard_map.115.down0_ref = bf16[448,2048]{1,0:T(8,128)(2,1)S(1)} custom-call(bf16[448,2048]{1,0:T(8,128)(2,1)} %bitcast.37), custom_call_target="tpu_custom_call" | custom-call | bytes 1835008 | tf_op jit(solution)/shard_map/pallas_call | solution.py:41
  40.4 13.3 %all-to-all-done = bf16[16,24,2048]{2,1,0:T(8,128)(2,1)S(1)} async-done(((bf16[16,24,2048]{2,1,0:T(8,128)(2,1)}), bf16[16,24,2048]{2,1,0:T(8,128)(2,1)S(1)}, u32[]{:S(2)}, u32[]{:S(2)}) %all-to-all-start) | async-done | bytes 1572896 | tf_op jit(solution)/shard_map/all_to_all | solution.py:392
  53.7 3.7 %collective-permute-start.12 = (bf16[384,2048]{1,0:T(8,128)(2,1)S(1)}, bf16[384,2048]{1,0:T(8,128)(2,1)}, u32[]{:S(2)}, u32[]{:S(2)}) collective-permute-start(bf16[384,2048]{1,0:T(8,128)(2,1)S(1)} %bitcast.28), channel_id=1, source_target_pairs={{0,1},{1,0},{2,3},{3,2},{4,5},{5,4},{6,7},{7,6},{8,9},{9,8},{10,11... | collective-permute-start | bytes 4718600 | tf_op jit(solution)/shard_map/ppermute | solution.py:386
  57.4 0.0 collective-permute-done.low_ref
  57.4 0.0 collective-permute-done.1.high_ref
  57.4 0.0 collective-permute-done.2.other_ref
  57.4 0.0 copy-start.1
  57.4 1.1 copy-done.1
  58.5 8.7 %shard_map.114 = (bf16[2,3,384,448]{3,2,1,0:T(8,128)(2,1)}, bf16[2,384,1024]{2,1,0:T(8,128)(2,1)}, bf16[384,448]{1,0:T(8,128)(2,1)}) custom-call(bf16[384,1024]{1,0:T(8,128)(2,1)S(1)} %bitcast.32, bf16[192,1024]{1,0:T(8,128)(2,1)} %collective-permute-done.low_ref, bf16[192,1024]{1,0:T(8,128)(2,1)} %collective-permute-done.1.high_ref, ...), custom_call_target="tpu_custom_call" | custom-call | flops 2818572288 | bytes 8912896 | tf_op jit(solution)/shard_map/pallas_call | solution.py:41
  67.2 0.0 collective-permute-done.3.down1_ref
  67.2 6.1 %shard_map.116 = (bf16[192,1152]{1,0:T(8,128)(2,1)S(1)}, bf16[192,1152]{1,0:T(8,128)(2,1)S(1)}, bf16[2,384,448]{2,1,0:T(8,128)(2,1)}, bf16[768,512]{1,0:T(8,128)(2,1)}, f32[384,128]{1,0:T(8,128)S(1)}) custom-call(bf16[384,2048]{1,0:T(8,128)(2,1)S(1)} %bitcast.29, bf16[2,3,384,448]{3,2,1,0:T(8,128)(2,1)} %get-tuple-element.23.mid_ref, ...), custom_call_target="tpu_custom_call" | custom-call | flops 2818572288 | bytes 14647296 | tf_op jit(solution)/shard_map/pallas_call | solution.py:41
  73.3 5.9 %collective-permute-start.4 = (bf16[192,1152]{1,0:T(8,128)(2,1)S(1)}, bf16[192,1152]{1,0:T(8,128)(2,1)S(1)}, u32[]{:S(2)}, u32[]{:S(2)}) collective-permute-start(bf16[192,1152]{1,0:T(8,128)(2,1)S(1)} %get-tuple-element.27), channel_id=1, source_target_pairs={{0,14},{2,0},{4,2},{6,4},{8,6},{10,8},{12,10},{14,12},{1,15},{3,1}... | collective-permute-start | bytes 1327112 | tf_op jit(solution)/shard_map/ppermute | solution.py:389
  79.2 0.0 collective-permute-start.5
  79.2 0.3 collective-permute-start.10
  79.5 4.3 %shard_map.117.own_ref = f32[384,1152]{1,0:T(8,128)S(1)} custom-call(bf16[2,384,448]{2,1,0:T(8,128)(2,1)} %get-tuple-element.24.grads_ref.refs_2_, bf16[768,512]{1,0:T(8,128)(2,1)} %get-tuple-element.25.theirs_ref, f32[384,128]{1,0:T(8,128)S(1)} %get-tuple-element.26.gate_ref, bf16[2,2,448,1024]{3,2,1,0:T(8,128)(2,1)} %shard_map.113.own_ref, ...), custom_call_target="tpu_custom_call" | custom-call | flops 1409286144 | bytes 9011200 | tf_op jit(solution)/shard_map/pallas_call | solution.py:41
  83.8 0.0 copy-start.2
  83.8 4.9 %collective-permute-done.4.low_ref = bf16[192,1152]{1,0:T(8,128)(2,1)S(1)} collective-permute-done((bf16[192,1152]{1,0:T(8,128)(2,1)S(1)}, bf16[192,1152]{1,0:T(8,128)(2,1)S(1)}, u32[]{:S(2)}, u32[]{:S(2)}) %collective-permute-start.4) | collective-permute-done | bytes 442400 | tf_op jit(solution)/shard_map/ppermute | solution.py:389
  88.7 3.1 %collective-permute-done.5.high_ref = bf16[192,1152]{1,0:T(8,128)(2,1)S(1)} collective-permute-done((bf16[192,1152]{1,0:T(8,128)(2,1)S(1)}, bf16[192,1152]{1,0:T(8,128)(2,1)S(1)}, u32[]{:S(2)}, u32[]{:S(2)}) %collective-permute-start.5) | collective-permute-done | bytes 442400 | tf_op jit(solution)/shard_map/ppermute | solution.py:389
  91.8 1.0 shard_map.118
  92.8 3.6 %all-to-all-start.2 = ((bf16[16,24,1152]{2,1,0:T(8,128)(2,1)}), bf16[16,24,1152]{2,1,0:T(8,128)(2,1)S(1)}, u32[]{:S(2)}, u32[]{:S(2)}) async-start(bf16[16,24,1152]{2,1,0:T(8,128)(2,1)} %bitcast.34), calls=%async_computation.2 | async-start | bytes 1769472 | tf_op jit(solution)/shard_map/all_to_all | solution.py:392
  96.5 1.2 collective-permute-start.11
  97.7 0.1 collective-permute-start.13
  97.8 12.7 %all-to-all-done.2 = bf16[16,24,1152]{2,1,0:T(8,128)(2,1)S(1)} async-done(((bf16[16,24,1152]{2,1,0:T(8,128)(2,1)}), bf16[16,24,1152]{2,1,0:T(8,128)(2,1)S(1)}, u32[]{:S(2)}, u32[]{:S(2)}) %all-to-all-start.2) | async-done | bytes 884768 | tf_op jit(solution)/shard_map/all_to_all | solution.py:392
  110.6 0.4 shard_map.119
  111.0 2.6 %collective-permute-start.6 = (bf16[4,208,128]{2,1,0:T(8,128)(2,1)S(1)}, bf16[4,208,128]{2,1,0:T(8,128)(2,1)S(1)}, u32[]{:S(2)}, u32[]{:S(2)}) collective-permute-start(bf16[4,208,128]{2,1,0:T(8,128)(2,1)S(1)} %get-tuple-element.30), channel_id=1, source_target_pairs={{0,1},{1,0},{2,3},{3,2},{4,5},{5,4},{6,7},{7,6},{8,9},{9,8},{10,11... | collective-permute-start | bytes 638984 | tf_op jit(solution)/shard_map/ppermute | solution.py:386
  113.6 1.1 collective-permute-done.6.got_ref
  114.8 0.1 collective-permute-start.7
  114.9 0.0 collective-permute-done.12.cot1_ref
  114.9 2.0 %collective-permute-start.8 = (bf16[208,128]{1,0:T(8,128)(2,1)S(1)}, bf16[208,128]{1,0:T(8,128)(2,1)S(1)}, u32[]{:S(2)}, u32[]{:S(2)}) collective-permute-start(bf16[208,128]{1,0:T(8,128)(2,1)S(1)} %get-tuple-element.33), channel_id=1, source_target_pairs={{0,8},{2,10},{4,12},{6,14},{8,0},{10,2},{12,4},{14,6},{1,9},{3,11}... | collective-permute-start | bytes 159752 | tf_op jit(solution)/shard_map/ppermute | solution.py:389
  116.9 0.0 collective-permute-done.13.hid1_ref
  116.9 3.2 %collective-permute-start.9 = (bf16[208,128]{1,0:T(8,128)(2,1)S(1)}, bf16[208,128]{1,0:T(8,128)(2,1)S(1)}, u32[]{:S(2)}, u32[]{:S(2)}) collective-permute-start(bf16[208,128]{1,0:T(8,128)(2,1)S(1)} %get-tuple-element.34), channel_id=1, source_target_pairs={{0,12},{2,14},{4,0},{6,2},{8,4},{10,6},{12,8},{14,10},{1,13},{3,15... | collective-permute-start | bytes 159752 | tf_op jit(solution)/shard_map/ppermute | solution.py:389
  120.1 4.9 %shard_map.123 = bf16[448,2048]{1,0:T(8,128)(2,1)} custom-call(bf16[384,2048]{1,0:T(8,128)(2,1)S(1)} %bitcast.30, bf16[2,3,384,448]{3,2,1,0:T(8,128)(2,1)} %get-tuple-element.23.mid_ref, bf16[384,2048]{1,0:T(8,128)(2,1)} %collective-permute-done.12.cot1_ref, bf16[384,448]{1,0:T(8,128)(2,1)} %collective-permute-done.13.hid1_ref), custom_call_target="tpu_custom_call" | custom-call | flops 1409286144 | bytes 5554176 | tf_op jit(solution)/shard_map/pallas_call | solution.py:41
  125.1 0.0 collective-permute-done.8.refs_2_
  125.1 0.0 collective-permute-done.9.refs_3_
  125.1 0.7 shard_map.121
  125.8 8.1 %shard_map.122 = (bf16[448,2048]{1,0:T(8,128)(2,1)}, bf16[448,2048]{1,0:T(8,128)(2,1)}) custom-call(s32[1]{0:T(128)} %bitcast.6.par_ref, bf16[2,384,1024]{2,1,0:T(8,128)(2,1)} %get-tuple-element.37.refs_0_, bf16[2,384,1024]{2,1,0:T(8,128)(2,1)} %collective-permute-done.10.refs_1_, bf16[2,384,448]{2,1,0:T(8,128)(2,1)} %get-tuple-element.24.grads_ref.refs_2_, ...), custom_call_target="tpu_custom_call" | custom-call | flops 2818572288 | bytes 4620292 | tf_op jit(solution)/shard_map/pallas_call | solution.py:41
  (7 shorter events, 0.1 us)
Async XLA Ops:
  4.1 53.3 %collective-permute-start.2 = (bf16[2,2,448,1024]{3,2,1,0:T(8,128)(2,1)}, bf16[2,2,448,1024]{3,2,1,0:T(8,128)(2,1)}, u32[]{:S(2)}, u32[]{:S(2)}) collective-permute-start(bf16[2,2,448,1024]{3,2,1,0:T(8,128)(2,1)} %shard_map.113.own_ref), channel_id=1, source_target_pairs={{0,1},{1,0},{2,3},{3,2},{4,5},{5,4},{6,7},{7,6},{8,9},{9,8},{10,11... | collective-permute-start | bytes 11010056 | tf_op jit(solution)/shard_map/ppermute | solution.py:386
  9.7 18.9 %all-to-all-start.1 = ((bf16[16,24,1024]{2,1,0:T(8,128)(2,1)}), bf16[16,24,1024]{2,1,0:T(8,128)(2,1)S(1)}, u32[]{:S(2)}, u32[]{:S(2)}) async-start(bf16[16,24,1024]{2,1,0:T(8,128)(2,1)} %bitcast.35), calls=%async_computation.1 | async-start | bytes 1572864 | tf_op jit(solution)/shard_map/all_to_all | solution.py:392
  14.8 52.5 %collective-permute-start.3 = (bf16[448,2048]{1,0:T(8,128)(2,1)}, bf16[448,2048]{1,0:T(8,128)(2,1)}, u32[]{:S(2)}, u32[]{:S(2)}) collective-permute-start(bf16[448,2048]{1,0:T(8,128)(2,1)} %bitcast.36), channel_id=1, source_target_pairs={{0,1},{1,0},{2,3},{3,2},{4,5},{5,4},{6,7},{7,6},{8,9},{9,8},{10,11... | collective-permute-start | bytes 5505032 | tf_op jit(solution)/shard_map/ppermute | solution.py:386
  28.6 4.6 %copy-start = (bf16[16,24,1024]{2,1,0:T(8,128)(2,1)}, bf16[16,24,1024]{2,1,0:T(8,128)(2,1)S(1)}, u32[]{:S(2)}) copy-start(bf16[16,24,1024]{2,1,0:T(8,128)(2,1)S(1)} %all-to-all-done.1) | copy-start | bytes 2359300
  28.6 25.1 %all-to-all-start = ((bf16[16,24,2048]{2,1,0:T(8,128)(2,1)}), bf16[16,24,2048]{2,1,0:T(8,128)(2,1)S(1)}, u32[]{:S(2)}, u32[]{:S(2)}) async-start(bf16[16,24,2048]{2,1,0:T(8,128)(2,1)} %bitcast.33), calls=%async_computation | async-start | bytes 3145728 | tf_op jit(solution)/shard_map/all_to_all | solution.py:392
  33.3 24.1 %collective-permute-start = (bf16[192,1024]{1,0:T(8,128)(2,1)}, bf16[192,1024]{1,0:T(8,128)(2,1)}, u32[]{:S(2)}, u32[]{:S(2)}) collective-permute-start(bf16[192,1024]{1,0:T(8,128)(2,1)} %bitcast.9), channel_id=1, source_target_pairs={{0,2},{2,4},{4,6},{6,8},{8,10},{10,12},{12,14},{14,0},{1,3},{3,5},... | collective-permute-start | bytes 1179656 | tf_op jit(solution)/shard_map/ppermute | solution.py:389
  34.9 22.5 %collective-permute-start.1 = (bf16[192,1024]{1,0:T(8,128)(2,1)}, bf16[192,1024]{1,0:T(8,128)(2,1)}, u32[]{:S(2)}, u32[]{:S(2)}) collective-permute-start(bf16[192,1024]{1,0:T(8,128)(2,1)} %bitcast.10), channel_id=1, source_target_pairs={{0,14},{2,0},{4,2},{6,4},{8,6},{10,8},{12,10},{14,12},{1,15},{3,1}... | collective-permute-start | bytes 1179656 | tf_op jit(solution)/shard_map/ppermute | solution.py:389
  53.7 61.2 %collective-permute-start.12 = (bf16[384,2048]{1,0:T(8,128)(2,1)S(1)}, bf16[384,2048]{1,0:T(8,128)(2,1)}, u32[]{:S(2)}, u32[]{:S(2)}) collective-permute-start(bf16[384,2048]{1,0:T(8,128)(2,1)S(1)} %bitcast.28), channel_id=1, source_target_pairs={{0,1},{1,0},{2,3},{3,2},{4,5},{5,4},{6,7},{7,6},{8,9},{9,8},{10,11... | collective-permute-start | bytes 4718600 | tf_op jit(solution)/shard_map/ppermute | solution.py:386
  57.4 1.1 copy-start.1
  73.3 15.4 %collective-permute-start.4 = (bf16[192,1152]{1,0:T(8,128)(2,1)S(1)}, bf16[192,1152]{1,0:T(8,128)(2,1)S(1)}, u32[]{:S(2)}, u32[]{:S(2)}) collective-permute-start(bf16[192,1152]{1,0:T(8,128)(2,1)S(1)} %get-tuple-element.27), channel_id=1, source_target_pairs={{0,14},{2,0},{4,2},{6,4},{8,6},{10,8},{12,10},{14,12},{1,15},{3,1}... | collective-permute-start | bytes 1327112 | tf_op jit(solution)/shard_map/ppermute | solution.py:389
  79.2 12.7 %collective-permute-start.5 = (bf16[192,1152]{1,0:T(8,128)(2,1)S(1)}, bf16[192,1152]{1,0:T(8,128)(2,1)S(1)}, u32[]{:S(2)}, u32[]{:S(2)}) collective-permute-start(bf16[192,1152]{1,0:T(8,128)(2,1)S(1)} %get-tuple-element.28), channel_id=1, source_target_pairs={{0,2},{2,4},{4,6},{6,8},{8,10},{10,12},{12,14},{14,0},{1,3},{3,5},... | collective-permute-start | bytes 1327112 | tf_op jit(solution)/shard_map/ppermute | solution.py:389
  79.2 46.6 %collective-permute-start.10 = (bf16[2,384,1024]{2,1,0:T(8,128)(2,1)}, bf16[2,384,1024]{2,1,0:T(8,128)(2,1)}, u32[]{:S(2)}, u32[]{:S(2)}) collective-permute-start(bf16[2,384,1024]{2,1,0:T(8,128)(2,1)} %get-tuple-element.37.refs_0_), channel_id=1, source_target_pairs={{0,1},{1,0},{2,3},{3,2},{4,5},{5,4},{6,7},{7,6},{8,9},{9,8},{10,11... | collective-permute-start | bytes 4718600 | tf_op jit(solution)/shard_map/ppermute | solution.py:386
  83.8 12.7 %copy-start.2 = (bf16[768,512]{1,0:T(8,128)(2,1)S(1)}, bf16[768,512]{1,0:T(8,128)(2,1)}, u32[]{:S(2)}) copy-start(bf16[768,512]{1,0:T(8,128)(2,1)} %get-tuple-element.25.theirs_ref) | copy-start | bytes 2359300
  92.8 17.7 %all-to-all-start.2 = ((bf16[16,24,1152]{2,1,0:T(8,128)(2,1)}), bf16[16,24,1152]{2,1,0:T(8,128)(2,1)S(1)}, u32[]{:S(2)}, u32[]{:S(2)}) async-start(bf16[16,24,1152]{2,1,0:T(8,128)(2,1)} %bitcast.34), calls=%async_computation.2 | async-start | bytes 1769472 | tf_op jit(solution)/shard_map/all_to_all | solution.py:392
  96.5 29.3 %collective-permute-start.11 = (bf16[768,512]{1,0:T(8,128)(2,1)S(1)}, bf16[768,512]{1,0:T(8,128)(2,1)}, u32[]{:S(2)}, u32[]{:S(2)}) collective-permute-start(bf16[768,512]{1,0:T(8,128)(2,1)S(1)} %copy-done.2), channel_id=1, source_target_pairs={{0,1},{1,0},{2,3},{3,2},{4,5},{5,4},{6,7},{7,6},{8,9},{9,8},{10,11... | collective-permute-start | bytes 2359304 | tf_op jit(solution)/shard_map/ppermute | solution.py:386
  97.7 19.2 %collective-permute-start.13 = (bf16[384,448]{1,0:T(8,128)(2,1)}, bf16[384,448]{1,0:T(8,128)(2,1)}, u32[]{:S(2)}, u32[]{:S(2)}) collective-permute-start(bf16[384,448]{1,0:T(8,128)(2,1)} %get-tuple-element.40), channel_id=1, source_target_pairs={{0,1},{1,0},{2,3},{3,2},{4,5},{5,4},{6,7},{7,6},{8,9},{9,8},{10,11... | collective-permute-start | bytes 1032200 | tf_op jit(solution)/shard_map/ppermute | solution.py:386
  111.0 3.7 %collective-permute-start.6 = (bf16[4,208,128]{2,1,0:T(8,128)(2,1)S(1)}, bf16[4,208,128]{2,1,0:T(8,128)(2,1)S(1)}, u32[]{:S(2)}, u32[]{:S(2)}) collective-permute-start(bf16[4,208,128]{2,1,0:T(8,128)(2,1)S(1)} %get-tuple-element.30), channel_id=1, source_target_pairs={{0,1},{1,0},{2,3},{3,2},{4,5},{5,4},{6,7},{7,6},{8,9},{9,8},{10,11... | collective-permute-start | bytes 638984 | tf_op jit(solution)/shard_map/ppermute | solution.py:386
  114.8 10.3 %collective-permute-start.7 = (bf16[208,128]{1,0:T(8,128)(2,1)S(1)}, bf16[208,128]{1,0:T(8,128)(2,1)S(1)}, u32[]{:S(2)}, u32[]{:S(2)}) collective-permute-start(bf16[208,128]{1,0:T(8,128)(2,1)S(1)} %get-tuple-element.32), channel_id=1, source_target_pairs={{0,4},{2,6},{4,8},{6,10},{8,12},{10,14},{12,0},{14,2},{1,5},{3,7},... | collective-permute-start | bytes 159752 | tf_op jit(solution)/shard_map/ppermute | solution.py:389
  114.9 10.2 %collective-permute-start.8 = (bf16[208,128]{1,0:T(8,128)(2,1)S(1)}, bf16[208,128]{1,0:T(8,128)(2,1)S(1)}, u32[]{:S(2)}, u32[]{:S(2)}) collective-permute-start(bf16[208,128]{1,0:T(8,128)(2,1)S(1)} %get-tuple-element.33), channel_id=1, source_target_pairs={{0,8},{2,10},{4,12},{6,14},{8,0},{10,2},{12,4},{14,6},{1,9},{3,11}... | collective-permute-start | bytes 159752 | tf_op jit(solution)/shard_map/ppermute | solution.py:389
  116.9 8.2 %collective-permute-start.9 = (bf16[208,128]{1,0:T(8,128)(2,1)S(1)}, bf16[208,128]{1,0:T(8,128)(2,1)S(1)}, u32[]{:S(2)}, u32[]{:S(2)}) collective-permute-start(bf16[208,128]{1,0:T(8,128)(2,1)S(1)} %get-tuple-element.34), channel_id=1, source_target_pairs={{0,12},{2,14},{4,0},{6,2},{8,4},{10,6},{12,8},{14,10},{1,13},{3,15... | collective-permute-start | bytes 159752 | tf_op jit(solution)/shard_map/ppermute | solution.py:389
